TPU v7x, 256 devices: a whole 4x4x8 slice. The times are simulated.
256 devices in a mesh: ep: 64 (over z, y, core), tp: 4 (over x).
Axes of the slice: x: 4, y: 4, z: 8, core: 2. Of those that a mesh axis runs over, the one named last changes fastest.
Arguments:
- tokens: bfloat16 [1024, 2048], P('ep'), may hold values from -6 to 6
- norm_gain: bfloat16 [2048], replicated, may hold values from 0.099609375 to 1.8984375
- query_weight: bfloat16 [2048, 1024], P('ep', 'tp'), may hold values from -0.125 to 0.125
- key_weight: bfloat16 [2048, 1024], P('ep', 'tp'), may hold values from -0.125 to 0.125
- value_weight: bfloat16 [2048, 2048], P('ep', 'tp'), may hold values from -0.125 to 0.125
- outgate_weight: bfloat16 [2048, 2048], P('ep', 'tp'), may hold values from -0.125 to 0.125
- beta_weight: bfloat16 [2048, 16], replicated, may hold values from -0.125 to 0.125
- decay_weight: bfloat16 [2048, 16], replicated, may hold values from -0.125 to 0.125
- decay_rate: float32 [16], P('tp'), may hold values from 0.02 to 6
- decay_bias: float32 [16], P('tp'), may hold values from -3 to 3
- head_gain: bfloat16 [128], replicated, may hold values from 0.099609375 to 1.8984375
- recurrent: float32 [1024, 16, 128, 128], P('ep', 'tp'), may hold values from -3 to 3
- output_weight: bfloat16 [2048, 2048], P('tp', 'ep'), may hold values from -0.125 to 0.125
- ffn_gain: bfloat16 [2048], replicated, may hold values from 0.099609375 to 1.8984375
- routes: int32 [1024, 4], P('ep'), may hold values from 0 to 63, all different within a row; in each aligned block of 16 rows (0 to 15, 16 to 31, ...) at most 2 rows name the same one
- route_weight: float32 [1024, 4], P('ep'), may hold values from 0.1 to 1
- expert_gate: bfloat16 [64, 2048, 512], P('ep', None, 'tp'), may hold values from -0.125 to 0.125
- expert_up: bfloat16 [64, 2048, 512], P('ep', None, 'tp'), may hold values from -0.125 to 0.125
- expert_down: bfloat16 [64, 512, 2048], P('ep', 'tp'), may hold values from -0.25 to 0.25
- shared_gate: bfloat16 [2048, 512], P('ep', 'tp'), may hold values from -0.125 to 0.125
- shared_up: bfloat16 [2048, 512], P('ep', 'tp'), may hold values from -0.125 to 0.125
- shared_down: bfloat16 [512, 2048], P('tp', 'ep'), may hold values from -0.25 to 0.25
- branch_gate: bfloat16 [2048], replicated, may hold values from -0.125 to 0.125
Outputs:
- layer_out: bfloat16 [1024, 2048], P('ep')
- new_state: float32 [1024, 16, 128, 128], P('ep', 'tp')
Inputs may be any that keep to these rules, and one draw needn't show every extreme that they name: `routes`: each row names 4 different experts. Among the rows of one aligned block of 16 rows no expert is named more than 2 times, and some block reaches it: one expert is named exactly 2 times there.
All inputs are finite; a program needn't handle non-finite values.
Results may differ from a plain program's by a relative error of at most 0.019.
Values may be sent and summed in bfloat16 or wider, within the bound.
A program may use at most 64 MiB of HBM per device.

v0:
```python
import jax
import jax.numpy as jnp
from jax import lax
from jax.sharding import PartitionSpec as P

EPS = 1e-06
ROUTED_SCALE = 2.5


def side_by_side(arrays, axis, dim, along):
    both = jnp.concatenate(arrays, axis=along)
    whole, at, outs = (lax.all_gather(both, axis, axis=dim, tiled=True), 0, [])
    for a in arrays:
        outs.append(lax.slice_in_dim(whole, at, at + a.shape[along], axis=along))
        at += a.shape[along]
    return tuple(outs)


def copy_for_each(array, axis):
    copies = jnp.broadcast_to(array, (lax.axis_size(axis), *array.shape))
    return lax.all_to_all(copies, axis, split_axis=0, concat_axis=0, tiled=True)


def laid_out(pieces, dim):
    dims = list(pieces.shape[1:])
    dims[dim] *= pieces.shape[0]
    return jnp.moveaxis(pieces, 0, dim).reshape(dims)


def collect(array, axis, dim):
    pieces = copy_for_each(array, axis)
    return laid_out(pieces, dim)


def over_copies(array, axis):
    everything = copy_for_each(array, axis)
    return jnp.sum(everything.astype(jnp.float32), axis=0)


def in_blocks(array, dim, peers):
    dims = array.shape
    pieces = array.reshape(*dims[:dim], peers, dims[dim] // peers, *dims[dim + 1 :])
    return jnp.moveaxis(pieces, dim, 0)


def summed_on_arrival(array, axis, dim):
    pieces = in_blocks(array, dim, lax.axis_size(axis))
    arrived = lax.all_to_all(pieces, axis, split_axis=0, concat_axis=0, tiled=True)
    return arrived.astype(jnp.float32).sum(axis=0)


def rms_scale(values, gain):
    values = values.astype(jnp.float32)
    return (
        values
        * lax.rsqrt(jnp.mean(values * values, axis=-1, keepdims=True) + EPS)
        * gain.astype(jnp.float32)
    )


def unit_rows(values):
    return values * lax.rsqrt(jnp.sum(values * values, axis=-1, keepdims=True) + EPS)


def per_device(
    tokens,
    norm_gain,
    query_weight,
    key_weight,
    value_weight,
    outgate_weight,
    beta_weight,
    decay_weight,
    decay_rate,
    decay_bias,
    head_gain,
    recurrent,
    output_weight,
    ffn_gain,
    routes,
    route_weight,
    expert_gate,
    expert_up,
    expert_down,
    shared_gate,
    shared_up,
    shared_down,
    branch_gate,
):
    ep_count = lax.axis_size("ep")
    tp_count = lax.axis_size("tp")
    seq_local, width = tokens.shape
    heads_local, key_dim, value_dim = (recurrent.shape[1], recurrent.shape[2], recurrent.shape[3])
    normed = rms_scale(tokens, norm_gain).astype(jnp.bfloat16)
    query_cols = query_weight.shape[1]
    pieces = side_by_side((query_weight, key_weight, value_weight, outgate_weight), "ep", 0, 1)
    token_block = normed
    query_sum, key_sum, value_sum, gate_sum = tuple(
        (
            jnp.dot(token_block, weight_piece, preferred_element_type=jnp.float32)
            for weight_piece in pieces
        )
    )
    query_proj = query_sum.astype(jnp.bfloat16)
    key_proj = key_sum.astype(jnp.bfloat16)
    value_proj = value_sum.astype(jnp.bfloat16)
    gate_proj = gate_sum.astype(jnp.bfloat16)
    key_local = query_cols // key_dim
    repeat_count = heads_local // key_local
    queries = unit_rows(
        jax.nn.silu(query_proj.astype(jnp.float32)).reshape(seq_local, key_local, key_dim)
    )
    queries = jnp.repeat(queries, repeat_count, axis=1) * key_dim ** (-0.5)
    key_rows = unit_rows(
        jax.nn.silu(key_proj.astype(jnp.float32)).reshape(seq_local, key_local, key_dim)
    )
    key_rows = jnp.repeat(key_rows, repeat_count, axis=1)
    value_rows = jax.nn.silu(value_proj.astype(jnp.float32)).reshape(
        seq_local, heads_local, value_dim
    )
    head_start = lax.axis_index("tp") * heads_local
    beta_logit = jnp.dot(
        normed,
        lax.dynamic_slice_in_dim(beta_weight, head_start, heads_local, 1),
        preferred_element_type=jnp.float32,
    )
    decay_logit = jnp.dot(
        normed,
        lax.dynamic_slice_in_dim(decay_weight, head_start, heads_local, 1),
        preferred_element_type=jnp.float32,
    )
    strength = jax.nn.sigmoid(beta_logit)
    retain = jnp.exp(-decay_rate[None, :] * jax.nn.softplus(decay_logit + decay_bias[None, :]))
    decayed = recurrent * retain[:, :, None, None]
    predicted = jnp.einsum("shde,shd->she", decayed, key_rows)
    correction = strength[:, :, None] * (value_rows - predicted)
    new_state = decayed + key_rows[:, :, :, None] * correction[:, :, None, :]
    readout = jnp.einsum("shde,shd->she", new_state, queries)
    out_gate = jax.nn.silu(gate_proj.astype(jnp.float32)).reshape(seq_local, heads_local, value_dim)
    heads_out = (
        (rms_scale(readout, head_gain) * out_gate)
        .astype(jnp.bfloat16)
        .reshape(seq_local, heads_local * value_dim)
    )
    partial_mix = jnp.dot(
        heads_out, collect(output_weight, "ep", 1), preferred_element_type=jnp.float32
    )
    partial_mix = partial_mix.astype(jnp.bfloat16).astype(jnp.float32)
    mixed = over_copies(partial_mix.astype(jnp.bfloat16), "tp").astype(jnp.float32)
    residual = (tokens.astype(jnp.float32) + mixed).astype(jnp.bfloat16)
    ffn_in = rms_scale(residual, ffn_gain).astype(jnp.bfloat16)
    pieces = side_by_side((shared_gate, shared_up), "ep", 0, 1)
    token_block = ffn_in
    shared_g = jnp.dot(token_block, pieces[0], preferred_element_type=jnp.float32)
    shared_u = jnp.dot(token_block, pieces[1], preferred_element_type=jnp.float32)
    shared_act = (jax.nn.silu(shared_g) * shared_u).astype(jnp.bfloat16)
    shared_partial = jnp.dot(
        shared_act, collect(shared_down, "ep", 1), preferred_element_type=jnp.float32
    )
    shared_out = over_copies(
        shared_partial.astype(jnp.bfloat16).astype(jnp.float32).astype(jnp.bfloat16), "tp"
    ).astype(jnp.float32)
    topk = routes.shape[1]
    pair_count = seq_local * topk
    capacity = 2 * ((pair_count + ep_count - 1) // ep_count)
    expert_ids = routes.reshape(pair_count)
    onehot = (expert_ids[:, None] == jnp.arange(ep_count)[None, :]).astype(jnp.float32)
    earlier = (jnp.arange(pair_count)[:, None] > jnp.arange(pair_count)[None, :]).astype(
        jnp.float32
    )
    slots = jnp.sum(jnp.dot(earlier, onehot) * onehot, axis=1).astype(jnp.int32)
    target = expert_ids * capacity + slots
    placement_matrix = (target[:, None] == jnp.arange(ep_count * capacity)[None, :]).astype(
        jnp.bfloat16
    )
    dispatch_matrix = jnp.sum(
        placement_matrix.reshape(seq_local, topk, ep_count * capacity).astype(jnp.float32), axis=1
    ).astype(jnp.bfloat16)
    outgoing = jnp.dot(dispatch_matrix.T, ffn_in, preferred_element_type=jnp.float32).astype(
        jnp.bfloat16
    )
    outgoing = outgoing.reshape(ep_count, capacity, width)
    share_cols = width // tp_count
    received = lax.all_to_all(outgoing, "ep", split_axis=0, concat_axis=0, tiled=True)
    flat_rows = received.reshape(-1, width)
    gate_part = jnp.dot(flat_rows, expert_gate[0], preferred_element_type=jnp.float32)
    up_part = jnp.dot(flat_rows, expert_up[0], preferred_element_type=jnp.float32)
    act = (jax.nn.silu(gate_part) * up_part).astype(jnp.bfloat16)
    partial_rows = (
        jnp.dot(act, expert_down[0], preferred_element_type=jnp.float32)
        .astype(jnp.bfloat16)
        .astype(jnp.float32)
    )
    part_cols = summed_on_arrival(partial_rows.astype(jnp.bfloat16), "tp", 1).astype(jnp.bfloat16)
    returned = lax.all_to_all(
        part_cols.reshape(received.shape[0], received.shape[1], share_cols),
        "ep",
        split_axis=0,
        concat_axis=0,
        tiled=True,
    )
    scaled = route_weight / jnp.sum(route_weight, axis=1, keepdims=True) * ROUTED_SCALE
    branch = jax.nn.sigmoid(jnp.dot(ffn_in, branch_gate, preferred_element_type=jnp.float32))
    col_begin = lax.axis_index("tp") * share_cols
    pair_out = jnp.dot(
        placement_matrix,
        returned.reshape(ep_count * capacity, share_cols),
        preferred_element_type=jnp.float32,
    )
    moe_cols = jnp.sum(pair_out.reshape(seq_local, topk, share_cols) * scaled[:, :, None], axis=1)
    resid_part = lax.dynamic_slice_in_dim(residual, col_begin, share_cols, 1).astype(jnp.float32)
    shared_part = lax.dynamic_slice_in_dim(shared_out, col_begin, share_cols, 1)
    out_cols = (resid_part + moe_cols + branch[:, None] * shared_part).astype(jnp.bfloat16)
    layer_out = collect(out_cols, "tp", 1)
    return (layer_out, new_state)


def solution(mesh):
    return jax.shard_map(
        per_device,
        mesh=mesh,
        in_specs=(
            P("ep", None),
            P(),
            P("ep", "tp"),
            P("ep", "tp"),
            P("ep", "tp"),
            P("ep", "tp"),
            P(),
            P(),
            P("tp"),
            P("tp"),
            P(),
            P("ep", "tp", None, None),
            P("tp", "ep"),
            P(),
            P("ep", None),
            P("ep", None),
            P("ep", None, "tp"),
            P("ep", None, "tp"),
            P("ep", "tp", None),
            P("ep", "tp"),
            P("ep", "tp"),
            P("tp", "ep"),
            P(),
        ),
        out_specs=(P("ep", None), P("ep", "tp", None, None)),
        check_vma=False,
    )
```

profile of v0, /device:TPU:1, one launch (start us, length us, event | category | flops | bytes accessed | tf_op | source)
XLA Modules:
  0.0 266.9 jit_solution(13242425956207793846)
XLA Ops:
  8.8 2.3 broadcast_in_dim.16
  11.1 13.1 %all-to-all-start = ((bf16[64,512,32]{1,2,0:T(8,128)(2,1)}), bf16[64,512,32]{1,2,0:T(8,128)(2,1)S(1)}, u32[]{:S(2)}, u32[]{:S(2)}) async-start(bf16[64,512,32]{1,2,0:T(8,128)(2,1)} %broadcast_in_dim.16), calls=%async_computation | async-start | bytes 4194304 | tf_op jit(solution)/shard_map/all_to_all | solution.py:21
  27.2 74.0 %all-gather.3.cloned.1.call-done = bf16[2048,1536]{1,0:T(8,128)(2,1)} async-done(((bf16[32,1536]{1,0:T(8,128)(2,1)}), bf16[2048,1536]{1,0:T(8,128)(2,1)}) %all-gather.3.cloned.1.call-update) | async-done | bytes 6291472 | tf_op jit(solution)/shard_map/all_gather | solution.py:12
  101.1 1.5 divide_multiply_fusion.2
  102.7 1.5 divide_multiply_fusion.3
  104.2 2.0 divide_multiply_fusion.1
  106.3 2.0 divide_multiply_fusion
  108.8 3.1 %fusion = f32[16,4,1,128]{3,2,1,0:T(1,128)S(1)} fusion(f32[16,4,128,1]{2,3,1,0:T(1,128)S(1)} %bitcast.70, f32[16,4,128,128]{3,2,1,0:T(8,128)} %param.34, f32[16,4]{1,0:T(8,128)S(1)} %copy.58), kind=kOutput, calls=%fused_computation.1 | convolution fusion | flops 3145728 | bytes 4260096 | tf_op jit(solution)/shard_map/shde,shd->she/dot_general | solution.py:135
  113.5 2.0 copy-done.2
  117.8 3.9 %all-to-all-start.1 = ((bf16[4,16,2048]{2,1,0:T(8,128)(2,1)}), bf16[4,16,2048]{2,1,0:T(8,128)(2,1)S(1)}, u32[]{:S(2)}, u32[]{:S(2)}) async-start(bf16[4,16,2048]{2,1,0:T(8,128)(2,1)} %broadcast_in_dim.17), calls=%async_computation.1 | async-start | bytes 524288 | tf_op jit(solution)/shard_map/all_to_all | solution.py:21
  121.7 5.8 %all-to-all-done.1 = bf16[4,16,2048]{2,1,0:T(8,128)(2,1)S(1)} async-done(((bf16[4,16,2048]{2,1,0:T(8,128)(2,1)}), bf16[4,16,2048]{2,1,0:T(8,128)(2,1)S(1)}, u32[]{:S(2)}, u32[]{:S(2)}) %all-to-all-start.1) | async-done | bytes 262176 | tf_op jit(solution)/shard_map/all_to_all | solution.py:21
  129.3 9.7 %all-to-all-start.2 = ((bf16[64,2,2048]{2,1,0:T(2,128)(2,1)}), bf16[64,2,2048]{2,1,0:T(2,128)(2,1)S(1)}, u32[]{:S(2)}, u32[]{:S(2)}) async-start(bf16[64,2,2048]{2,1,0:T(2,128)(2,1)} %reshape.147), calls=%async_computation.2 | async-start | bytes 1048576 | tf_op jit(solution)/shard_map/all_to_all | solution.py:184
  139.8 16.9 %all-to-all-done.2 = bf16[64,2,2048]{2,1,0:T(2,128)(2,1)S(1)} async-done(((bf16[64,2,2048]{2,1,0:T(2,128)(2,1)}), bf16[64,2,2048]{2,1,0:T(2,128)(2,1)S(1)}, u32[]{:S(2)}, u32[]{:S(2)}) %all-to-all-start.2) | async-done | bytes 524320 | tf_op jit(solution)/shard_map/all_to_all | solution.py:184
  157.6 5.7 %all-to-all-start.5 = ((bf16[64,128,32]{1,2,0:T(8,128)(2,1)}), bf16[64,128,32]{1,2,0:T(8,128)(2,1)S(1)}, u32[]{:S(2)}, u32[]{:S(2)}) async-start(bf16[64,128,32]{1,2,0:T(8,128)(2,1)} %broadcast_in_dim.18), calls=%async_computation.5 | async-start | bytes 1048576 | tf_op jit(solution)/shard_map/all_to_all | solution.py:21
  163.8 1.6 convolution_convert_fusion
  166.3 15.0 %all-to-all-done.5 = bf16[64,128,32]{1,2,0:T(8,128)(2,1)S(1)} async-done(((bf16[64,128,32]{1,2,0:T(8,128)(2,1)}), bf16[64,128,32]{1,2,0:T(8,128)(2,1)S(1)}, u32[]{:S(2)}, u32[]{:S(2)}) %all-to-all-start.5) | async-done | bytes 524320 | tf_op jit(solution)/shard_map/all_to_all | solution.py:21
  181.3 3.5 %all-to-all-start.3 = ((bf16[4,128,512]{2,1,0:T(8,128)(2,1)}), bf16[4,128,512]{2,1,0:T(8,128)(2,1)S(1)}, u32[]{:S(2)}, u32[]{:S(2)}) async-start(bf16[4,128,512]{2,1,0:T(8,128)(2,1)} %bitcast.66), calls=%async_computation.3 | async-start | bytes 1048576 | tf_op jit(solution)/shard_map/all_to_all | solution.py:48
  184.7 34.9 %all-gather.5.cloned.1.call-done = bf16[2048,256]{1,0:T(8,128)(2,1)} async-done(((bf16[32,256]{1,0:T(8,128)(2,1)}), bf16[2048,256]{1,0:T(8,128)(2,1)}) %all-gather.5.cloned.1.call-update) | async-done | bytes 1048592 | tf_op jit(solution)/shard_map/all_gather | solution.py:12
  220.9 1.5 convolution_convert_fusion.2
  223.1 4.0 %all-to-all-start.6 = ((bf16[4,16,2048]{2,1,0:T(8,128)(2,1)}), bf16[4,16,2048]{2,1,0:T(8,128)(2,1)S(1)}, u32[]{:S(2)}, u32[]{:S(2)}) async-start(bf16[4,16,2048]{2,1,0:T(8,128)(2,1)} %broadcast_in_dim.19), calls=%async_computation.6 | async-start | bytes 524288 | tf_op jit(solution)/shard_map/all_to_all | solution.py:21
  227.9 5.1 %all-to-all-done.6 = bf16[4,16,2048]{2,1,0:T(8,128)(2,1)S(1)} async-done(((bf16[4,16,2048]{2,1,0:T(8,128)(2,1)}), bf16[4,16,2048]{2,1,0:T(8,128)(2,1)S(1)}, u32[]{:S(2)}, u32[]{:S(2)}) %all-to-all-start.6) | async-done | bytes 262176 | tf_op jit(solution)/shard_map/all_to_all | solution.py:21
  233.0 8.2 %all-to-all-start.4 = ((bf16[64,2,512]{2,1,0:T(2,128)(2,1)}), bf16[64,2,512]{2,1,0:T(2,128)(2,1)S(1)}, u32[]{:S(2)}, u32[]{:S(2)}) async-start(bf16[64,2,512]{2,1,0:T(2,128)(2,1)} %reshape.150), calls=%async_computation.4 | async-start | bytes 262144 | tf_op jit(solution)/shard_map/all_to_all | solution.py:195
  241.4 10.8 %all-to-all-done.4 = bf16[64,2,512]{2,1,0:T(2,128)(2,1)S(1)} async-done(((bf16[64,2,512]{2,1,0:T(2,128)(2,1)}), bf16[64,2,512]{2,1,0:T(2,128)(2,1)S(1)}, u32[]{:S(2)}, u32[]{:S(2)}) %all-to-all-start.4) | async-done | bytes 131104 | tf_op jit(solution)/shard_map/all_to_all | solution.py:195
  252.6 6.8 %all_to_all.40 = bf16[4,16,512]{2,1,0:T(8,128)(2,1)S(1)} all-to-all(bf16[4,16,512]{2,1,0:T(8,128)(2,1)S(1)} %broadcast_in_dim.20), channel_id=1, replica_groups=mesh['ep'=64,'tp'=4] {'tp'}, dimensions={0} | all-to-all | bytes 131072 | tf_op jit(solution)/shard_map/all_to_all | solution.py:21
  (100 shorter events, 17.4 us)
Async XLA Ops:
  7.2 156.7 %copy-start = (bf16[1,128,2048]{2,1,0:T(8,128)(2,1)S(1)}, bf16[1,128,2048]{2,1,0:T(8,128)(2,1)}, u32[]{:S(2)}) copy-start(bf16[1,128,2048]{2,1,0:T(8,128)(2,1)} %param.41) | copy-start | bytes 1572868
  7.2 17.1 %copy-start.13 = (f32[4]{0:T(128)S(1)}, f32[4]{0:T(128)}, u32[]{:S(2)}) copy-start(f32[4]{0:T(128)} %param.31) | copy-start | bytes 52
  7.2 17.1 %copy-start.10 = (bf16[2048]{0:T(1024)(128)(2,1)S(1)}, bf16[2048]{0:T(1024)(128)(2,1)}, u32[]{:S(2)}) copy-start(bf16[2048]{0:T(1024)(128)(2,1)} %param.24) | copy-start | bytes 12292
  7.2 17.1 %copy-start.6 = (s32[16,4]{0,1:T(4,128)S(1)}, s32[16,4]{0,1:T(4,128)}, u32[]{:S(2)}) copy-start(s32[16,4]{0,1:T(4,128)} %param.37) | copy-start | bytes 772
  7.2 17.3 %copy-start.4 = (bf16[16,2048]{1,0:T(8,128)(2,1)S(1)}, bf16[16,2048]{1,0:T(8,128)(2,1)}, u32[]{:S(2)}) copy-start(bf16[16,2048]{1,0:T(8,128)(2,1)} %param.23) | copy-start | bytes 196612
  7.2 18.4 %copy-start.14 = (f32[4]{0:T(128)S(1)}, f32[4]{0:T(128)}, u32[]{:S(2)}) copy-start(f32[4]{0:T(128)} %param.32) | copy-start | bytes 52
  7.2 19.6 %copy-start.15 = (bf16[128]{0:T(256)(128)(2,1)S(1)}, bf16[128]{0:T(256)(128)(2,1)}, u32[]{:S(2)}) copy-start(bf16[128]{0:T(256)(128)(2,1)} %param.33) | copy-start | bytes 772
  7.2 93.9 %all-gather.3.cloned.1.call-start = ((), (), s32[]{:S(2)}) async-start(), calls=%async_computation.8 | async-start | bytes 6389760 | tf_op jit(solution)/shard_map/all_gather | solution.py:12
  11.1 105.3 %all-to-all-start = ((bf16[64,512,32]{1,2,0:T(8,128)(2,1)}), bf16[64,512,32]{1,2,0:T(8,128)(2,1)S(1)}, u32[]{:S(2)}, u32[]{:S(2)}) async-start(bf16[64,512,32]{1,2,0:T(8,128)(2,1)} %broadcast_in_dim.16), calls=%async_computation | async-start | bytes 4194304 | tf_op jit(solution)/shard_map/all_to_all | solution.py:21
  108.3 3.6 %copy-start.1 = (f32[16,4,128,128]{3,2,1,0:T(8,128)S(1)}, f32[16,4,128,128]{3,2,1,0:T(8,128)}, u32[]{:S(2)}) copy-start(f32[16,4,128,128]{3,2,1,0:T(8,128)} %param.34) | copy-start | bytes 12582916
  113.5 8.1 %copy-start.11 = (bf16[2048]{0:T(1024)(128)(2,1)S(1)}, bf16[2048]{0:T(1024)(128)(2,1)}, u32[]{:S(2)}) copy-start(bf16[2048]{0:T(1024)(128)(2,1)} %param.36) | copy-start | bytes 12292
  116.2 22.9 %copy-start.8 = (bf16[32,128]{1,0:T(8,128)(2,1)S(1)}, bf16[32,128]{1,0:T(8,128)(2,1)}, u32[]{:S(2)}) copy-start(bf16[32,128]{1,0:T(8,128)(2,1)} %param.43) | copy-start | bytes 24580
  116.2 22.9 %copy-start.9 = (bf16[32,128]{1,0:T(8,128)(2,1)S(1)}, bf16[32,128]{1,0:T(8,128)(2,1)}, u32[]{:S(2)}) copy-start(bf16[32,128]{1,0:T(8,128)(2,1)} %param.42) | copy-start | bytes 24580
  116.2 40.5 %copy-start.5 = (bf16[128,32]{0,1:T(8,128)(2,1)S(1)}, bf16[128,32]{0,1:T(8,128)(2,1)}, u32[]{:S(2)}) copy-start(bf16[128,32]{0,1:T(8,128)(2,1)} %param.44) | copy-start | bytes 24580
  116.2 47.1 %copy-start.12 = (bf16[2048]{0:T(1024)(128)(2,1)S(1)}, bf16[2048]{0:T(1024)(128)(2,1)}, u32[]{:S(2)}) copy-start(bf16[2048]{0:T(1024)(128)(2,1)} %param.45) | copy-start | bytes 12292
  116.2 47.1 %copy-start.7 = (f32[16,4]{0,1:T(4,128)S(1)}, f32[16,4]{0,1:T(4,128)}, u32[]{:S(2)}) copy-start(f32[16,4]{0,1:T(4,128)} %param.38) | copy-start | bytes 772
  116.4 47.1 %copy-start.3 = (bf16[1,2048,128]{2,1,0:T(8,128)(2,1)S(1)}, bf16[1,2048,128]{2,1,0:T(8,128)(2,1)}, u32[]{:S(2)}) copy-start(bf16[1,2048,128]{2,1,0:T(8,128)(2,1)} %param.39) | copy-start | bytes 1572868
  117.8 9.8 %all-to-all-start.1 = ((bf16[4,16,2048]{2,1,0:T(8,128)(2,1)}), bf16[4,16,2048]{2,1,0:T(8,128)(2,1)S(1)}, u32[]{:S(2)}, u32[]{:S(2)}) async-start(bf16[4,16,2048]{2,1,0:T(8,128)(2,1)} %broadcast_in_dim.17), calls=%async_computation.1 | async-start | bytes 524288 | tf_op jit(solution)/shard_map/all_to_all | solution.py:21
  129.3 27.4 %all-to-all-start.2 = ((bf16[64,2,2048]{2,1,0:T(2,128)(2,1)}), bf16[64,2,2048]{2,1,0:T(2,128)(2,1)S(1)}, u32[]{:S(2)}, u32[]{:S(2)}) async-start(bf16[64,2,2048]{2,1,0:T(2,128)(2,1)} %reshape.147), calls=%async_computation.2 | async-start | bytes 1048576 | tf_op jit(solution)/shard_map/all_to_all | solution.py:184
  139.0 80.6 %all-gather.5.cloned.1.call-start = ((), (), s32[]{:S(2)}) async-start(), calls=%async_computation.9 | async-start | bytes 1064960 | tf_op jit(solution)/shard_map/all_gather | solution.py:12
  157.6 23.7 %all-to-all-start.5 = ((bf16[64,128,32]{1,2,0:T(8,128)(2,1)}), bf16[64,128,32]{1,2,0:T(8,128)(2,1)S(1)}, u32[]{:S(2)}, u32[]{:S(2)}) async-start(bf16[64,128,32]{1,2,0:T(8,128)(2,1)} %broadcast_in_dim.18), calls=%async_computation.5 | async-start | bytes 1048576 | tf_op jit(solution)/shard_map/all_to_all | solution.py:21
  181.3 41.1 %all-to-all-start.3 = ((bf16[4,128,512]{2,1,0:T(8,128)(2,1)}), bf16[4,128,512]{2,1,0:T(8,128)(2,1)S(1)}, u32[]{:S(2)}, u32[]{:S(2)}) async-start(bf16[4,128,512]{2,1,0:T(8,128)(2,1)} %bitcast.66), calls=%async_computation.3 | async-start | bytes 1048576 | tf_op jit(solution)/shard_map/all_to_all | solution.py:48
  223.1 9.9 %all-to-all-start.6 = ((bf16[4,16,2048]{2,1,0:T(8,128)(2,1)}), bf16[4,16,2048]{2,1,0:T(8,128)(2,1)S(1)}, u32[]{:S(2)}, u32[]{:S(2)}) async-start(bf16[4,16,2048]{2,1,0:T(8,128)(2,1)} %broadcast_in_dim.19), calls=%async_computation.6 | async-start | bytes 524288 | tf_op jit(solution)/shard_map/all_to_all | solution.py:21
  233.0 19.3 %all-to-all-start.4 = ((bf16[64,2,512]{2,1,0:T(2,128)(2,1)}), bf16[64,2,512]{2,1,0:T(2,128)(2,1)S(1)}, u32[]{:S(2)}, u32[]{:S(2)}) async-start(bf16[64,2,512]{2,1,0:T(2,128)(2,1)} %reshape.150), calls=%async_computation.4 | async-start | bytes 262144 | tf_op jit(solution)/shard_map/all_to_all | solution.py:195
  (1 other events, 2.0 us)
Sparse Core Ops, SparseCore 0:
  11.4 89.7 all-gather.2
  143.2 76.4 all-gather.4
where the time goes:
time: 268 us; the launch traced here: 267 us
  waiting for transfers between devices  163 us (61%)
  starting transfers between devices  48.1 us (18%)
  matrix products  19 us (7%)
  between operations  14.6 us (5%)
  local copies, waits for them, and re-layouts  10.9 us (4%)
  blocking collectives  6.84 us (3%)
  other arithmetic  4.85 us (2%)
    all_gather x2, waiting for transfers between devices, side_by_side(): whole, at, outs = (lax.all_gather(both, axis, axis=dim, tiled=True), 0, [])  109 us
    all_to_all x4, starting transfers between devices, copy_for_each(): return lax.all_to_all(copies, axis, split_axis=0, concat_axis=0, tiled=True)  26.7 us
    all_to_all x4, waiting for transfers between devices, copy_for_each(): return lax.all_to_all(copies, axis, split_axis=0, concat_axis=0, tiled=True)  25.9 us
    all_to_all x1, waiting for transfers between devices, per_device(): lax.all_to_all(outgoing, 'ep', split_axis=0, concat_axis=0, tiled=True)  16.9 us
    all_to_all x1, waiting for transfers between devices, per_device(): lax.all_to_all(part_cols.reshape(received.shape[0], received.shape[1], sh...  10.8 us
    all_to_all x1, starting transfers between devices, per_device(): lax.all_to_all(outgoing, 'ep', split_axis=0, concat_axis=0, tiled=True)  9.74 us
    all_to_all x1, starting transfers between devices, per_device(): lax.all_to_all(part_cols.reshape(received.shape[0], received.shape[1], sh...  8.16 us
    dot_general x4, matrix products, per_device(): jnp.dot(token_block, weight_piece, preferred_element_type=jnp.float32)  7.1 us
  transfers between devices with their start and end apart: 9, of which 7 were waited for; matrix products, arithmetic and copies ran while one was open for 10% of the time, Pallas kernels for 0%

commit v1 on v0

--- a/solution.py
+++ b/solution.py
@@ -1,10 +1,328 @@
+import functools
+
 import jax
 import jax.numpy as jnp
 from jax import lax
+from jax.experimental import pallas as pl
+from jax.experimental.pallas import tpu as pltpu
 from jax.sharding import PartitionSpec as P
 
 EPS = 1e-06
 ROUTED_SCALE = 2.5
+NZ, NY, NC = 8, 4, 2
+MESH = pl.DeviceIdType.MESH
+BF = jnp.bfloat16
+F32 = jnp.float32
+
+
+def silu(v):
+    return v / (1.0 + jnp.exp(-v))
+
+
+def sigmoid(v):
+    return 1.0 / (1.0 + jnp.exp(-v))
+
+
+def rms(values, gain):
+    return (
+        values
+        * lax.rsqrt(jnp.mean(values * values, axis=-1, keepdims=True) + EPS)
+        * gain
+    )
+
+
+def unit(v):
+    return v * lax.rsqrt(jnp.sum(v * v, axis=-1, keepdims=True) + EPS)
+
+
+def attn_kernel(
+    tokens, norm_gain, wq, wk, wv, wg, bw, dw, rate, bias, head_gain, rec, ow, ffn_gain,
+    residual_out, ffn_out, state_out,
+    state, wbuf, tok_src, tokbuf, psend, prec, obuf, mix_send, mix_rec,
+    kt, qt, vals, rs_ref, corr, ro,
+    load_sem, w_s, w_r, wf_s, wf_r, t_s, t_r, p_s, p_r, o1_s, o1_r, o2_s, o2_r, o3_s, o3_r, m_s, m_r,
+    st_sem,
+):
+    e = lax.axis_index("ep")
+    x = lax.axis_index("tp")
+    nx = lax.axis_size("tp")
+    z, yc = e // (NY * NC), e % (NY * NC)
+    y, c = yc // NC, yc % NC
+    partner = e + 1 - 2 * c
+    zdev = lambda d: ((z + d) % NZ) * (NY * NC) + yc
+    ydev = lambda d: z * (NY * NC) + ((y + d) % NY) * NC + c
+
+    def rcopy(src, dst, ss, rs, ep, tp):
+        return pltpu.make_async_remote_copy(
+            src_ref=src, dst_ref=dst, send_sem=ss, recv_sem=rs, device_id=(ep, tp), device_id_type=MESH
+        )
+
+    barrier = pltpu.get_barrier_semaphore()
+    for d in range(1, NZ):
+        pl.semaphore_signal(barrier, inc=1, device_id=(zdev(d), x), device_id_type=MESH)
+    for d in range(1, NY):
+        pl.semaphore_signal(barrier, inc=1, device_id=(ydev(d), x), device_id_type=MESH)
+    pl.semaphore_signal(barrier, inc=1, device_id=(partner, x), device_id_type=MESH)
+    for d in range(1, nx):
+        pl.semaphore_signal(barrier, inc=1, device_id=(e, (x + d) % nx), device_id_type=MESH)
+
+    loads = []
+    at = 0
+    for i, w in enumerate((wq, wk, wv, wg)):
+        n = w.shape[1]
+        loads.append(pltpu.make_async_copy(w, wbuf.at[yc, :, at : at + n], load_sem.at[i]))
+        at += n
+    for l in loads:
+        l.start()
+    load_state = pltpu.make_async_copy(rec, state, load_sem.at[4])
+    load_state.start()
+
+    normed = rms(tokens[...].astype(F32), norm_gain[...].astype(F32)).astype(BF)
+    kz = tokbuf.shape[2]
+    for i in range(NZ):
+        tok_src[i] = normed[:, i * kz : (i + 1) * kz]
+    n_own = ow.shape[1]
+    eye = (
+        lax.broadcasted_iota(jnp.int32, (n_own, n_own), 0)
+        == lax.broadcasted_iota(jnp.int32, (n_own, n_own), 1)
+    ).astype(BF)
+    obuf[e] = lax.dot_general(
+        eye, ow[...], (((1,), (1,)), ((), ())), preferred_element_type=F32
+    ).astype(BF)
+    for l in loads:
+        l.wait()
+    pl.semaphore_wait(barrier, (NZ - 1) + (NY - 1) + 1 + (nx - 1))
+
+    toks = [
+        rcopy(tok_src.at[(z + d) % NZ], tokbuf.at[d], t_s.at[d], t_r.at[d], zdev(d), x)
+        for d in range(1, NZ)
+    ]
+    for cp in toks:
+        cp.start()
+    ws = [rcopy(wbuf.at[yc], wbuf.at[yc], w_s.at[d], w_r.at[d], ydev(d), x) for d in range(1, NY)]
+    for cp in ws:
+        cp.start()
+    fwd = [rcopy(wbuf.at[yc], wbuf.at[yc], wf_s.at[0], wf_r.at[0], partner, x)]
+    fwd[0].start()
+    o1 = [rcopy(obuf.at[e], obuf.at[e], o1_s.at[d], o1_r.at[d], zdev(d), x) for d in range(1, NZ)]
+    for cp in o1:
+        cp.start()
+    tokbuf[0] = tok_src[z]
+
+    bl = jnp.dot(normed, bw[...], preferred_element_type=F32)
+    dl = jnp.dot(normed, dw[...], preferred_element_type=F32)
+    lanes = lax.broadcasted_iota(jnp.int32, bl.shape, 1)
+    heads = rec.shape[1]
+    retain, strength = [], []
+    for h in range(heads):
+        mine = lanes == x * heads + h
+        b = jnp.sum(jnp.where(mine, bl, 0.0), axis=1, keepdims=True)
+        g = jnp.sum(jnp.where(mine, dl, 0.0), axis=1, keepdims=True) + bias[0, h]
+        soft = jnp.maximum(g, 0.0) + jnp.log1p(jnp.exp(-jnp.abs(g)))
+        strength.append(sigmoid(b))
+        retain.append(jnp.exp(-rate[0, h] * soft))
+    lane = lax.broadcasted_iota(jnp.int32, rs_ref.shape, 1)
+    packed = jnp.zeros(rs_ref.shape, F32)
+    for h in range(heads):
+        packed = jnp.where(lane == h, retain[h], packed)
+        packed = jnp.where(lane == heads + h, strength[h], packed)
+
+    for d in range(1, NY):
+        ws[d - 1].wait_recv()
+        j = ((y + NY - d) % NY) * NC + c
+        cp = rcopy(wbuf.at[j], wbuf.at[j], wf_s.at[d], wf_r.at[d], partner, x)
+        cp.start()
+        fwd.append(cp)
+    for cp in toks:
+        cp.wait_recv()
+    for cp in fwd:
+        cp.wait_recv()
+    cols = wbuf.shape[2]
+    seqs = tokens.shape[0]
+    partial = jnp.dot(
+        tokbuf[...].reshape(NZ * seqs, kz), wbuf[...].reshape(kz, cols), preferred_element_type=F32
+    ).astype(BF)
+    psend[...] = partial.reshape(NZ, seqs, cols)
+    sums = [
+        rcopy(psend.at[d], prec.at[d], p_s.at[d], p_r.at[d], zdev(NZ - d), x) for d in range(1, NZ)
+    ]
+    for d in (4, 3, 5, 2, 6, 1, 7):
+        sums[d - 1].start()
+
+    o2, o3 = [], []
+    for d in range(NZ):
+        if d:
+            o1[d - 1].wait_recv()
+        j = ((z + NZ - d) % NZ) * (NY * NC) + yc
+        for dy in range(1, NY):
+            cp = rcopy(obuf.at[j], obuf.at[j], o2_s.at[dy, d], o2_r.at[dy, d], ydev(dy), x)
+            cp.start()
+            o2.append((dy, d, cp))
+        cp = rcopy(obuf.at[j], obuf.at[j], o3_s.at[0, d], o3_r.at[0, d], partner, x)
+        cp.start()
+        o3.append(cp)
+
+    for cp in sums:
+        cp.wait_recv()
+    total = psend[0].astype(F32)
+    for d in range(1, NZ):
+        total = total + prec[d].astype(F32)
+    proj = total.astype(BF).astype(F32)
+
+    for dy, d, cp in o2:
+        cp.wait_recv()
+        j = ((z + NZ - d) % NZ) * (NY * NC) + ((y + NY - dy) % NY) * NC + c
+        f = rcopy(obuf.at[j], obuf.at[j], o3_s.at[dy, d], o3_r.at[dy, d], partner, x)
+        f.start()
+        o3.append(f)
+
+    dk = rec.shape[2]
+    dv = rec.shape[3]
+    khs = wq.shape[1] // dk
+    per = heads // khs
+    qs, ks, kq = [], [], []
+    for i in range(khs):
+        q = unit(silu(proj[:, i * dk : (i + 1) * dk])) * dk ** (-0.5)
+        k = unit(silu(proj[:, (khs + i) * dk : (khs + i + 1) * dk]))
+        kt[i] = k.T
+        qt[i] = q.T
+        kq.append(jnp.sum(k * q, axis=1, keepdims=True))
+    for i in range(khs):
+        packed = jnp.where(lane == 2 * heads + i, kq[i], packed)
+    rs_ref[...] = packed
+    vbase = 2 * khs * dk
+    for h in range(heads):
+        vals[h] = silu(proj[:, vbase + h * dv : vbase + (h + 1) * dv])
+    gate = proj[:, vbase + heads * dv :]
+    load_state.wait()
+
+    def column(ref, i, s):
+        t = ref[i]
+        pick = lax.broadcasted_iota(jnp.int32, t.shape, 1) == s
+        return jnp.sum(jnp.where(pick, t, 0.0), axis=1, keepdims=True)
+
+    def read_one(s, carry):
+        rowrs = rs_ref[pl.ds(s, 1), :]
+        for i in range(khs):
+            kcol = column(kt, i, s)
+            qcol = column(qt, i, s)
+            dotkq = rowrs[:, 2 * heads + i : 2 * heads + i + 1]
+            for h in range(i * per, (i + 1) * per):
+                st = state[s, h]
+                ret = rowrs[:, h : h + 1]
+                pred = jnp.sum(st * kcol, axis=0, keepdims=True) * ret
+                base = jnp.sum(st * qcol, axis=0, keepdims=True) * ret
+                cor = rowrs[:, heads + h : heads + h + 1] * (
+                    vals[h, pl.ds(s, 1), :] - pred
+                )
+                corr[h, pl.ds(s, 1), :] = cor
+                ro[h, pl.ds(s, 1), :] = base + dotkq * cor
+        return carry
+
+    lax.fori_loop(0, seqs, read_one, 0)
+
+    hg = head_gain[...].astype(F32)
+    parts = []
+    for h in range(heads):
+        parts.append(
+            rms(ro[h], hg) * silu(gate[:, h * dv : (h + 1) * dv])
+        )
+    heads_out = jnp.concatenate(parts, axis=1).astype(BF)
+    for cp in o3:
+        cp.wait_recv()
+    width = tokens.shape[1]
+    mix_send[...] = lax.dot_general(
+        heads_out,
+        obuf[...].reshape(width, heads * dv),
+        (((1,), (1,)), ((), ())),
+        preferred_element_type=F32,
+    ).astype(BF)
+    mixes = [
+        rcopy(mix_send, mix_rec.at[d], m_s.at[d], m_r.at[d], e, (x + d) % nx) for d in range(1, nx)
+    ]
+    for cp in mixes:
+        cp.start()
+
+    def write_one(s, carry):
+        rowrs = rs_ref[pl.ds(s, 1), :]
+        for i in range(khs):
+            kcol = column(kt, i, s)
+            for h in range(i * per, (i + 1) * per):
+                state[s, h] = state[s, h] * rowrs[:, h : h + 1] + kcol * corr[h, pl.ds(s, 1), :]
+        return carry
+
+    lax.fori_loop(0, seqs, write_one, 0)
+    store_state = pltpu.make_async_copy(state, state_out, st_sem)
+    store_state.start()
+
+    mixed = mix_send[...].astype(F32)
+    for d in range(1, nx):
+        mixes[d - 1].wait_recv()
+        mixed = mixed + mix_rec[d].astype(F32)
+    residual = (tokens[...].astype(F32) + mixed).astype(BF)
+    residual_out[...] = residual
+    ffn_out[...] = rms(residual.astype(F32), ffn_gain[...].astype(F32)).astype(BF)
+
+    for group in (toks, ws, o1, fwd, sums, [t[2] for t in o2], o3, mixes):
+        for cp in group:
+            cp.wait_send()
+    store_state.wait()
+
+
+def attention(tokens, norm_gain, wq, wk, wv, wg, bw, dw, rate, bias, head_gain, rec, ow, ffn_gain):
+    nx = lax.axis_size("tp")
+    seqs, width = tokens.shape
+    heads, dk, dv = rec.shape[1:]
+    cols = wq.shape[1] + wk.shape[1] + wv.shape[1] + wg.shape[1]
+    rows = wq.shape[0]
+    kz = rows * NY * NC
+    vmem = pl.BlockSpec(memory_space=pltpu.VMEM)
+    smem = pl.BlockSpec(memory_space=pltpu.SMEM)
+    hbm = pl.BlockSpec(memory_space=pl.ANY)
+    dma = pltpu.SemaphoreType.DMA
+    ep = NZ * NY * NC
+    khs = wq.shape[1] // dk
+    return pl.pallas_call(
+        attn_kernel,
+        out_shape=(
+            jax.ShapeDtypeStruct((seqs, width), BF),
+            jax.ShapeDtypeStruct((seqs, width), BF),
+            jax.ShapeDtypeStruct(rec.shape, F32),
+        ),
+        in_specs=[vmem, vmem, hbm, hbm, hbm, hbm, vmem, vmem, smem, smem, vmem, hbm, vmem, vmem],
+        out_specs=(vmem, vmem, hbm),
+        scratch_shapes=[
+            pltpu.VMEM(rec.shape, F32),
+            pltpu.VMEM((NY * NC, rows, cols), BF),
+            pltpu.VMEM((NZ, seqs, kz), BF),
+            pltpu.VMEM((NZ, seqs, kz), BF),
+            pltpu.VMEM((NZ, seqs, cols), BF),
+            pltpu.VMEM((NZ, seqs, cols), BF),
+            pltpu.VMEM((ep, ow.shape[1], ow.shape[0]), BF),
+            pltpu.VMEM((seqs, width), BF),
+            pltpu.VMEM((nx, seqs, width), BF),
+            pltpu.VMEM((khs, dk, seqs), F32),
+            pltpu.VMEM((khs, dk, seqs), F32),
+            pltpu.VMEM((heads, seqs, dv), F32),
+            pltpu.VMEM((seqs, 128), F32),
+            pltpu.VMEM((heads, seqs, dv), F32),
+            pltpu.VMEM((heads, seqs, dv), F32),
+            dma((5,)),
+            dma((NY,)), dma((NY,)), dma((NY,)), dma((NY,)),
+            dma((NZ,)), dma((NZ,)), dma((NZ,)), dma((NZ,)),
+            dma((NZ,)), dma((NZ,)),
+            dma((NY, NZ)), dma((NY, NZ)), dma((NY, NZ)), dma((NY, NZ)),
+            dma((nx,)), dma((nx,)),
+            dma,
+        ],
+        compiler_params=pltpu.CompilerParams(
+            collective_id=1, has_side_effects=True, vmem_limit_bytes=40 * 1024 * 1024
+        ),
+        name="attention",
+    )(
+        tokens, norm_gain.reshape(1, -1), wq, wk, wv, wg, bw, dw, rate.reshape(1, -1), bias.reshape(1, -1),
+        head_gain.reshape(1, -1), rec, ow, ffn_gain.reshape(1, -1),
+    )
 
 
 def side_by_side(arrays, axis, dim, along):
@@ -56,10 +374,6 @@
         * lax.rsqrt(jnp.mean(values * values, axis=-1, keepdims=True) + EPS)
         * gain.astype(jnp.float32)
     )
-
-
-def unit_rows(values):
-    return values * lax.rsqrt(jnp.sum(values * values, axis=-1, keepdims=True) + EPS)
 
 
 def per_device(
@@ -90,65 +404,10 @@
     ep_count = lax.axis_size("ep")
     tp_count = lax.axis_size("tp")
     seq_local, width = tokens.shape
-    heads_local, key_dim, value_dim = (recurrent.shape[1], recurrent.shape[2], recurrent.shape[3])
-    normed = rms_scale(tokens, norm_gain).astype(jnp.bfloat16)
-    query_cols = query_weight.shape[1]
-    pieces = side_by_side((query_weight, key_weight, value_weight, outgate_weight), "ep", 0, 1)
-    token_block = normed
-    query_sum, key_sum, value_sum, gate_sum = tuple(
-        (
-            jnp.dot(token_block, weight_piece, preferred_element_type=jnp.float32)
-            for weight_piece in pieces
-        )
-    )
-    query_proj = query_sum.astype(jnp.bfloat16)
-    key_proj = key_sum.astype(jnp.bfloat16)
-    value_proj = value_sum.astype(jnp.bfloat16)
-    gate_proj = gate_sum.astype(jnp.bfloat16)
-    key_local = query_cols // key_dim
-    repeat_count = heads_local // key_local
-    queries = unit_rows(
-        jax.nn.silu(query_proj.astype(jnp.float32)).reshape(seq_local, key_local, key_dim)
-    )
-    queries = jnp.repeat(queries, repeat_count, axis=1) * key_dim ** (-0.5)
-    key_rows = unit_rows(
-        jax.nn.silu(key_proj.astype(jnp.float32)).reshape(seq_local, key_local, key_dim)
-    )
-    key_rows = jnp.repeat(key_rows, repeat_count, axis=1)
-    value_rows = jax.nn.silu(value_proj.astype(jnp.float32)).reshape(
-        seq_local, heads_local, value_dim
-    )
-    head_start = lax.axis_index("tp") * heads_local
-    beta_logit = jnp.dot(
-        normed,
-        lax.dynamic_slice_in_dim(beta_weight, head_start, heads_local, 1),
-        preferred_element_type=jnp.float32,
-    )
-    decay_logit = jnp.dot(
-        normed,
-        lax.dynamic_slice_in_dim(decay_weight, head_start, heads_local, 1),
-        preferred_element_type=jnp.float32,
-    )
-    strength = jax.nn.sigmoid(beta_logit)
-    retain = jnp.exp(-decay_rate[None, :] * jax.nn.softplus(decay_logit + decay_bias[None, :]))
-    decayed = recurrent * retain[:, :, None, None]
-    predicted = jnp.einsum("shde,shd->she", decayed, key_rows)
-    correction = strength[:, :, None] * (value_rows - predicted)
-    new_state = decayed + key_rows[:, :, :, None] * correction[:, :, None, :]
-    readout = jnp.einsum("shde,shd->she", new_state, queries)
-    out_gate = jax.nn.silu(gate_proj.astype(jnp.float32)).reshape(seq_local, heads_local, value_dim)
-    heads_out = (
-        (rms_scale(readout, head_gain) * out_gate)
-        .astype(jnp.bfloat16)
-        .reshape(seq_local, heads_local * value_dim)
-    )
-    partial_mix = jnp.dot(
-        heads_out, collect(output_weight, "ep", 1), preferred_element_type=jnp.float32
-    )
-    partial_mix = partial_mix.astype(jnp.bfloat16).astype(jnp.float32)
-    mixed = over_copies(partial_mix.astype(jnp.bfloat16), "tp").astype(jnp.float32)
-    residual = (tokens.astype(jnp.float32) + mixed).astype(jnp.bfloat16)
-    ffn_in = rms_scale(residual, ffn_gain).astype(jnp.bfloat16)
+    residual, ffn_in, new_state = attention(
+        tokens, norm_gain, query_weight, key_weight, value_weight, outgate_weight, beta_weight,
+        decay_weight, decay_rate, decay_bias, head_gain, recurrent, output_weight, ffn_gain,
+    )
     pieces = side_by_side((shared_gate, shared_up), "ep", 0, 1)
     token_block = ffn_in
     shared_g = jnp.dot(token_block, pieces[0], preferred_element_type=jnp.float32)

time: 268 us -> 192 us (0.72)
  waiting for transfers between devices: 163 us -> 64.2 us
  Pallas kernels: 0 us -> 44 us
  starting transfers between devices: 48.1 us -> 25.9 us
  matrix products: 19 us -> 4.3 us
  local copies, waits for them, and re-layouts: 10.9 us -> 25.2 us
  blocking collectives: 6.84 us -> 11 us
  other arithmetic: 4.85 us -> 1.61 us
    all_gather x2 -> x1, waiting for transfers between devices: 109 us -> 20.3 us  [side_by_side(): whole, at, outs = (lax.all_gather(both, axis, axis=dim, tiled=True), 0, [])]
    pallas_call x0 -> x1, Pallas kernels: none -> 44 us  [attention(): pl.pallas_call(attn_kernel, out_shape=(jax.ShapeDtypeStruct((seqs, width)...]
    unnamed x34 -> x42, local copies, waits for them, and re-layouts: 2.14 us -> 18.5 us
    dot_general x9 -> x0, matrix products: 13.5 us -> none  [the longest x4 7.1 us: per_device(): jnp.dot(token_block, weight_piece, preferred_element_type=jnp.float32)]
    all_to_all x4 -> x3, starting transfers between devices: 26.7 us -> 14.1 us  [copy_for_each(): return lax.all_to_all(copies, axis, split_axis=0, concat_axis=0, tiled=True)]
    all_to_all x1, waiting for transfers between devices: 10.8 us -> 0.01 us  [per_device(): lax.all_to_all(part_cols.reshape(received.shape[0], received.shape[1], sh...]
    all_to_all x1, blocking collectives: 6.84 us -> 11 us  [summed_on_arrival(): lax.all_to_all(pieces, axis, split_axis=0, concat_axis=0, tiled=True)]
    all_to_all x1, starting transfers between devices: 9.74 us -> 6.18 us  [per_device(): lax.all_to_all(outgoing, 'ep', split_axis=0, concat_axis=0, tiled=True)]
  transfers between devices with their start and end apart: 9 -> 6, of which waited for: 7 -> 5; matrix products, arithmetic and copies ran while one was open for 10% -> 3% of each run, Pallas kernels for 0% -> 0%
where the time goes in v1:
time: 192 us; the launch traced here: 190 us
  waiting for transfers between devices  64.2 us (33%)
  Pallas kernels  44 us (23%)
  starting transfers between devices  25.9 us (13%)
  local copies, waits for them, and re-layouts  25.2 us (13%)
  between operations  14.3 us (7%)
  blocking collectives  11 us (6%)
  matrix products  4.3 us (2%)
    pallas_call x1, Pallas kernels, attention(): pl.pallas_call(attn_kernel, out_shape=(jax.ShapeDtypeStruct((seqs, width)...  44 us
    all_to_all x3, waiting for transfers between devices, copy_for_each(): return lax.all_to_all(copies, axis, split_axis=0, concat_axis=0, tiled=True)  26.8 us
    all_gather x1, waiting for transfers between devices, side_by_side(): whole, at, outs = (lax.all_gather(both, axis, axis=dim, tiled=True), 0, [])  20.3 us
    unnamed x42, local copies, waits for them, and re-layouts  18.5 us
    all_to_all x1, waiting for transfers between devices, per_device(): lax.all_to_all(outgoing, 'ep', split_axis=0, concat_axis=0, tiled=True)  16.9 us
    all_to_all x3, starting transfers between devices, copy_for_each(): return lax.all_to_all(copies, axis, split_axis=0, concat_axis=0, tiled=True)  14.1 us
    all_to_all x1, blocking collectives, summed_on_arrival(): lax.all_to_all(pieces, axis, split_axis=0, concat_axis=0, tiled=True)  11 us
    all_to_all x1, starting transfers between devices, per_device(): lax.all_to_all(outgoing, 'ep', split_axis=0, concat_axis=0, tiled=True)  6.18 us
  transfers between devices with their start and end apart: 6, of which 5 were waited for; matrix products, arithmetic and copies ran while one was open for 3% of the time, Pallas kernels for 0%

profile of v1, /device:TPU:1, one launch (start us, length us, event | category | flops | bytes accessed | tf_op | source)
XLA Modules:
  0.0 190.5 jit_solution(3272634088657437864)
XLA Ops:
  8.6 0.8 copy.65
  10.6 0.9 copy.64.ow
  11.5 1.1 copy.62.bw
  12.6 1.1 copy.63.dw
  13.8 2.2 %copy-done.1 = f32[16,4,128,128]{3,2,1,0:T(8,128)S(1)} copy-done((f32[16,4,128,128]{3,2,1,0:T(8,128)S(1)}, f32[16,4,128,128]{3,2,1,0:T(8,128)}, u32[]{:S(2)}) %copy-start.1) | copy-done | bytes 4194328
  15.9 0.8 copy-done.3
  21.7 44.0 %attention.1 = (bf16[16,2048]{1,0:T(8,128)(2,1)S(1)}, bf16[16,2048]{1,0:T(8,128)(2,1)S(1)}, f32[16,4,128,128]{3,2,1,0:T(8,128)S(1)}) custom-call(bf16[16,2048]{1,0:T(8,128)(2,1)S(1)} %copy-done.3, bf16[1,2048]{1,0:T(2,128)(2,1)S(1)} %reshape.88.norm_gain, bf16[32,256]{1,0:T(8,128)(2,1)S(1)} %copy-done.6, bf16[32,256]{1,0:T(8,128)(2,1)S(1)} %copy-done.7, ...), custom_call_target="tpu_custom_call" | custom-call | tf_op jit(solution)/shard_map/attention/pallas_call | solution.py:285
  65.7 1.9 %copy-done.2 = f32[16,4,128,128]{3,2,1,0:T(8,128)} copy-done((f32[16,4,128,128]{3,2,1,0:T(8,128)}, f32[16,4,128,128]{3,2,1,0:T(8,128)S(1)}, u32[]{:S(2)}) %copy-start.2) | copy-done | bytes 4194328
  68.0 1.1 reshape.93
  69.1 6.2 %all-to-all-start = ((bf16[64,2,2048]{2,1,0:T(2,128)(2,1)}), bf16[64,2,2048]{2,1,0:T(2,128)(2,1)S(1)}, u32[]{:S(2)}, u32[]{:S(2)}) async-start(bf16[64,2,2048]{2,1,0:T(2,128)(2,1)} %reshape.93), calls=%async_computation | async-start | bytes 1048576 | tf_op jit(solution)/shard_map/all_to_all | solution.py:443
  76.1 16.9 %all-to-all-done = bf16[64,2,2048]{2,1,0:T(2,128)(2,1)S(1)} async-done(((bf16[64,2,2048]{2,1,0:T(2,128)(2,1)}), bf16[64,2,2048]{2,1,0:T(2,128)(2,1)S(1)}, u32[]{:S(2)}, u32[]{:S(2)}) %all-to-all-start) | async-done | bytes 524320 | tf_op jit(solution)/shard_map/all_to_all | solution.py:443
  94.1 11.0 %all_to_all.30 = bf16[4,128,512]{2,1,0:T(8,128)(2,1)S(1)} all-to-all(bf16[4,128,512]{2,1,0:T(8,128)(2,1)S(1)} %bitcast.53), channel_id=1, replica_groups=mesh['ep'=64,'tp'=4] {'tp'}, dimensions={0} | all-to-all | bytes 1048576 | tf_op jit(solution)/shard_map/all_to_all | solution.py:366
  105.1 0.9 broadcast_in_dim.6
  106.0 6.8 %all-to-all-start.3 = ((bf16[64,128,32]{1,2,0:T(8,128)(2,1)}), bf16[64,128,32]{1,2,0:T(8,128)(2,1)S(1)}, u32[]{:S(2)}, u32[]{:S(2)}) async-start(bf16[64,128,32]{1,2,0:T(8,128)(2,1)} %broadcast_in_dim.6), calls=%async_computation.3 | async-start | bytes 1048576 | tf_op jit(solution)/shard_map/all_to_all | solution.py:339
  113.8 16.8 %all-to-all-done.3 = bf16[64,128,32]{1,2,0:T(8,128)(2,1)S(1)} async-done(((bf16[64,128,32]{1,2,0:T(8,128)(2,1)}), bf16[64,128,32]{1,2,0:T(8,128)(2,1)S(1)}, u32[]{:S(2)}, u32[]{:S(2)}) %all-to-all-start.3) | async-done | bytes 524320 | tf_op jit(solution)/shard_map/all_to_all | solution.py:339
  130.6 5.6 %all-to-all-start.2 = ((bf16[64,2,512]{2,1,0:T(2,128)(2,1)}), bf16[64,2,512]{2,1,0:T(2,128)(2,1)S(1)}, u32[]{:S(2)}, u32[]{:S(2)}) async-start(bf16[64,2,512]{2,1,0:T(2,128)(2,1)} %reshape.96), calls=%async_computation.2 | async-start | bytes 262144 | tf_op jit(solution)/shard_map/all_to_all | solution.py:454
  136.2 20.3 %all-gather.2.cloned.1.call-done = bf16[2048,256]{1,0:T(8,128)(2,1)} async-done(((bf16[32,256]{1,0:T(8,128)(2,1)}), bf16[2048,256]{1,0:T(8,128)(2,1)}) %all-gather.2.cloned.1.call-update) | async-done | bytes 1048592 | tf_op jit(solution)/shard_map/all_gather | solution.py:330
  156.5 1.2 fusion.10
  157.7 1.4 convolution_convert_fusion.2
  159.9 4.0 %all-to-all-start.4 = ((bf16[4,16,2048]{2,1,0:T(8,128)(2,1)}), bf16[4,16,2048]{2,1,0:T(8,128)(2,1)S(1)}, u32[]{:S(2)}, u32[]{:S(2)}) async-start(bf16[4,16,2048]{2,1,0:T(8,128)(2,1)} %broadcast_in_dim.7), calls=%async_computation.4 | async-start | bytes 524288 | tf_op jit(solution)/shard_map/all_to_all | solution.py:339
  164.2 5.6 %all-to-all-done.4 = bf16[4,16,2048]{2,1,0:T(8,128)(2,1)S(1)} async-done(((bf16[4,16,2048]{2,1,0:T(8,128)(2,1)}), bf16[4,16,2048]{2,1,0:T(8,128)(2,1)S(1)}, u32[]{:S(2)}, u32[]{:S(2)}) %all-to-all-start.4) | async-done | bytes 262176 | tf_op jit(solution)/shard_map/all_to_all | solution.py:339
  170.6 3.3 %all-to-all-start.5 = ((bf16[4,16,512]{2,1,0:T(8,128)(2,1)}), bf16[4,16,512]{2,1,0:T(8,128)(2,1)S(1)}, u32[]{:S(2)}, u32[]{:S(2)}) async-start(bf16[4,16,512]{2,1,0:T(8,128)(2,1)} %broadcast_in_dim.8), calls=%async_computation.5 | async-start | bytes 131072 | tf_op jit(solution)/shard_map/all_to_all | solution.py:339
  173.9 4.4 %all-to-all-done.5 = bf16[4,16,512]{2,1,0:T(8,128)(2,1)S(1)} async-done(((bf16[4,16,512]{2,1,0:T(8,128)(2,1)}), bf16[4,16,512]{2,1,0:T(8,128)(2,1)S(1)}, u32[]{:S(2)}, u32[]{:S(2)}) %all-to-all-start.5) | async-done | bytes 65568 | tf_op jit(solution)/shard_map/all_to_all | solution.py:339
  178.9 4.7 %copy.74 = f32[16,4,128,128]{3,2,1,0:T(8,128)} copy(f32[16,4,128,128]{3,2,1,0:T(8,128)} %copy-done.2) | data formatting | bytes 8388608
  (64 shorter events, 13.1 us)
Async XLA Ops:
  7.2 86.3 %copy-start = (bf16[1,128,2048]{2,1,0:T(8,128)(2,1)S(1)}, bf16[1,128,2048]{2,1,0:T(8,128)(2,1)}, u32[]{:S(2)}) copy-start(bf16[1,128,2048]{2,1,0:T(8,128)(2,1)} %param.41) | copy-start | bytes 1572868
  12.6 62.8 %copy-start.15 = (bf16[32,128]{1,0:T(8,128)(2,1)S(1)}, bf16[32,128]{1,0:T(8,128)(2,1)}, u32[]{:S(2)}) copy-start(bf16[32,128]{1,0:T(8,128)(2,1)} %param.43) | copy-start | bytes 24580
  12.6 62.8 %copy-start.16 = (bf16[32,128]{1,0:T(8,128)(2,1)S(1)}, bf16[32,128]{1,0:T(8,128)(2,1)}, u32[]{:S(2)}) copy-start(bf16[32,128]{1,0:T(8,128)(2,1)} %param.42) | copy-start | bytes 24580
  13.7 2.2 %copy-start.1 = (f32[16,4,128,128]{3,2,1,0:T(8,128)S(1)}, f32[16,4,128,128]{3,2,1,0:T(8,128)}, u32[]{:S(2)}) copy-start(f32[16,4,128,128]{3,2,1,0:T(8,128)} %rec.1) | copy-start | bytes 12582916
  15.9 0.8 copy-start.3
  16.8 0.8 copy-start.4
  17.5 0.8 copy-start.5
  18.3 0.7 copy-start.6
  19.0 0.7 copy-start.7
  19.7 0.7 copy-start.8
  20.4 0.7 copy-start.9
  21.0 0.7 copy-start.10
  21.7 71.5 %copy-start.11 = (bf16[1,2048,128]{2,1,0:T(8,128)(2,1)S(1)}, bf16[1,2048,128]{2,1,0:T(8,128)(2,1)}, u32[]{:S(2)}) copy-start(bf16[1,2048,128]{2,1,0:T(8,128)(2,1)} %param.39) | copy-start | bytes 1572868
  21.7 71.8 %copy-start.12 = (bf16[1,2048,128]{2,1,0:T(8,128)(2,1)S(1)}, bf16[1,2048,128]{2,1,0:T(8,128)(2,1)}, u32[]{:S(2)}) copy-start(bf16[1,2048,128]{2,1,0:T(8,128)(2,1)} %param.40) | copy-start | bytes 1572868
  65.7 1.9 %copy-start.2 = (f32[16,4,128,128]{3,2,1,0:T(8,128)}, f32[16,4,128,128]{3,2,1,0:T(8,128)S(1)}, u32[]{:S(2)}) copy-start(f32[16,4,128,128]{3,2,1,0:T(8,128)S(1)} %get-tuple-element.11) | copy-start | bytes 12582916
  68.0 37.1 %copy-start.13 = (bf16[128,32]{0,1:T(8,128)(2,1)S(1)}, bf16[128,32]{0,1:T(8,128)(2,1)}, u32[]{:S(2)}) copy-start(bf16[128,32]{0,1:T(8,128)(2,1)} %param.44) | copy-start | bytes 24580
  69.1 23.9 %all-to-all-start = ((bf16[64,2,2048]{2,1,0:T(2,128)(2,1)}), bf16[64,2,2048]{2,1,0:T(2,128)(2,1)S(1)}, u32[]{:S(2)}, u32[]{:S(2)}) async-start(bf16[64,2,2048]{2,1,0:T(2,128)(2,1)} %reshape.93), calls=%async_computation | async-start | bytes 1048576 | tf_op jit(solution)/shard_map/all_to_all | solution.py:443
  75.3 37.5 %copy-start.17 = (bf16[2048]{0:T(1024)(128)(2,1)S(1)}, bf16[2048]{0:T(1024)(128)(2,1)}, u32[]{:S(2)}) copy-start(bf16[2048]{0:T(1024)(128)(2,1)} %param.45) | copy-start | bytes 12292
  75.3 37.5 %copy-start.14 = (f32[16,4]{0,1:T(4,128)S(1)}, f32[16,4]{0,1:T(4,128)}, u32[]{:S(2)}) copy-start(f32[16,4]{0,1:T(4,128)} %param.38) | copy-start | bytes 772
  75.3 81.2 %all-gather.2.cloned.1.call-start = ((), (), s32[]{:S(2)}) async-start(), calls=%async_computation.6 | async-start | bytes 1064960 | tf_op jit(solution)/shard_map/all_gather | solution.py:330
  106.0 24.6 %all-to-all-start.3 = ((bf16[64,128,32]{1,2,0:T(8,128)(2,1)}), bf16[64,128,32]{1,2,0:T(8,128)(2,1)S(1)}, u32[]{:S(2)}, u32[]{:S(2)}) async-start(bf16[64,128,32]{1,2,0:T(8,128)(2,1)} %broadcast_in_dim.6), calls=%async_computation.3 | async-start | bytes 1048576 | tf_op jit(solution)/shard_map/all_to_all | solution.py:339
  130.6 28.6 %all-to-all-start.2 = ((bf16[64,2,512]{2,1,0:T(2,128)(2,1)}), bf16[64,2,512]{2,1,0:T(2,128)(2,1)S(1)}, u32[]{:S(2)}, u32[]{:S(2)}) async-start(bf16[64,2,512]{2,1,0:T(2,128)(2,1)} %reshape.96), calls=%async_computation.2 | async-start | bytes 262144 | tf_op jit(solution)/shard_map/all_to_all | solution.py:454
  159.9 9.9 %all-to-all-start.4 = ((bf16[4,16,2048]{2,1,0:T(8,128)(2,1)}), bf16[4,16,2048]{2,1,0:T(8,128)(2,1)S(1)}, u32[]{:S(2)}, u32[]{:S(2)}) async-start(bf16[4,16,2048]{2,1,0:T(8,128)(2,1)} %broadcast_in_dim.7), calls=%async_computation.4 | async-start | bytes 524288 | tf_op jit(solution)/shard_map/all_to_all | solution.py:339
  170.6 7.7 %all-to-all-start.5 = ((bf16[4,16,512]{2,1,0:T(8,128)(2,1)}), bf16[4,16,512]{2,1,0:T(8,128)(2,1)S(1)}, u32[]{:S(2)}, u32[]{:S(2)}) async-start(bf16[4,16,512]{2,1,0:T(8,128)(2,1)} %broadcast_in_dim.8), calls=%async_computation.5 | async-start | bytes 131072 | tf_op jit(solution)/shard_map/all_to_all | solution.py:339
Sparse Core Ops, SparseCore 0:
  79.5 76.9 all-gather.1

commit v2 on v1

v2 whole, which is shorter than its diff:
```python
import jax
import jax.numpy as jnp
from jax import lax
from jax.experimental import pallas as pl
from jax.experimental.pallas import tpu as pltpu
from jax.sharding import PartitionSpec as P

EPS = 1e-06
ROUTED_SCALE = 2.5
NZ, NY, NC = 8, 4, 2
YC = NY * NC
EP = NZ * YC
SLOTS = 2
LANES = 128
MESH = pl.DeviceIdType.MESH
BF = jnp.bfloat16
F32 = jnp.float32
I32 = jnp.int32


def silu(v):
    return v / (1.0 + jnp.exp(-v))


def sigmoid(v):
    return 1.0 / (1.0 + jnp.exp(-v))


def rms(values, gain):
    return values * lax.rsqrt(jnp.mean(values * values, axis=-1, keepdims=True) + EPS) * gain


def unit(v):
    return v * lax.rsqrt(jnp.sum(v * v, axis=-1, keepdims=True) + EPS)


def iota(shape, dim):
    return lax.broadcasted_iota(I32, shape, dim)


def nt_dot(a, b):
    return lax.dot_general(a, b, (((1,), (1,)), ((), ())), preferred_element_type=F32)


def layer_kernel(
    tokens_h, norm_gain_h, wq, wk, wv, wg, bw_h, dw_h, rate_h, bias_h, head_gain_h, rec, ow_h, ffn_gain_h,
    routes_h, rweight_h, eg_h, eu_h, ed_h, sg_h, su_h, sd_h, branch_h,
    out_ref, keys_out, corr_out, retain_out,
    tokens, norm_gain, bw, dw, rate, bias, head_gain, ffn_gain, routes, rweight, branch_gate,
    state, wbuf, tok_src, tokbuf, psend, prec, obuf, sbuf, mix_send, mix_rec,
    kt, qt, vals, rs_ref, ro,
    egu, dsrc, dbuf, chunks, res_chunks, dsend, xrows, rowsf, act_all, outf, rsend, rrecv, sh_send, sh_rec, fin,
    load_sem, w_s, w_r, wf_s, wf_r, t_s, t_r, p_s, p_r, o1_s, o1_r, o2_s, o2_r, o3_s, o3_r,
    s1_s, s1_r, s2_s, s2_r, s3_s, s3_r, m_s, m_r, ed_s, ed_r, d_s, d_r, x_s, x_r, a_s, a_r, r_s, r_r,
    h_s, h_r, f_s, f_r,
):
    e = lax.axis_index("ep")
    x = lax.axis_index("tp")
    nx = lax.axis_size("tp")
    z, yc = e // YC, e % YC
    y, c = yc // NC, yc % NC
    partner = e + 1 - 2 * c
    zdev = lambda d: ((z + d) % NZ) * YC + yc
    ydev = lambda d: z * YC + ((y + d) % NY) * NC + c
    xdev = lambda d: (x + d) % nx
    seqs, width = tokens.shape
    heads, dk, dv = rec.shape[1:]
    pending = []

    def rcopy(src, dst, ss, rs, ep, tp):
        cp = pltpu.make_async_remote_copy(
            src_ref=src, dst_ref=dst, send_sem=ss, recv_sem=rs, device_id=(ep, tp), device_id_type=MESH
        )
        cp.start()
        pending.append(cp)
        return cp

    barrier = pltpu.get_barrier_semaphore()

    def greet(d, carry):
        pl.semaphore_signal(barrier, inc=1, device_id=((e + d) % EP, x), device_id_type=MESH)
        return carry

    lax.fori_loop(1, EP, greet, 0)
    for d in range(1, nx):
        pl.semaphore_signal(barrier, inc=1, device_id=(e, xdev(d)), device_id_type=MESH)

    count = [0]

    def load(src, dst):
        cp = pltpu.make_async_copy(src, dst, load_sem.at[count[0]])
        count[0] += 1
        cp.start()
        return cp

    first = [load(tokens_h, tokens), load(norm_gain_h, norm_gain)]
    wloads = []
    at = 0
    for w in (wq, wk, wv, wg):
        n = w.shape[1]
        wloads.append(load(w, wbuf.at[yc, :, at : at + n]))
        at += n
    oload = load(ow_h, obuf.at[e])
    qc = width // nx
    edloads = [load(ed_h.at[0, :, q * qc : (q + 1) * qc], dsrc.at[q]) for q in range(nx)]
    small = [
        load(a, b)
        for a, b in (
            (bw_h, bw), (dw_h, dw), (rate_h, rate), (bias_h, bias), (head_gain_h, head_gain),
            (ffn_gain_h, ffn_gain), (routes_h, routes), (rweight_h, rweight), (branch_h, branch_gate),
        )
    ]
    hs = sg_h.shape[1]
    sloads = [
        load(a, sbuf.at[e, :, i * hs : (i + 1) * hs]) for i, a in enumerate((sg_h, su_h, sd_h))
    ]
    load_state = load(rec, state)
    he = eg_h.shape[2]
    eloads = [load(eg_h.at[0], egu.at[:, 0:he]), load(eu_h.at[0], egu.at[:, he : 2 * he])]

    for l in first:
        l.wait()
    normed = rms(tokens[...].astype(F32), norm_gain[...].reshape(1, width).astype(F32)).astype(BF)
    kz = tokbuf.shape[2]
    for i in range(NZ):
        tok_src[i] = normed[:, i * kz : (i + 1) * kz]
    for l in wloads + [oload] + edloads:
        l.wait()
    pl.semaphore_wait(barrier, (EP - 1) + (nx - 1))

    toks = [
        rcopy(tok_src.at[(z + d) % NZ], tokbuf.at[d], t_s.at[d], t_r.at[d], zdev(d), x)
        for d in range(1, NZ)
    ]
    ws = [rcopy(wbuf.at[yc], wbuf.at[yc], w_s.at[d], w_r.at[d], ydev(d), x) for d in range(1, NY)]
    fwd = [rcopy(wbuf.at[yc], wbuf.at[yc], wf_s.at[0], wf_r.at[0], partner, x)]

    def spread_z(buf, ss, rs):
        return [rcopy(buf.at[e], buf.at[e], ss.at[d], rs.at[d], zdev(d), x) for d in range(1, NZ)]

    def spread_y(buf, before, ss, rs, fs, fr):
        over_y, over_c = [], []
        for d in range(NZ):
            if d:
                before[d - 1].wait_recv()
            j = ((z + NZ - d) % NZ) * YC + yc
            for dy in range(1, NY):
                over_y.append((dy, d, rcopy(buf.at[j], buf.at[j], ss.at[dy, d], rs.at[dy, d], ydev(dy), x)))
            over_c.append(rcopy(buf.at[j], buf.at[j], fs.at[0, d], fr.at[0, d], partner, x))
        return over_y, over_c

    def spread_c(buf, over_y, fs, fr):
        over_c = []
        for dy, d, cp in over_y:
            cp.wait_recv()
            j = ((z + NZ - d) % NZ) * YC + ((y + NY - dy) % NY) * NC + c
            over_c.append(rcopy(buf.at[j], buf.at[j], fs.at[dy, d], fr.at[dy, d], partner, x))
        return over_c

    o1 = spread_z(obuf, o1_s, o1_r)
    downs = [
        rcopy(dsrc.at[xdev(d)], dbuf.at[d], ed_s.at[d], ed_r.at[d], e, xdev(d)) for d in range(1, nx)
    ]
    tokbuf[0] = tok_src[z]

    for l in small:
        l.wait()
    bl = nt_dot(normed, bw[...])
    dl = nt_dot(normed, dw[...])
    lanes = iota(bl.shape, 1)
    retain, strength = [], []
    for h in range(heads):
        mine = lanes == x * heads + h
        b = jnp.sum(jnp.where(mine, bl, 0.0), axis=1, keepdims=True)
        g = jnp.sum(jnp.where(mine, dl, 0.0), axis=1, keepdims=True) + bias[h]
        soft = jnp.maximum(g, 0.0) + jnp.log1p(jnp.exp(-jnp.abs(g)))
        strength.append(sigmoid(b))
        retain.append(jnp.exp(-rate[h] * soft))
    lane = iota(rs_ref.shape, 1)
    packed = jnp.zeros(rs_ref.shape, F32)
    for h in range(heads):
        packed = jnp.where(lane == h, retain[h], packed)
        packed = jnp.where(lane == heads + h, strength[h], packed)

    for d in range(1, NY):
        ws[d - 1].wait_recv()
        j = ((y + NY - d) % NY) * NC + c
        fwd.append(rcopy(wbuf.at[j], wbuf.at[j], wf_s.at[d], wf_r.at[d], partner, x))
    for cp in toks + fwd:
        cp.wait_recv()
    cols = wbuf.shape[2]
    partial = jnp.dot(
        tokbuf[...].reshape(NZ * seqs, kz), wbuf[...].reshape(kz, cols), preferred_element_type=F32
    ).astype(BF)
    psend[...] = partial.reshape(NZ, seqs, cols)
    sums = [
        rcopy(psend.at[d], prec.at[d], p_s.at[d], p_r.at[d], zdev(NZ - d), x)
        for d in (4, 3, 5, 2, 6, 1, 7)
    ]
    o2, o3 = spread_y(obuf, o1, o2_s, o2_r, o3_s, o3_r)
    for l in sloads:
        l.wait()
    s1 = spread_z(sbuf, s1_s, s1_r)

    topk = routes.shape[0]
    rrow = [routes[k : k + 1, :] for k in range(topk)]
    square = (seqs, seqs)
    diag = iota(square, 0) == iota(square, 1)
    upright = lambda row, zero: jnp.sum(
        jnp.where(diag, jnp.broadcast_to(row, square), zero), axis=1, keepdims=True
    )
    rcol = [upright(r.astype(F32), 0.0) for r in rrow]
    rrow = [r.astype(F32) for r in rrow]
    before_c = iota(square, 1) < iota(square, 0)
    before_r = iota(square, 0) < iota(square, 1)
    tcol, trow = [], []
    for k in range(topk):
        hits_c = jnp.zeros(square, F32)
        hits_r = jnp.zeros(square, F32)
        for k2 in range(topk):
            hits_c += jnp.where(before_c & (rcol[k] == rrow[k2]), 1.0, 0.0)
            hits_r += jnp.where(before_r & (rrow[k] == rcol[k2]), 1.0, 0.0)
        tcol.append(rcol[k] * SLOTS + jnp.sum(hits_c, axis=1, keepdims=True))
        trow.append(rrow[k] * SLOTS + jnp.sum(hits_r, axis=0, keepdims=True))
    ch = qc // LANES
    wide = ch * seqs
    spreadm = (iota((seqs, wide), 1) % seqs == iota((seqs, wide), 0)).astype(BF)
    rows_all = EP * SLOTS * ch
    rid = iota((rows_all, wide), 0)
    okc = rid % ch == iota((rows_all, wide), 1) // seqs
    ridf = (rid // ch).astype(F32)
    place = jnp.zeros((rows_all, wide), F32)
    for k in range(topk):
        tw = jnp.dot(
            jnp.broadcast_to(trow[k], (8, seqs)).astype(BF), spreadm, preferred_element_type=F32
        )[0:1, :]
        place = jnp.where(okc & (ridf == tw), 1.0, place)
    place = place.astype(BF)
    rw = [rweight[k : k + 1, :] for k in range(topk)]
    rsum = rw[0]
    for k in range(1, topk):
        rsum = rsum + rw[k]
    scol = [upright(rw[k] / rsum * ROUTED_SCALE, 0.0) for k in range(topk)]
    pick_col = jnp.concatenate([tcol[k] * ch + cc for k in range(topk) for cc in range(ch)], axis=0)
    scale_col = jnp.concatenate([scol[k] for k in range(topk) for cc in range(ch)], axis=0)
    pick = (
        jnp.broadcast_to(pick_col, (topk * wide, rows_all))
        == iota((topk * wide, rows_all), 1).astype(F32)
    ).astype(BF)

    for cp in sums:
        cp.wait_recv()
    total = psend[0].astype(F32)
    for d in range(1, NZ):
        total = total + prec[d].astype(F32)
    proj = total.astype(BF).astype(F32)
    o3 += spread_c(obuf, o2, o3_s, o3_r)

    khs = wq.shape[1] // dk
    per = heads // khs
    kq = []
    for i in range(khs):
        q = unit(silu(proj[:, i * dk : (i + 1) * dk])) * dk ** (-0.5)
        k = unit(silu(proj[:, (khs + i) * dk : (khs + i + 1) * dk]))
        keys_out[:, i * dk : (i + 1) * dk] = k
        kt[i] = k.T
        qt[i] = q.T
        kq.append(jnp.sum(k * q, axis=1, keepdims=True))
    for i in range(khs):
        packed = jnp.where(lane == 2 * heads + i, kq[i], packed)
    rs_ref[...] = packed
    retain_out[...] = packed
    vbase = 2 * khs * dk
    for h in range(heads):
        vals[h] = silu(proj[:, vbase + h * dv : vbase + (h + 1) * dv])
    gate = proj[:, vbase + heads * dv :]
    load_state.wait()

    def column(ref, i, s):
        t = ref[i]
        return jnp.sum(jnp.where(iota(t.shape, 1) == s, t, 0.0), axis=1, keepdims=True)

    def read_one(s, carry):
        rowrs = rs_ref[pl.ds(s, 1), :]
        for i in range(khs):
            kcol = column(kt, i, s)
            qcol = column(qt, i, s)
            dotkq = rowrs[:, 2 * heads + i : 2 * heads + i + 1]
            for h in range(i * per, (i + 1) * per):
                st = state[s, h]
                ret = rowrs[:, h : h + 1]
                pred = jnp.sum(st * kcol, axis=0, keepdims=True) * ret
                base = jnp.sum(st * qcol, axis=0, keepdims=True) * ret
                cor = rowrs[:, heads + h : heads + h + 1] * (vals[h, pl.ds(s, 1), :] - pred)
                corr_out[h, pl.ds(s, 1), :] = cor
                ro[h, pl.ds(s, 1), :] = base + dotkq * cor
        return carry

    lax.fori_loop(0, seqs, read_one, 0)

    s2, s3 = spread_y(sbuf, s1, s2_s, s2_r, s3_s, s3_r)
    hg = head_gain[...].reshape(1, dv).astype(F32)
    parts = [rms(ro[h], hg) * silu(gate[:, h * dv : (h + 1) * dv]) for h in range(heads)]
    heads_out = jnp.concatenate(parts, axis=1).astype(BF)
    for cp in o3:
        cp.wait_recv()
    mix_send[...] = nt_dot(heads_out, obuf[...].reshape(width, heads * dv)).astype(BF)
    mixes = [
        rcopy(mix_send, mix_rec.at[d], m_s.at[d], m_r.at[d], e, xdev(d)) for d in range(1, nx)
    ]
    for l in eloads:
        l.wait()
    mixed = mix_send[...].astype(F32)
    for d in range(1, nx):
        mixes[d - 1].wait_recv()
        mixed = mixed + mix_rec[d].astype(F32)
    residual = (tokens[...].astype(F32) + mixed).astype(BF)
    ffn_in = rms(residual.astype(F32), ffn_gain[...].reshape(1, width).astype(F32)).astype(BF)
    for i in range(nx * ch):
        chunks[i] = ffn_in[:, i * LANES : (i + 1) * LANES]
        res_chunks[i] = residual[:, i * LANES : (i + 1) * LANES]

    mine = chunks[pl.ds(x * ch, ch)].reshape(wide, LANES)
    msg = SLOTS * ch
    dsend[...] = (
        jnp.dot(place, mine, preferred_element_type=F32).astype(BF).reshape(EP, msg, LANES)
    )

    def exchange(src, dst, ss, rs):
        def one(i, carry):
            dz, d = i // YC, i % YC
            to = ((z + dz) % NZ) * YC + (yc + d) % YC
            cp = pltpu.make_async_remote_copy(
                src_ref=src.at[to], dst_ref=dst.at[e], send_sem=ss, recv_sem=rs.at[dz],
                device_id=(to, x), device_id_type=MESH,
            )
            cp.start()
            return carry

        lax.fori_loop(1, EP, one, 0)

    def group_wait(dst, dz, rs):
        zs = (z + NZ - dz) % NZ
        n = YC - 1 if dz == 0 else YC
        ref = dst.at[pl.ds(0, n)]
        pltpu.make_async_copy(ref, ref, rs.at[dz]).wait()
        return zs

    def sent_wait(src, ss):
        ref = src.at[pl.ds(0, EP - 1)]
        pltpu.make_async_copy(ref, ref, ss).wait()

    exchange(dsend, xrows.at[x], d_s, d_r)
    xrows[x, e] = dsend[e]

    s3 += spread_c(sbuf, s2, s3_s, s3_r)
    xs = []
    for dz in range(NZ):
        zs = group_wait(xrows.at[x], dz, d_r)
        for d in range(1, nx):
            block = xrows.at[x, pl.ds(zs * YC, YC)]
            xs.append(rcopy(block, block, x_s.at[d, dz], x_r.at[d, dz], e, xdev(d)))
    for cp in s3:
        cp.wait_recv()
    sgu = jnp.dot(ffn_in, sbuf[:, :, 0 : 2 * hs].reshape(width, 2 * hs), preferred_element_type=F32)
    sact = (silu(sgu[:, 0:hs]) * sgu[:, hs:]).astype(BF)
    spart = nt_dot(sact, sbuf[:, :, 2 * hs :].reshape(width, hs)).astype(BF)
    for i in range(nx * ch):
        sh_send[i // ch, (i % ch) * seqs : (i % ch + 1) * seqs, :] = spart[:, i * LANES : (i + 1) * LANES]
    shs = [
        rcopy(sh_send.at[xdev(d)], sh_rec.at[d], h_s.at[d], h_r.at[d], e, xdev(d)) for d in range(1, nx)
    ]
    branch = sigmoid(
        jnp.sum(
            ffn_in.astype(F32) * branch_gate[...].reshape(1, width).astype(F32), axis=1, keepdims=True
        )
    )

    for cp in xs:
        cp.wait_recv()
    gu = jnp.zeros((EP * SLOTS, 2 * he), F32)
    for q in range(nx):
        rowsf[q] = xrows[q].reshape(rows_all, LANES).astype(F32)
    for q in range(nx):
        left = jnp.concatenate(
            [rowsf[q, pl.ds(cc, EP * SLOTS, stride=ch), :] for cc in range(ch)], axis=1
        ).astype(BF)
        gu = gu + jnp.dot(left, egu[q * qc : (q + 1) * qc, :], preferred_element_type=F32)
    act_all[0] = (silu(gu[:, 0:he]) * gu[:, he:]).astype(BF)
    acts = [
        rcopy(act_all.at[0], act_all.at[d], a_s.at[d], a_r.at[d], e, xdev(d)) for d in range(1, nx)
    ]
    for cp in downs:
        cp.wait_recv()
    eout = jnp.dot(act_all[0], dsrc[x], preferred_element_type=F32)
    for d in range(1, nx):
        acts[d - 1].wait_recv()
        eout = eout + jnp.dot(act_all[d], dbuf[d], preferred_element_type=F32)
    for cc in range(ch):
        outf[pl.ds(cc, EP * SLOTS, stride=ch), :] = eout[:, cc * LANES : (cc + 1) * LANES]
    rsend[...] = outf[...].astype(BF).reshape(EP, msg, LANES)
    exchange(rsend, rrecv, r_s, r_r)
    rrecv[e] = rsend[e]

    shared = sh_send[x].astype(F32)
    for d in range(1, nx):
        shs[d - 1].wait_recv()
        shared = shared + sh_rec[d].astype(F32)
    base = res_chunks[pl.ds(x * ch, ch)].reshape(wide, LANES).astype(F32)
    base = base + jnp.concatenate([branch] * ch, axis=0) * shared
    for dz in range(NZ):
        group_wait(rrecv, dz, r_r)
    got = jnp.dot(pick, rrecv[...].reshape(rows_all, LANES), preferred_element_type=F32) * scale_col
    for k in range(topk):
        base = base + got[k * wide : (k + 1) * wide]
    fin[x] = base.astype(BF)
    fins = [rcopy(fin.at[x], fin.at[x], f_s.at[d], f_r.at[d], e, xdev(d)) for d in range(1, nx)]
    for cp in fins:
        cp.wait_recv()
    for i in range(nx * ch):
        out_ref[:, i * LANES : (i + 1) * LANES] = fin[i // ch, (i % ch) * seqs : (i % ch + 1) * seqs, :]

    for cp in pending:
        cp.wait_send()
    sent_wait(dsend, d_s)
    sent_wait(rsend, r_s)


def layer(*args):
    (tokens, norm_gain, wq, wk, wv, wg, bw, dw, rate, bias, head_gain, rec, ow, ffn_gain, routes, rweight,
     eg, eu, ed, sg, su, sd, branch_gate) = args
    nx = lax.axis_size("tp")
    seqs, width = tokens.shape
    heads, dk, dv = rec.shape[1:]
    cols = wq.shape[1] + wk.shape[1] + wv.shape[1] + wg.shape[1]
    rows = wq.shape[0]
    kz = rows * YC
    khs = wq.shape[1] // dk
    topk = routes.shape[1]
    qc = width // nx
    ch = qc // LANES
    he = eg.shape[2]
    hs = sg.shape[1]
    msg = SLOTS * ch
    wide = ch * seqs
    hbm = pl.BlockSpec(memory_space=pltpu.HBM)
    vmem = pl.BlockSpec(memory_space=pltpu.VMEM)
    dma = pltpu.SemaphoreType.DMA
    V = pltpu.VMEM
    return pl.pallas_call(
        layer_kernel,
        out_shape=(
            jax.ShapeDtypeStruct((seqs, width), BF),
            jax.ShapeDtypeStruct((seqs, khs * dk), F32),
            jax.ShapeDtypeStruct((heads, seqs, dv), F32),
            jax.ShapeDtypeStruct((seqs, LANES), F32),
        ),
        in_specs=[hbm] * 23,
        out_specs=(vmem,) * 4,
        scratch_shapes=[
            V((seqs, width), BF), V((width,), BF), V(bw.shape[::-1], BF), V(dw.shape[::-1], BF),
            pltpu.SMEM((heads,), F32), pltpu.SMEM((heads,), F32), V((dv,), BF), V((width,), BF),
            V((topk, seqs), I32), V((topk, seqs), F32), V((width,), BF),
            V(rec.shape, F32),
            V((YC, rows, cols), BF), V((NZ, seqs, kz), BF), V((NZ, seqs, kz), BF),
            V((NZ, seqs, cols), BF), V((NZ, seqs, cols), BF),
            V((EP, ow.shape[1], ow.shape[0]), BF), V((EP, sg.shape[0], 3 * hs), BF),
            V((seqs, width), BF), V((nx, seqs, width), BF),
            V((khs, dk, seqs), F32), V((khs, dk, seqs), F32), V((heads, seqs, dv), F32),
            V((seqs, LANES), F32), V((heads, seqs, dv), F32),
            V((width, 2 * he), BF), V((nx, he, qc), BF), V((nx, he, qc), BF),
            V((nx * ch, seqs, LANES), BF), V((nx * ch, seqs, LANES), BF),
            V((EP, msg, LANES), BF), V((nx, EP, msg, LANES), BF), V((nx, EP * msg, LANES), F32),
            V((nx, EP * SLOTS, he), BF), V((EP * msg, LANES), F32),
            V((EP, msg, LANES), BF), V((EP, msg, LANES), BF),
            V((nx, wide, LANES), BF), V((nx, wide, LANES), BF), V((nx, wide, LANES), BF),
            dma((32,)),
            dma((NY,)), dma((NY,)), dma((NY,)), dma((NY,)),
            dma((NZ,)), dma((NZ,)), dma((NZ,)), dma((NZ,)),
            dma((NZ,)), dma((NZ,)), dma((NY, NZ)), dma((NY, NZ)), dma((NY, NZ)), dma((NY, NZ)),
            dma((NZ,)), dma((NZ,)), dma((NY, NZ)), dma((NY, NZ)), dma((NY, NZ)), dma((NY, NZ)),
            dma((nx,)), dma((nx,)), dma((nx,)), dma((nx,)),
            dma, dma((NZ,)), dma((nx, NZ)), dma((nx, NZ)), dma((nx,)), dma((nx,)), dma, dma((NZ,)),
            dma((nx,)), dma((nx,)), dma((nx,)), dma((nx,)),
        ],
        compiler_params=pltpu.CompilerParams(
            collective_id=1, has_side_effects=True, vmem_limit_bytes=67043328
        ),
        name="layer",
    )(
        tokens, norm_gain, wq, wk, wv, wg, bw.T, dw.T, rate, bias, head_gain, rec, ow.T, ffn_gain,
        routes.T, rweight.T, eg, eu, ed, sg, su, sd.T, branch_gate,
    )


def per_device(*args):
    recurrent = args[11]
    seqs, heads, dk, _ = recurrent.shape
    layer_out, keys, corr, packed = layer(*args)
    keys = jnp.repeat(keys.reshape(seqs, -1, dk), heads * dk // keys.shape[1], axis=1)
    retain = packed[:, 0:heads]
    new_state = (
        recurrent * retain[:, :, None, None]
        + keys[:, :, :, None] * jnp.swapaxes(corr, 0, 1)[:, :, None, :]
    )
    return layer_out, new_state


def solution(mesh):
    return jax.shard_map(
        per_device,
        mesh=mesh,
        in_specs=(
            P("ep", None),
            P(),
            P("ep", "tp"),
            P("ep", "tp"),
            P("ep", "tp"),
            P("ep", "tp"),
            P(),
            P(),
            P("tp"),
            P("tp"),
            P(),
            P("ep", "tp", None, None),
            P("tp", "ep"),
            P(),
            P("ep", None),
            P("ep", None),
            P("ep", None, "tp"),
            P("ep", None, "tp"),
            P("ep", "tp", None),
            P("ep", "tp"),
            P("ep", "tp"),
            P("tp", "ep"),
            P(),
        ),
        out_specs=(P("ep", None), P("ep", "tp", None, None)),
        check_vma=False,
    )
```

time: 192 us -> 86.3 us (0.45)
  waiting for transfers between devices: 64.2 us -> 0 us
  Pallas kernels: 44 us -> 78.9 us
  starting transfers between devices: 25.9 us -> 0 us
  local copies, waits for them, and re-layouts: 25.2 us -> 2.15 us
  between operations: 14.3 us -> 0.67 us
  blocking collectives: 11 us -> 0 us
  matrix products: 4.3 us -> 0 us
  other arithmetic: 1.61 us -> 4.39 us
    all_to_all x5 -> x0, waiting for transfers between devices: 43.8 us -> none  [the longest x3 26.8 us: copy_for_each(): return lax.all_to_all(copies, axis, split_axis=0, concat_axis=0, tiled=True)]
    pallas_call x1, Pallas kernels: 44 us -> 78.9 us  [layer(): pl.pallas_call(layer_kernel, out_shape=(jax.ShapeDtypeStruct((seqs, width...]
    all_to_all x5 -> x0, starting transfers between devices: 25.8 us -> none  [the longest x3 14.1 us: copy_for_each(): return lax.all_to_all(copies, axis, split_axis=0, concat_axis=0, tiled=True)]
    all_gather x1 -> x0, waiting for transfers between devices: 20.3 us -> none  [side_by_side(): whole, at, outs = (lax.all_gather(both, axis, axis=dim, tiled=True), 0, [])]
    unnamed x42 -> x3, local copies, waits for them, and re-layouts: 18.5 us -> 0.63 us
    all_to_all x1 -> x0, blocking collectives: 11 us -> none  [summed_on_arrival(): lax.all_to_all(pieces, axis, split_axis=0, concat_axis=0, tiled=True)]
    dot_general x8 -> x0, matrix products: 4.3 us -> none  [the longest x1 1.43 us: per_device(): jnp.dot(shared_act, collect(shared_down, 'ep', 1), preferred_element_type...]
    add x1, other arithmetic: 0.7 us -> 4.39 us  [per_device(): recurrent * retain[:, :, None, None]]
  transfers between devices with their start and end apart: 6 -> 0, of which waited for: 5 -> 0; matrix products, arithmetic and copies ran while one was open for 3% -> 0% of each run, Pallas kernels for 0% -> 0%
where the time goes in v2:
time: 86.3 us; the launch traced here: 86.1 us
  Pallas kernels  78.9 us (91%)
  other arithmetic  4.39 us (5%)
  local copies, waits for them, and re-layouts  2.15 us (2%)
    pallas_call x1, Pallas kernels, layer(): pl.pallas_call(layer_kernel, out_shape=(jax.ShapeDtypeStruct((seqs, width...  78.9 us
    add x1, other arithmetic, per_device(): recurrent * retain[:, :, None, None]  4.39 us

profile of v2, /device:TPU:1, one launch (start us, length us, event | category | flops | bytes accessed | tf_op | source)
XLA Modules:
  0.0 86.1 jit_solution(5734367264955590270)
XLA Ops:
  0.6 78.9 %layer.1 = (bf16[16,2048]{1,0:T(8,128)(2,1)}, f32[16,256]{1,0:T(8,128)}, f32[4,16,128]{2,1,0:T(8,128)}, f32[16,128]{1,0:T(8,128)}) custom-call(bf16[16,2048]{1,0:T(8,128)(2,1)} %tokens_h.1, bf16[2048]{0:T(1024)(128)(2,1)} %norm_gain_h.1, bf16[32,256]{1,0:T(8,128)(2,1)} %wq.1, bf16[32,256]{1,0:T(8,128)(2,1)} %wk.1, bf16[32,512]{1,0:T(8,128)(2,1)} %wv.1, ...), custom_call_target="tpu_custom_call" | custom-call | tf_op jit(solution)/shard_map/layer/pallas_call | solution.py:450
  79.5 0.7 reshape.10
  80.3 0.8 copy.25
  81.1 0.0 copy-start
  81.1 4.4 %multiply_add_fusion = f32[16,4,128,128]{3,2,1,0:T(8,128)} fusion(f32[16,4,128,128]{3,2,1,0:T(8,128)} %rec.1, f32[16,4,128]{2,1,0:T(4,128)S(1)} %copy.25, f32[16,4,128]{2,1,0:T(4,128)S(1)} %bitcast.9, f32[16,4]{1,0:T(8,128)} %bitcast.15), kind=kLoop, calls=%fused_computation | loop fusion | flops 3145728 | bytes 8454400 | tf_op jit(solution)/shard_map/add | solution.py:503
  85.5 0.0 copy-done
  85.5 0.6 copy.27
  (1 shorter events, 0.0 us)
Async XLA Ops:
  81.1 4.4 %copy-start = (bf16[16,2048]{1,0:T(8,128)(2,1)S(1)}, bf16[16,2048]{1,0:T(8,128)(2,1)}, u32[]{:S(2)}) copy-start(bf16[16,2048]{1,0:T(8,128)(2,1)} %get-tuple-element.12) | copy-start | bytes 196612

commit v3 on v2

--- a/solution.py
+++ b/solution.py
@@ -11,6 +11,9 @@
 YC = NY * NC
 EP = NZ * YC
 SLOTS = 2
+UNROLL = 4
+STATE_COPIES = 4
+LAYER_VMEM = 40 * 1024 * 1024
 LANES = 128
 MESH = pl.DeviceIdType.MESH
 BF = jnp.bfloat16
@@ -45,24 +48,24 @@
 def layer_kernel(
     tokens_h, norm_gain_h, wq, wk, wv, wg, bw_h, dw_h, rate_h, bias_h, head_gain_h, rec, ow_h, ffn_gain_h,
     routes_h, rweight_h, eg_h, eu_h, ed_h, sg_h, su_h, sd_h, branch_h,
-    out_ref, keys_out, corr_out, retain_out,
+    out_ref, state,
     tokens, norm_gain, bw, dw, rate, bias, head_gain, ffn_gain, routes, rweight, branch_gate,
-    state, wbuf, tok_src, tokbuf, psend, prec, obuf, sbuf, mix_send, mix_rec,
-    kt, qt, vals, rs_ref, ro,
+    wbuf, tok_src, tokbuf, psend, prec, gsend, grec, obuf, sbuf, mix_send, mix_rec,
+    kt, qt, vals, rs_ref, ro, corr,
     egu, dsrc, dbuf, chunks, res_chunks, dsend, xrows, rowsf, act_all, outf, rsend, rrecv, sh_send, sh_rec, fin,
-    load_sem, w_s, w_r, wf_s, wf_r, t_s, t_r, p_s, p_r, o1_s, o1_r, o2_s, o2_r, o3_s, o3_r,
+    load_sem, w_s, w_r, wf_s, wf_r, t_s, t_r, p_s, p_r, g_s, g_r, o1_s, o1_r, o2_s, o2_r, o3_s, o3_r,
     s1_s, s1_r, s2_s, s2_r, s3_s, s3_r, m_s, m_r, ed_s, ed_r, d_s, d_r, x_s, x_r, a_s, a_r, r_s, r_r,
     h_s, h_r, f_s, f_r,
 ):
     e = lax.axis_index("ep")
     x = lax.axis_index("tp")
     nx = lax.axis_size("tp")
-    z, yc = e // YC, e % YC
-    y, c = yc // NC, yc % NC
+    z, yc = lax.div(e, YC), lax.rem(e, YC)
+    y, c = lax.div(yc, NC), lax.rem(yc, NC)
     partner = e + 1 - 2 * c
-    zdev = lambda d: ((z + d) % NZ) * YC + yc
-    ydev = lambda d: z * YC + ((y + d) % NY) * NC + c
-    xdev = lambda d: (x + d) % nx
+    zdev = lambda d: lax.rem(z + d, NZ) * YC + yc
+    ydev = lambda d: z * YC + lax.rem(y + d, NY) * NC + c
+    xdev = lambda d: lax.rem(x + d, nx)
     seqs, width = tokens.shape
     heads, dk, dv = rec.shape[1:]
     pending = []
@@ -74,16 +77,6 @@
         cp.start()
         pending.append(cp)
         return cp
-
-    barrier = pltpu.get_barrier_semaphore()
-
-    def greet(d, carry):
-        pl.semaphore_signal(barrier, inc=1, device_id=((e + d) % EP, x), device_id_type=MESH)
-        return carry
-
-    lax.fori_loop(1, EP, greet, 0)
-    for d in range(1, nx):
-        pl.semaphore_signal(barrier, inc=1, device_id=(e, xdev(d)), device_id_type=MESH)
 
     count = [0]
 
@@ -118,6 +111,16 @@
     he = eg_h.shape[2]
     eloads = [load(eg_h.at[0], egu.at[:, 0:he]), load(eu_h.at[0], egu.at[:, he : 2 * he])]
 
+    barrier = pltpu.get_barrier_semaphore()
+    zbase = [lax.rem(z + d, NZ) * YC for d in range(NZ)]
+    ypart = [lax.rem(yc + d, YC) for d in range(YC)]
+    far_first = [(dz, d) for dz in (4, 3, 5, 2, 6, 1, 7, 0) for d in range(YC) if dz or d]
+    near_first = far_first[::-1]
+    for dz, d in far_first:
+        pl.semaphore_signal(barrier, inc=1, device_id=(zbase[dz] + ypart[d], x), device_id_type=MESH)
+    for d in range(1, nx):
+        pl.semaphore_signal(barrier, inc=1, device_id=(e, xdev(d)), device_id_type=MESH)
+
     for l in first:
         l.wait()
     normed = rms(tokens[...].astype(F32), norm_gain[...].reshape(1, width).astype(F32)).astype(BF)
@@ -129,7 +132,7 @@
     pl.semaphore_wait(barrier, (EP - 1) + (nx - 1))
 
     toks = [
-        rcopy(tok_src.at[(z + d) % NZ], tokbuf.at[d], t_s.at[d], t_r.at[d], zdev(d), x)
+        rcopy(tok_src.at[lax.rem(z + d, NZ)], tokbuf.at[d], t_s.at[d], t_r.at[d], zdev(d), x)
         for d in range(1, NZ)
     ]
     ws = [rcopy(wbuf.at[yc], wbuf.at[yc], w_s.at[d], w_r.at[d], ydev(d), x) for d in range(1, NY)]
@@ -143,7 +146,7 @@
         for d in range(NZ):
             if d:
                 before[d - 1].wait_recv()
-            j = ((z + NZ - d) % NZ) * YC + yc
+            j = lax.rem(z + NZ - d, NZ) * YC + yc
             for dy in range(1, NY):
                 over_y.append((dy, d, rcopy(buf.at[j], buf.at[j], ss.at[dy, d], rs.at[dy, d], ydev(dy), x)))
             over_c.append(rcopy(buf.at[j], buf.at[j], fs.at[0, d], fr.at[0, d], partner, x))
@@ -153,7 +156,7 @@
         over_c = []
         for dy, d, cp in over_y:
             cp.wait_recv()
-            j = ((z + NZ - d) % NZ) * YC + ((y + NY - dy) % NY) * NC + c
+            j = lax.rem(z + NZ - d, NZ) * YC + lax.rem(y + NY - dy, NY) * NC + c
             over_c.append(rcopy(buf.at[j], buf.at[j], fs.at[dy, d], fr.at[dy, d], partner, x))
         return over_c
 
@@ -184,7 +187,7 @@
 
     for d in range(1, NY):
         ws[d - 1].wait_recv()
-        j = ((y + NY - d) % NY) * NC + c
+        j = lax.rem(y + NY - d, NY) * NC + c
         fwd.append(rcopy(wbuf.at[j], wbuf.at[j], wf_s.at[d], wf_r.at[d], partner, x))
     for cp in toks + fwd:
         cp.wait_recv()
@@ -192,11 +195,12 @@
     partial = jnp.dot(
         tokbuf[...].reshape(NZ * seqs, kz), wbuf[...].reshape(kz, cols), preferred_element_type=F32
     ).astype(BF)
-    psend[...] = partial.reshape(NZ, seqs, cols)
-    sums = [
-        rcopy(psend.at[d], prec.at[d], p_s.at[d], p_r.at[d], zdev(NZ - d), x)
-        for d in (4, 3, 5, 2, 6, 1, 7)
-    ]
+    gcols = wg.shape[1]
+    psend[...] = partial[:, 0 : cols - gcols].reshape(NZ, seqs, cols - gcols)
+    gsend[...] = partial[:, cols - gcols :].reshape(NZ, seqs, gcols)
+    far = (4, 3, 5, 2, 6, 1, 7)
+    sums = [rcopy(psend.at[d], prec.at[d], p_s.at[d], p_r.at[d], zdev(NZ - d), x) for d in far]
+    gsums = [rcopy(gsend.at[d], grec.at[d], g_s.at[d], g_r.at[d], zdev(NZ - d), x) for d in far]
     o2, o3 = spread_y(obuf, o1, o2_s, o2_r, o3_s, o3_r)
     for l in sloads:
         l.wait()
@@ -254,31 +258,22 @@
     for d in range(1, NZ):
         total = total + prec[d].astype(F32)
     proj = total.astype(BF).astype(F32)
-    o3 += spread_c(obuf, o2, o3_s, o3_r)
-
     khs = wq.shape[1] // dk
     per = heads // khs
     kq = []
     for i in range(khs):
         q = unit(silu(proj[:, i * dk : (i + 1) * dk])) * dk ** (-0.5)
         k = unit(silu(proj[:, (khs + i) * dk : (khs + i + 1) * dk]))
-        keys_out[:, i * dk : (i + 1) * dk] = k
         kt[i] = k.T
         qt[i] = q.T
         kq.append(jnp.sum(k * q, axis=1, keepdims=True))
     for i in range(khs):
         packed = jnp.where(lane == 2 * heads + i, kq[i], packed)
     rs_ref[...] = packed
-    retain_out[...] = packed
     vbase = 2 * khs * dk
     for h in range(heads):
         vals[h] = silu(proj[:, vbase + h * dv : vbase + (h + 1) * dv])
-    gate = proj[:, vbase + heads * dv :]
     load_state.wait()
-
-    def column(ref, i, s):
-        t = ref[i]
-        return jnp.sum(jnp.where(iota(t.shape, 1) == s, t, 0.0), axis=1, keepdims=True)
 
     def read_one(s, carry):
         rowrs = rs_ref[pl.ds(s, 1), :]
@@ -292,13 +287,19 @@
                 pred = jnp.sum(st * kcol, axis=0, keepdims=True) * ret
                 base = jnp.sum(st * qcol, axis=0, keepdims=True) * ret
                 cor = rowrs[:, heads + h : heads + h + 1] * (vals[h, pl.ds(s, 1), :] - pred)
-                corr_out[h, pl.ds(s, 1), :] = cor
+                corr[h, pl.ds(s, 1), :] = cor
                 ro[h, pl.ds(s, 1), :] = base + dotkq * cor
         return carry
 
-    lax.fori_loop(0, seqs, read_one, 0)
-
-    s2, s3 = spread_y(sbuf, s1, s2_s, s2_r, s3_s, s3_r)
+    lax.fori_loop(0, seqs, read_one, 0, unroll=UNROLL)
+
+    o3 += spread_c(obuf, o2, o3_s, o3_r)
+    for cp in gsums:
+        cp.wait_recv()
+    total = gsend[0].astype(F32)
+    for d in range(1, NZ):
+        total = total + grec[d].astype(F32)
+    gate = total.astype(BF).astype(F32)
     hg = head_gain[...].reshape(1, dv).astype(F32)
     parts = [rms(ro[h], hg) * silu(gate[:, h * dv : (h + 1) * dv]) for h in range(heads)]
     heads_out = jnp.concatenate(parts, axis=1).astype(BF)
@@ -308,8 +309,15 @@
     mixes = [
         rcopy(mix_send, mix_rec.at[d], m_s.at[d], m_r.at[d], e, xdev(d)) for d in range(1, nx)
     ]
-    for l in eloads:
-        l.wait()
+    def write_one(s, carry):
+        rowrs = rs_ref[pl.ds(s, 1), :]
+        for i in range(khs):
+            kcol = column(kt, i, s)
+            for h in range(i * per, (i + 1) * per):
+                state[s, h] = state[s, h] * rowrs[:, h : h + 1] + kcol * corr[h, pl.ds(s, 1), :]
+        return carry
+
+    lax.fori_loop(0, seqs, write_one, 0, unroll=UNROLL)
     mixed = mix_send[...].astype(F32)
     for d in range(1, nx):
         mixes[d - 1].wait_recv()
@@ -326,21 +334,16 @@
         jnp.dot(place, mine, preferred_element_type=F32).astype(BF).reshape(EP, msg, LANES)
     )
 
-    def exchange(src, dst, ss, rs):
-        def one(i, carry):
-            dz, d = i // YC, i % YC
-            to = ((z + dz) % NZ) * YC + (yc + d) % YC
-            cp = pltpu.make_async_remote_copy(
+    def exchange(src, dst, ss, rs, order):
+        for dz, d in order:
+            to = zbase[dz] + ypart[d]
+            pltpu.make_async_remote_copy(
                 src_ref=src.at[to], dst_ref=dst.at[e], send_sem=ss, recv_sem=rs.at[dz],
                 device_id=(to, x), device_id_type=MESH,
-            )
-            cp.start()
-            return carry
-
-        lax.fori_loop(1, EP, one, 0)
+            ).start()
 
     def group_wait(dst, dz, rs):
-        zs = (z + NZ - dz) % NZ
+        zs = lax.rem(z + NZ - dz, NZ)
         n = YC - 1 if dz == 0 else YC
         ref = dst.at[pl.ds(0, n)]
         pltpu.make_async_copy(ref, ref, rs.at[dz]).wait()
@@ -350,32 +353,17 @@
         ref = src.at[pl.ds(0, EP - 1)]
         pltpu.make_async_copy(ref, ref, ss).wait()
 
-    exchange(dsend, xrows.at[x], d_s, d_r)
+    exchange(dsend, xrows.at[x], d_s, d_r, near_first)
     xrows[x, e] = dsend[e]
-
-    s3 += spread_c(sbuf, s2, s3_s, s3_r)
+    s2, s3 = spread_y(sbuf, s1, s2_s, s2_r, s3_s, s3_r)
     xs = []
-    for dz in range(NZ):
+    for dz in (0, 7, 1, 6, 2, 5, 3, 4):
         zs = group_wait(xrows.at[x], dz, d_r)
         for d in range(1, nx):
             block = xrows.at[x, pl.ds(zs * YC, YC)]
             xs.append(rcopy(block, block, x_s.at[d, dz], x_r.at[d, dz], e, xdev(d)))
-    for cp in s3:
-        cp.wait_recv()
-    sgu = jnp.dot(ffn_in, sbuf[:, :, 0 : 2 * hs].reshape(width, 2 * hs), preferred_element_type=F32)
-    sact = (silu(sgu[:, 0:hs]) * sgu[:, hs:]).astype(BF)
-    spart = nt_dot(sact, sbuf[:, :, 2 * hs :].reshape(width, hs)).astype(BF)
-    for i in range(nx * ch):
-        sh_send[i // ch, (i % ch) * seqs : (i % ch + 1) * seqs, :] = spart[:, i * LANES : (i + 1) * LANES]
-    shs = [
-        rcopy(sh_send.at[xdev(d)], sh_rec.at[d], h_s.at[d], h_r.at[d], e, xdev(d)) for d in range(1, nx)
-    ]
-    branch = sigmoid(
-        jnp.sum(
-            ffn_in.astype(F32) * branch_gate[...].reshape(1, width).astype(F32), axis=1, keepdims=True
-        )
-    )
-
+    for l in eloads:
+        l.wait()
     for cp in xs:
         cp.wait_recv()
     gu = jnp.zeros((EP * SLOTS, 2 * he), F32)
@@ -390,6 +378,7 @@
     acts = [
         rcopy(act_all.at[0], act_all.at[d], a_s.at[d], a_r.at[d], e, xdev(d)) for d in range(1, nx)
     ]
+    s3 += spread_c(sbuf, s2, s3_s, s3_r)
     for cp in downs:
         cp.wait_recv()
     eout = jnp.dot(act_all[0], dsrc[x], preferred_element_type=F32)
@@ -399,8 +388,24 @@
     for cc in range(ch):
         outf[pl.ds(cc, EP * SLOTS, stride=ch), :] = eout[:, cc * LANES : (cc + 1) * LANES]
     rsend[...] = outf[...].astype(BF).reshape(EP, msg, LANES)
-    exchange(rsend, rrecv, r_s, r_r)
+    exchange(rsend, rrecv, r_s, r_r, far_first)
     rrecv[e] = rsend[e]
+    for cp in s3:
+        cp.wait_recv()
+    sgu = jnp.dot(ffn_in, sbuf[:, :, 0 : 2 * hs].reshape(width, 2 * hs), preferred_element_type=F32)
+    sact = (silu(sgu[:, 0:hs]) * sgu[:, hs:]).astype(BF)
+    spart = nt_dot(sact, sbuf[:, :, 2 * hs :].reshape(width, hs)).astype(BF)
+    for i in range(nx * ch):
+        sh_send[i // ch, (i % ch) * seqs : (i % ch + 1) * seqs, :] = spart[:, i * LANES : (i + 1) * LANES]
+    shs = [
+        rcopy(sh_send.at[xdev(d)], sh_rec.at[d], h_s.at[d], h_r.at[d], e, xdev(d)) for d in range(1, nx)
+    ]
+    branch = sigmoid(
+        jnp.sum(
+            ffn_in.astype(F32) * branch_gate[...].reshape(1, width).astype(F32), axis=1, keepdims=True
+        )
+    )
+
 
     shared = sh_send[x].astype(F32)
     for d in range(1, nx):
@@ -451,23 +456,21 @@
         layer_kernel,
         out_shape=(
             jax.ShapeDtypeStruct((seqs, width), BF),
-            jax.ShapeDtypeStruct((seqs, khs * dk), F32),
-            jax.ShapeDtypeStruct((heads, seqs, dv), F32),
-            jax.ShapeDtypeStruct((seqs, LANES), F32),
+            pltpu.VMEM(rec.shape, F32),
         ),
         in_specs=[hbm] * 23,
-        out_specs=(vmem,) * 4,
+        out_specs=(vmem,) * 2,
         scratch_shapes=[
             V((seqs, width), BF), V((width,), BF), V(bw.shape[::-1], BF), V(dw.shape[::-1], BF),
             pltpu.SMEM((heads,), F32), pltpu.SMEM((heads,), F32), V((dv,), BF), V((width,), BF),
             V((topk, seqs), I32), V((topk, seqs), F32), V((width,), BF),
-            V(rec.shape, F32),
             V((YC, rows, cols), BF), V((NZ, seqs, kz), BF), V((NZ, seqs, kz), BF),
-            V((NZ, seqs, cols), BF), V((NZ, seqs, cols), BF),
+            V((NZ, seqs, cols - wg.shape[1]), BF), V((NZ, seqs, cols - wg.shape[1]), BF),
+            V((NZ, seqs, wg.shape[1]), BF), V((NZ, seqs, wg.shape[1]), BF),
             V((EP, ow.shape[1], ow.shape[0]), BF), V((EP, sg.shape[0], 3 * hs), BF),
             V((seqs, width), BF), V((nx, seqs, width), BF),
             V((khs, dk, seqs), F32), V((khs, dk, seqs), F32), V((heads, seqs, dv), F32),
-            V((seqs, LANES), F32), V((heads, seqs, dv), F32),
+            V((seqs, LANES), F32), V((heads, seqs, dv), F32), V((heads, seqs, dv), F32),
             V((width, 2 * he), BF), V((nx, he, qc), BF), V((nx, he, qc), BF),
             V((nx * ch, seqs, LANES), BF), V((nx * ch, seqs, LANES), BF),
             V((EP, msg, LANES), BF), V((nx, EP, msg, LANES), BF), V((nx, EP * msg, LANES), F32),
@@ -476,7 +479,7 @@
             V((nx, wide, LANES), BF), V((nx, wide, LANES), BF), V((nx, wide, LANES), BF),
             dma((32,)),
             dma((NY,)), dma((NY,)), dma((NY,)), dma((NY,)),
-            dma((NZ,)), dma((NZ,)), dma((NZ,)), dma((NZ,)),
+            dma((NZ,)), dma((NZ,)), dma((NZ,)), dma((NZ,)), dma((NZ,)), dma((NZ,)),
             dma((NZ,)), dma((NZ,)), dma((NY, NZ)), dma((NY, NZ)), dma((NY, NZ)), dma((NY, NZ)),
             dma((NZ,)), dma((NZ,)), dma((NY, NZ)), dma((NY, NZ)), dma((NY, NZ)), dma((NY, NZ)),
             dma((nx,)), dma((nx,)), dma((nx,)), dma((nx,)),
@@ -484,26 +487,56 @@
             dma((nx,)), dma((nx,)), dma((nx,)), dma((nx,)),
         ],
         compiler_params=pltpu.CompilerParams(
-            collective_id=1, has_side_effects=True, vmem_limit_bytes=67043328
+            collective_id=1, has_side_effects=True, vmem_limit_bytes=LAYER_VMEM
         ),
         name="layer",
     )(
-        tokens, norm_gain, wq, wk, wv, wg, bw.T, dw.T, rate, bias, head_gain, rec, ow.T, ffn_gain,
-        routes.T, rweight.T, eg, eu, ed, sg, su, sd.T, branch_gate,
+        *(
+            pltpu.with_memory_space_constraint(a, pltpu.HBM)
+            for a in (
+                tokens, norm_gain, wq, wk, wv, wg, bw.T, dw.T, rate, bias, head_gain, rec, ow.T, ffn_gain,
+                routes.T, rweight.T, eg, eu, ed, sg, su, sd.T, branch_gate,
+            )
+        )
     )
 
 
+def column(ref, i, s):
+    t = ref[i]
+    return jnp.sum(jnp.where(iota(t.shape, 1) == s, t, 0.0), axis=1, keepdims=True)
+
+
+def store_kernel(layer_in, state, layer_out, new, sems):
+    n = state.shape[0] // STATE_COPIES
+    copies = [
+        pltpu.make_async_copy(
+            state.at[pl.ds(i * n, n)], new.at[pl.ds(i * n, n)], sems.at[i]
+        )
+        for i in range(STATE_COPIES)
+    ]
+    copies.append(pltpu.make_async_copy(layer_in, layer_out, sems.at[STATE_COPIES]))
+    for cp in copies:
+        cp.start()
+    for cp in copies:
+        cp.wait()
+
+
 def per_device(*args):
-    recurrent = args[11]
-    seqs, heads, dk, _ = recurrent.shape
-    layer_out, keys, corr, packed = layer(*args)
-    keys = jnp.repeat(keys.reshape(seqs, -1, dk), heads * dk // keys.shape[1], axis=1)
-    retain = packed[:, 0:heads]
-    new_state = (
-        recurrent * retain[:, :, None, None]
-        + keys[:, :, :, None] * jnp.swapaxes(corr, 0, 1)[:, :, None, :]
-    )
-    return layer_out, new_state
+    layer_out, state = layer(*args)
+    hbm = pl.BlockSpec(memory_space=pltpu.HBM)
+    vmem = pl.BlockSpec(memory_space=pltpu.VMEM)
+    return pl.pallas_call(
+        store_kernel,
+        out_shape=(
+            jax.ShapeDtypeStruct(layer_out.shape, BF),
+            jax.ShapeDtypeStruct(state.shape, F32),
+        ),
+        in_specs=[vmem, vmem],
+        out_specs=(hbm, hbm),
+        scratch_shapes=[pltpu.SemaphoreType.DMA((STATE_COPIES + 1,))],
+        compiler_params=pltpu.CompilerParams(vmem_limit_bytes=8 * 1024 * 1024),
+        name="store",
+    )(layer_out, pltpu.with_memory_space_constraint(state, pltpu.VMEM))
 
 
 def solution(mesh):

time: 86.3 us -> 75.1 us (0.87)
  Pallas kernels: 78.9 us -> 74.3 us
  other arithmetic: 4.39 us -> 0 us
  local copies, waits for them, and re-layouts: 2.15 us -> 0 us
    pallas_call x1, Pallas kernels: 78.9 us -> 72.3 us  [layer(): pl.pallas_call(layer_kernel, out_shape=(jax.ShapeDtypeStruct((seqs, width...]
    add x1 -> x0, other arithmetic: 4.39 us -> none  [per_device(): recurrent * retain[:, :, None, None]]
    pallas_call x0 -> x1, Pallas kernels: none -> 2.06 us  [per_device(): pl.pallas_call(store_kernel, out_shape=(jax.ShapeDtypeStruct(layer_out.sh...]
where the time goes in v3:
time: 75.1 us; the launch traced here: 75 us
  Pallas kernels  74.3 us (99%)
    pallas_call x1, Pallas kernels, layer(): pl.pallas_call(layer_kernel, out_shape=(jax.ShapeDtypeStruct((seqs, width...  72.3 us
    pallas_call x1, Pallas kernels, per_device(): pl.pallas_call(store_kernel, out_shape=(jax.ShapeDtypeStruct(layer_out.sh...  2.06 us

profile of v3, /device:TPU:1, one launch (start us, length us, event | category | flops | bytes accessed | tf_op | source)
XLA Modules:
  0.0 75.0 jit_solution(11348344016773617862)
XLA Ops:
  0.6 72.3 %layer.1 = (bf16[16,2048]{1,0:T(8,128)(2,1)S(1)}, f32[16,4,128,128]{3,2,1,0:T(8,128)S(1)}) custom-call(bf16[16,2048]{1,0:T(8,128)(2,1)} %tokens_h.1, bf16[2048]{0:T(1024)(128)(2,1)} %norm_gain_h.1, bf16[32,256]{1,0:T(8,128)(2,1)} %wq.1, bf16[32,256]{1,0:T(8,128)(2,1)} %wk.1, bf16[32,512]{1,0:T(8,128)(2,1)} %wv.1, bf16[32,512]{1,0:T(8,128)(2,1)} %wg.1, ...), custom_call_target="tpu_custom_call" | custom-call | tf_op jit(solution)/shard_map/layer/pallas_call | solution.py:455
  72.9 2.1 %store.1 = (bf16[16,2048]{1,0:T(8,128)(2,1)}, f32[16,4,128,128]{3,2,1,0:T(8,128)}) custom-call(bf16[16,2048]{1,0:T(8,128)(2,1)S(1)} %get-tuple-element.4.layer_in, f32[16,4,128,128]{3,2,1,0:T(8,128)S(1)} %get-tuple-element.5.state), custom_call_target="tpu_custom_call" | custom-call | tf_op jit(solution)/shard_map/store/pallas_call | solution.py:528

commit v4 on v3

--- a/solution.py
+++ b/solution.py
@@ -11,8 +11,13 @@
 YC = NY * NC
 EP = NZ * YC
 SLOTS = 2
-UNROLL = 4
+UNROLL = 2
 STATE_COPIES = 4
+MIX_CHUNKS = 4
+FAR = (4, 3, 5, 2, 6, 1, 7)
+NEAR = (1, 7, 2, 6, 3, 5, 4)
+GROUPS = ((0,), (1, 7), (2, 6), (3, 5, 4))
+GROUP = {d: i for i, g in enumerate(GROUPS) for d in g}
 LAYER_VMEM = 40 * 1024 * 1024
 LANES = 128
 MESH = pl.DeviceIdType.MESH
@@ -50,12 +55,12 @@
     routes_h, rweight_h, eg_h, eu_h, ed_h, sg_h, su_h, sd_h, branch_h,
     out_ref, state,
     tokens, norm_gain, bw, dw, rate, bias, head_gain, ffn_gain, routes, rweight, branch_gate,
-    wbuf, tok_src, tokbuf, psend, prec, gsend, grec, obuf, sbuf, mix_send, mix_rec,
-    kt, qt, vals, rs_ref, ro, corr,
+    wbuf, gbuf, tok_src, tokbuf, psend, prec, gsend, grec, obuf, sbuf, mix_send, mix_rec,
+    kqt, vals, rs_ref, ro, corr,
     egu, dsrc, dbuf, chunks, res_chunks, dsend, xrows, rowsf, act_all, outf, rsend, rrecv, sh_send, sh_rec, fin,
-    load_sem, w_s, w_r, wf_s, wf_r, t_s, t_r, p_s, p_r, g_s, g_r, o1_s, o1_r, o2_s, o2_r, o3_s, o3_r,
-    s1_s, s1_r, s2_s, s2_r, s3_s, s3_r, m_s, m_r, ed_s, ed_r, d_s, d_r, x_s, x_r, a_s, a_r, r_s, r_r,
-    h_s, h_r, f_s, f_r,
+    load_sem, w_r, gw_r, o1_r, o2_r, s1_r, s2_r, d_r,
+    t_r, wf_r, gf_r, p_r, g_r, o3_r, s3_r, m_r, ed_r, x_r, a_r, r_r, h_r, f_r,
+    t_s, w_s, gw_s, p_s, g_s, o_s, s_s, m_s, ed_s, d_s, x_s, a_s, r_s, h_s, f_s,
 ):
     e = lax.axis_index("ep")
     x = lax.axis_index("tp")
@@ -68,14 +73,15 @@
     xdev = lambda d: lax.rem(x + d, nx)
     seqs, width = tokens.shape
     heads, dk, dv = rec.shape[1:]
-    pending = []
+
+    def wait_all(ref, sem):
+        pltpu.make_async_copy(ref, ref, sem).wait()
 
     def rcopy(src, dst, ss, rs, ep, tp):
         cp = pltpu.make_async_remote_copy(
             src_ref=src, dst_ref=dst, send_sem=ss, recv_sem=rs, device_id=(ep, tp), device_id_type=MESH
         )
         cp.start()
-        pending.append(cp)
         return cp
 
     count = [0]
@@ -89,10 +95,11 @@
     first = [load(tokens_h, tokens), load(norm_gain_h, norm_gain)]
     wloads = []
     at = 0
-    for w in (wq, wk, wv, wg):
+    for w in (wq, wk, wv):
         n = w.shape[1]
         wloads.append(load(w, wbuf.at[yc, :, at : at + n]))
         at += n
+    wloads.append(load(wg, gbuf.at[yc]))
     oload = load(ow_h, obuf.at[e])
     qc = width // nx
     edloads = [load(ed_h.at[0, :, q * qc : (q + 1) * qc], dsrc.at[q]) for q in range(nx)]
@@ -116,8 +123,10 @@
     ypart = [lax.rem(yc + d, YC) for d in range(YC)]
     far_first = [(dz, d) for dz in (4, 3, 5, 2, 6, 1, 7, 0) for d in range(YC) if dz or d]
     near_first = far_first[::-1]
-    for dz, d in far_first:
-        pl.semaphore_signal(barrier, inc=1, device_id=(zbase[dz] + ypart[d], x), device_id_type=MESH)
+    for dz in (4, 3, 5, 2, 6, 1, 7):
+        pl.semaphore_signal(barrier, inc=1, device_id=(zbase[dz] + yc, x), device_id_type=MESH)
+    for d in range(1, YC):
+        pl.semaphore_signal(barrier, inc=1, device_id=(zbase[0] + ypart[d], x), device_id_type=MESH)
     for d in range(1, nx):
         pl.semaphore_signal(barrier, inc=1, device_id=(e, xdev(d)), device_id_type=MESH)
 
@@ -129,41 +138,50 @@
         tok_src[i] = normed[:, i * kz : (i + 1) * kz]
     for l in wloads + [oload] + edloads:
         l.wait()
-    pl.semaphore_wait(barrier, (EP - 1) + (nx - 1))
-
-    toks = [
-        rcopy(tok_src.at[lax.rem(z + d, NZ)], tokbuf.at[d], t_s.at[d], t_r.at[d], zdev(d), x)
-        for d in range(1, NZ)
-    ]
-    ws = [rcopy(wbuf.at[yc], wbuf.at[yc], w_s.at[d], w_r.at[d], ydev(d), x) for d in range(1, NY)]
-    fwd = [rcopy(wbuf.at[yc], wbuf.at[yc], wf_s.at[0], wf_r.at[0], partner, x)]
+    pl.semaphore_wait(barrier, (NZ - 1) + (YC - 1) + (nx - 1))
+
+    for d in FAR:
+        rcopy(tok_src.at[lax.rem(z + d, NZ)], tokbuf.at[d], t_s, t_r, zdev(d), x)
+
+    def rows_y(buf, ss, rs, fr):
+        rcopies = [rcopy(buf.at[yc], buf.at[yc], ss, rs.at[d], ydev(d), x) for d in range(1, NY)]
+        rcopy(buf.at[yc], buf.at[yc], ss, fr, partner, x)
+        return rcopies
+
+    def rows_c(buf, over_y, ss, fr, which):
+        for d in which:
+            over_y[d - 1].wait_recv()
+            j = lax.rem(y + NY - d, NY) * NC + c
+            rcopy(buf.at[j], buf.at[j], ss, fr, partner, x)
+
+    ws = rows_y(wbuf, w_s, w_r, wf_r)
+    gws = rows_y(gbuf, gw_s, gw_r, gf_r)
 
     def spread_z(buf, ss, rs):
-        return [rcopy(buf.at[e], buf.at[e], ss.at[d], rs.at[d], zdev(d), x) for d in range(1, NZ)]
-
-    def spread_y(buf, before, ss, rs, fs, fr):
-        over_y, over_c = [], []
-        for d in range(NZ):
-            if d:
-                before[d - 1].wait_recv()
-            j = lax.rem(z + NZ - d, NZ) * YC + yc
+        for d in NEAR:
+            rcopy(buf.at[e], buf.at[e], ss, rs.at[GROUP[d]], zdev(d), x)
+
+    def z_blocks(which):
+        return [lax.rem(z + NZ - d, NZ) * YC for d in which]
+
+    def spread_y(buf, group, ss, rs, fr):
+        for zb in z_blocks(GROUPS[group]):
+            j = zb + yc
             for dy in range(1, NY):
-                over_y.append((dy, d, rcopy(buf.at[j], buf.at[j], ss.at[dy, d], rs.at[dy, d], ydev(dy), x)))
-            over_c.append(rcopy(buf.at[j], buf.at[j], fs.at[0, d], fr.at[0, d], partner, x))
-        return over_y, over_c
-
-    def spread_c(buf, over_y, fs, fr):
-        over_c = []
-        for dy, d, cp in over_y:
-            cp.wait_recv()
-            j = lax.rem(z + NZ - d, NZ) * YC + lax.rem(y + NY - dy, NY) * NC + c
-            over_c.append(rcopy(buf.at[j], buf.at[j], fs.at[dy, d], fr.at[dy, d], partner, x))
-        return over_c
-
-    o1 = spread_z(obuf, o1_s, o1_r)
-    downs = [
-        rcopy(dsrc.at[xdev(d)], dbuf.at[d], ed_s.at[d], ed_r.at[d], e, xdev(d)) for d in range(1, nx)
-    ]
+                rcopy(buf.at[j], buf.at[j], ss, rs.at[group], ydev(dy), x)
+            rcopy(buf.at[j], buf.at[j], ss, fr, partner, x)
+
+    def spread_c(buf, group, ss, rs, fr):
+        wait_all(buf.at[pl.ds(0, len(GROUPS[group]) * (NY - 1))], rs.at[group])
+        for zb in z_blocks(GROUPS[group]):
+            for dy in range(1, NY):
+                j = zb + lax.rem(y + NY - dy, NY) * NC + c
+                rcopy(buf.at[j], buf.at[j], ss, fr, partner, x)
+
+    spread_z(obuf, o_s, o1_r)
+    spread_y(obuf, 0, o_s, o2_r, o3_r)
+    for d in range(1, nx):
+        rcopy(dsrc.at[xdev(d)], dbuf.at[d], ed_s, ed_r, e, xdev(d))
     tokbuf[0] = tok_src[z]
 
     for l in small:
@@ -185,26 +203,42 @@
         packed = jnp.where(lane == h, retain[h], packed)
         packed = jnp.where(lane == heads + h, strength[h], packed)
 
-    for d in range(1, NY):
-        ws[d - 1].wait_recv()
-        j = lax.rem(y + NY - d, NY) * NC + c
-        fwd.append(rcopy(wbuf.at[j], wbuf.at[j], wf_s.at[d], wf_r.at[d], partner, x))
-    for cp in toks + fwd:
-        cp.wait_recv()
-    cols = wbuf.shape[2]
-    partial = jnp.dot(
-        tokbuf[...].reshape(NZ * seqs, kz), wbuf[...].reshape(kz, cols), preferred_element_type=F32
-    ).astype(BF)
-    gcols = wg.shape[1]
-    psend[...] = partial[:, 0 : cols - gcols].reshape(NZ, seqs, cols - gcols)
-    gsend[...] = partial[:, cols - gcols :].reshape(NZ, seqs, gcols)
-    far = (4, 3, 5, 2, 6, 1, 7)
-    sums = [rcopy(psend.at[d], prec.at[d], p_s.at[d], p_r.at[d], zdev(NZ - d), x) for d in far]
-    gsums = [rcopy(gsend.at[d], grec.at[d], g_s.at[d], g_r.at[d], zdev(NZ - d), x) for d in far]
-    o2, o3 = spread_y(obuf, o1, o2_s, o2_r, o3_s, o3_r)
+    rows_c(wbuf, ws, w_s, wf_r, (1, 3))
+    wait_all(obuf.at[pl.ds(0, len(GROUPS[1]))], o1_r.at[1])
+    spread_y(obuf, 1, o_s, o2_r, o3_r)
+    rows_c(wbuf, ws, w_s, wf_r, (2,))
+    wait_all(tokbuf.at[pl.ds(1, NZ - 1)], t_r)
+    wait_all(wbuf.at[pl.ds(0, NY)], wf_r)
+    toks_all = tokbuf[...].reshape(NZ * seqs, kz)
+
+    def project(buf, sent, got, ss, rs):
+        n = buf.shape[2]
+        sent[...] = (
+            jnp.dot(toks_all, buf[...].reshape(kz, n), preferred_element_type=F32)
+            .astype(BF)
+            .reshape(NZ, seqs, n)
+        )
+        for d in FAR:
+            rcopy(sent.at[d], got.at[d], ss, rs, zdev(NZ - d), x)
+
+    def collected(sent, got, rs):
+        wait_all(got.at[pl.ds(1, NZ - 1)], rs)
+        total = sent[0].astype(F32)
+        for d in range(1, NZ):
+            total = total + got[d].astype(F32)
+        return total.astype(BF).astype(F32)
+
+    project(wbuf, psend, prec, p_s, p_r)
+    rows_c(gbuf, gws, gw_s, gf_r, (1, 3, 2))
+    wait_all(obuf.at[pl.ds(0, len(GROUPS[2]))], o1_r.at[2])
+    spread_y(obuf, 2, o_s, o2_r, o3_r)
+    wait_all(gbuf.at[pl.ds(0, NY)], gf_r)
+    project(gbuf, gsend, grec, g_s, g_r)
+    wait_all(obuf.at[pl.ds(0, len(GROUPS[3]))], o1_r.at[3])
+    spread_y(obuf, 3, o_s, o2_r, o3_r)
     for l in sloads:
         l.wait()
-    s1 = spread_z(sbuf, s1_s, s1_r)
+    spread_z(sbuf, s_s, s1_r)
 
     topk = routes.shape[0]
     rrow = [routes[k : k + 1, :] for k in range(topk)]
@@ -252,20 +286,24 @@
         == iota((topk * wide, rows_all), 1).astype(F32)
     ).astype(BF)
 
-    for cp in sums:
-        cp.wait_recv()
-    total = psend[0].astype(F32)
-    for d in range(1, NZ):
-        total = total + prec[d].astype(F32)
-    proj = total.astype(BF).astype(F32)
+    proj = collected(psend, prec, p_r)
+    for group in range(3):
+        spread_c(obuf, group, o_s, o2_r, o3_r)
     khs = wq.shape[1] // dk
     per = heads // khs
     kq = []
+
+    def split(i, t):
+        hi = t.astype(BF)
+        mid = (t - hi.astype(F32)).astype(BF)
+        lo = (t - hi.astype(F32) - mid.astype(F32)).astype(BF)
+        kqt[i * dk : (i + 1) * dk, :] = jnp.concatenate([hi, mid, lo], axis=1)
+
     for i in range(khs):
         q = unit(silu(proj[:, i * dk : (i + 1) * dk])) * dk ** (-0.5)
         k = unit(silu(proj[:, (khs + i) * dk : (khs + i + 1) * dk]))
-        kt[i] = k.T
-        qt[i] = q.T
+        split(i, k.T)
+        split(khs + i, q.T)
         kq.append(jnp.sum(k * q, axis=1, keepdims=True))
     for i in range(khs):
         packed = jnp.where(lane == 2 * heads + i, kq[i], packed)
@@ -275,53 +313,69 @@
         vals[h] = silu(proj[:, vbase + h * dv : vbase + (h + 1) * dv])
     load_state.wait()
 
-    def read_one(s, carry):
-        rowrs = rs_ref[pl.ds(s, 1), :]
-        for i in range(khs):
-            kcol = column(kt, i, s)
-            qcol = column(qt, i, s)
-            dotkq = rowrs[:, 2 * heads + i : 2 * heads + i + 1]
-            for h in range(i * per, (i + 1) * per):
-                st = state[s, h]
-                ret = rowrs[:, h : h + 1]
-                pred = jnp.sum(st * kcol, axis=0, keepdims=True) * ret
-                base = jnp.sum(st * qcol, axis=0, keepdims=True) * ret
-                cor = rowrs[:, heads + h : heads + h + 1] * (vals[h, pl.ds(s, 1), :] - pred)
-                corr[h, pl.ds(s, 1), :] = cor
-                ro[h, pl.ds(s, 1), :] = base + dotkq * cor
+    span = 2 * dv
+
+    def spread_columns(first, rows):
+        shape = (kqt.shape[1], span)
+        hot = (lax.rem(iota(shape, 0), seqs) == first + iota(shape, 1) // dv).astype(BF)
+        return jnp.dot(kqt[0:rows, :], hot, preferred_element_type=F32)
+
+    def read_pair(p, carry):
+        both = spread_columns(2 * p, 2 * khs * dk)
+        for j in range(2):
+            s = 2 * p + j
+            wide_cols = both[:, j * dv : (j + 1) * dv]
+            rowrs = rs_ref[pl.ds(s, 1), :]
+            for i in range(khs):
+                kcol = wide_cols[i * dk : (i + 1) * dk]
+                qcol = wide_cols[(khs + i) * dk : (khs + i + 1) * dk]
+                dotkq = rowrs[:, 2 * heads + i : 2 * heads + i + 1]
+                for h in range(i * per, (i + 1) * per):
+                    st = state[s, h]
+                    ret = rowrs[:, h : h + 1]
+                    pred = jnp.sum(st * kcol, axis=0, keepdims=True) * ret
+                    base = jnp.sum(st * qcol, axis=0, keepdims=True) * ret
+                    cor = rowrs[:, heads + h : heads + h + 1] * (vals[h, pl.ds(s, 1), :] - pred)
+                    corr[h, pl.ds(s, 1), :] = cor
+                    ro[h, pl.ds(s, 1), :] = base + dotkq * cor
         return carry
 
-    lax.fori_loop(0, seqs, read_one, 0, unroll=UNROLL)
-
-    o3 += spread_c(obuf, o2, o3_s, o3_r)
-    for cp in gsums:
-        cp.wait_recv()
-    total = gsend[0].astype(F32)
-    for d in range(1, NZ):
-        total = total + grec[d].astype(F32)
-    gate = total.astype(BF).astype(F32)
+    lax.fori_loop(0, seqs // 2, read_pair, 0, unroll=UNROLL)
+
+    spread_c(obuf, 3, o_s, o2_r, o3_r)
+    gate = collected(gsend, grec, g_r)
     hg = head_gain[...].reshape(1, dv).astype(F32)
     parts = [rms(ro[h], hg) * silu(gate[:, h * dv : (h + 1) * dv]) for h in range(heads)]
     heads_out = jnp.concatenate(parts, axis=1).astype(BF)
-    for cp in o3:
-        cp.wait_recv()
-    mix_send[...] = nt_dot(heads_out, obuf[...].reshape(width, heads * dv)).astype(BF)
-    mixes = [
-        rcopy(mix_send, mix_rec.at[d], m_s.at[d], m_r.at[d], e, xdev(d)) for d in range(1, nx)
-    ]
-    def write_one(s, carry):
-        rowrs = rs_ref[pl.ds(s, 1), :]
-        for i in range(khs):
-            kcol = column(kt, i, s)
-            for h in range(i * per, (i + 1) * per):
-                state[s, h] = state[s, h] * rowrs[:, h : h + 1] + kcol * corr[h, pl.ds(s, 1), :]
+    wait_all(obuf.at[pl.ds(0, EP // NC)], o3_r)
+    per_chunk = EP // MIX_CHUNKS
+    for i in range(MIX_CHUNKS):
+        n = width // MIX_CHUNKS
+        mix_send[i] = nt_dot(
+            heads_out, obuf[i * per_chunk : (i + 1) * per_chunk].reshape(n, heads * dv)
+        ).astype(BF)
+        for d in range(1, nx):
+            rcopy(mix_send.at[i], mix_rec.at[d, i], m_s, m_r, e, xdev(d))
+    def write_pair(p, carry):
+        both = spread_columns(2 * p, khs * dk)
+        for j in range(2):
+            s = 2 * p + j
+            rowrs = rs_ref[pl.ds(s, 1), :]
+            for i in range(khs):
+                kcol = both[i * dk : (i + 1) * dk, j * dv : (j + 1) * dv]
+                for h in range(i * per, (i + 1) * per):
+                    state[s, h] = state[s, h] * rowrs[:, h : h + 1] + kcol * corr[h, pl.ds(s, 1), :]
         return carry
 
-    lax.fori_loop(0, seqs, write_one, 0, unroll=UNROLL)
-    mixed = mix_send[...].astype(F32)
-    for d in range(1, nx):
-        mixes[d - 1].wait_recv()
-        mixed = mixed + mix_rec[d].astype(F32)
+    lax.fori_loop(0, seqs // 2, write_pair, 0, unroll=UNROLL)
+    wait_all(mix_rec.at[pl.ds(1, nx - 1)], m_r)
+    mixed = []
+    for i in range(MIX_CHUNKS):
+        part = mix_send[i].astype(F32)
+        for d in range(1, nx):
+            part = part + mix_rec[d, i].astype(F32)
+        mixed.append(part)
+    mixed = jnp.concatenate(mixed, axis=1)
     residual = (tokens[...].astype(F32) + mixed).astype(BF)
     ffn_in = rms(residual.astype(F32), ffn_gain[...].reshape(1, width).astype(F32)).astype(BF)
     for i in range(nx * ch):
@@ -338,7 +392,7 @@
         for dz, d in order:
             to = zbase[dz] + ypart[d]
             pltpu.make_async_remote_copy(
-                src_ref=src.at[to], dst_ref=dst.at[e], send_sem=ss, recv_sem=rs.at[dz],
+                src_ref=src.at[to], dst_ref=dst.at[e], send_sem=ss, recv_sem=rs(dz),
                 device_id=(to, x), device_id_type=MESH,
             ).start()
 
@@ -349,23 +403,20 @@
         pltpu.make_async_copy(ref, ref, rs.at[dz]).wait()
         return zs
 
-    def sent_wait(src, ss):
-        ref = src.at[pl.ds(0, EP - 1)]
-        pltpu.make_async_copy(ref, ref, ss).wait()
-
-    exchange(dsend, xrows.at[x], d_s, d_r, near_first)
+    exchange(dsend, xrows.at[x], d_s, lambda dz: d_r.at[dz], near_first)
     xrows[x, e] = dsend[e]
-    s2, s3 = spread_y(sbuf, s1, s2_s, s2_r, s3_s, s3_r)
-    xs = []
     for dz in (0, 7, 1, 6, 2, 5, 3, 4):
         zs = group_wait(xrows.at[x], dz, d_r)
         for d in range(1, nx):
             block = xrows.at[x, pl.ds(zs * YC, YC)]
-            xs.append(rcopy(block, block, x_s.at[d, dz], x_r.at[d, dz], e, xdev(d)))
+            rcopy(block, block, x_s, x_r, e, xdev(d))
     for l in eloads:
         l.wait()
-    for cp in xs:
-        cp.wait_recv()
+    for group in range(4):
+        if group:
+            wait_all(sbuf.at[pl.ds(0, len(GROUPS[group]))], s1_r.at[group])
+        spread_y(sbuf, group, s_s, s2_r, s3_r)
+    wait_all(xrows.at[pl.ds(1, nx - 1)], x_r)
     gu = jnp.zeros((EP * SLOTS, 2 * he), F32)
     for q in range(nx):
         rowsf[q] = xrows[q].reshape(rows_all, LANES).astype(F32)
@@ -375,31 +426,28 @@
         ).astype(BF)
         gu = gu + jnp.dot(left, egu[q * qc : (q + 1) * qc, :], preferred_element_type=F32)
     act_all[0] = (silu(gu[:, 0:he]) * gu[:, he:]).astype(BF)
-    acts = [
-        rcopy(act_all.at[0], act_all.at[d], a_s.at[d], a_r.at[d], e, xdev(d)) for d in range(1, nx)
-    ]
-    s3 += spread_c(sbuf, s2, s3_s, s3_r)
-    for cp in downs:
-        cp.wait_recv()
+    for d in range(1, nx):
+        rcopy(act_all.at[0], act_all.at[d], a_s, a_r, e, xdev(d))
+    wait_all(dbuf.at[pl.ds(1, nx - 1)], ed_r)
     eout = jnp.dot(act_all[0], dsrc[x], preferred_element_type=F32)
+    wait_all(act_all.at[pl.ds(1, nx - 1)], a_r)
     for d in range(1, nx):
-        acts[d - 1].wait_recv()
         eout = eout + jnp.dot(act_all[d], dbuf[d], preferred_element_type=F32)
     for cc in range(ch):
         outf[pl.ds(cc, EP * SLOTS, stride=ch), :] = eout[:, cc * LANES : (cc + 1) * LANES]
     rsend[...] = outf[...].astype(BF).reshape(EP, msg, LANES)
-    exchange(rsend, rrecv, r_s, r_r, far_first)
+    exchange(rsend, rrecv, r_s, lambda dz: r_r, far_first)
     rrecv[e] = rsend[e]
-    for cp in s3:
-        cp.wait_recv()
+    for group in range(4):
+        spread_c(sbuf, group, s_s, s2_r, s3_r)
+    wait_all(sbuf.at[pl.ds(0, EP // NC)], s3_r)
     sgu = jnp.dot(ffn_in, sbuf[:, :, 0 : 2 * hs].reshape(width, 2 * hs), preferred_element_type=F32)
     sact = (silu(sgu[:, 0:hs]) * sgu[:, hs:]).astype(BF)
     spart = nt_dot(sact, sbuf[:, :, 2 * hs :].reshape(width, hs)).astype(BF)
     for i in range(nx * ch):
         sh_send[i // ch, (i % ch) * seqs : (i % ch + 1) * seqs, :] = spart[:, i * LANES : (i + 1) * LANES]
-    shs = [
-        rcopy(sh_send.at[xdev(d)], sh_rec.at[d], h_s.at[d], h_r.at[d], e, xdev(d)) for d in range(1, nx)
-    ]
+    for d in range(1, nx):
+        rcopy(sh_send.at[xdev(d)], sh_rec.at[d], h_s, h_r, e, xdev(d))
     branch = sigmoid(
         jnp.sum(
             ffn_in.astype(F32) * branch_gate[...].reshape(1, width).astype(F32), axis=1, keepdims=True
@@ -408,27 +456,31 @@
 
 
     shared = sh_send[x].astype(F32)
+    wait_all(sh_rec.at[pl.ds(1, nx - 1)], h_r)
     for d in range(1, nx):
-        shs[d - 1].wait_recv()
         shared = shared + sh_rec[d].astype(F32)
     base = res_chunks[pl.ds(x * ch, ch)].reshape(wide, LANES).astype(F32)
     base = base + jnp.concatenate([branch] * ch, axis=0) * shared
-    for dz in range(NZ):
-        group_wait(rrecv, dz, r_r)
+    wait_all(rrecv.at[pl.ds(0, EP - 1)], r_r)
     got = jnp.dot(pick, rrecv[...].reshape(rows_all, LANES), preferred_element_type=F32) * scale_col
     for k in range(topk):
         base = base + got[k * wide : (k + 1) * wide]
     fin[x] = base.astype(BF)
-    fins = [rcopy(fin.at[x], fin.at[x], f_s.at[d], f_r.at[d], e, xdev(d)) for d in range(1, nx)]
-    for cp in fins:
-        cp.wait_recv()
+    for d in range(1, nx):
+        rcopy(fin.at[x], fin.at[x], f_s, f_r, e, xdev(d))
+    wait_all(fin.at[pl.ds(0, nx - 1)], f_r)
     for i in range(nx * ch):
         out_ref[:, i * LANES : (i + 1) * LANES] = fin[i // ch, (i % ch) * seqs : (i % ch + 1) * seqs, :]
 
-    for cp in pending:
-        cp.wait_send()
-    sent_wait(dsend, d_s)
-    sent_wait(rsend, r_s)
+    some = lambda ref, n: ref.at[pl.ds(0, n)]
+    for ref, sem in (
+        (some(tokbuf, NZ - 1), t_s), (some(wbuf, 2 * NY - 1), w_s), (some(gbuf, 2 * NY - 1), gw_s),
+        (some(psend, NZ - 1), p_s), (some(gsend, NZ - 1), g_s), (some(obuf, EP - 1), o_s),
+        (some(sbuf, EP - 1), s_s), (some(mix_rec, nx - 1), m_s), (some(dsrc, nx - 1), ed_s),
+        (some(dsend, EP - 1), d_s), (some(xrows, nx - 1), x_s), (some(act_all, nx - 1), a_s),
+        (some(rsend, EP - 1), r_s), (some(sh_send, nx - 1), h_s), (some(fin, nx - 1), f_s),
+    ):
+        wait_all(ref, sem)
 
 
 def layer(*args):
@@ -464,12 +516,12 @@
             V((seqs, width), BF), V((width,), BF), V(bw.shape[::-1], BF), V(dw.shape[::-1], BF),
             pltpu.SMEM((heads,), F32), pltpu.SMEM((heads,), F32), V((dv,), BF), V((width,), BF),
             V((topk, seqs), I32), V((topk, seqs), F32), V((width,), BF),
-            V((YC, rows, cols), BF), V((NZ, seqs, kz), BF), V((NZ, seqs, kz), BF),
+            V((YC, rows, cols - wg.shape[1]), BF), V((YC, rows, wg.shape[1]), BF), V((NZ, seqs, kz), BF), V((NZ, seqs, kz), BF),
             V((NZ, seqs, cols - wg.shape[1]), BF), V((NZ, seqs, cols - wg.shape[1]), BF),
             V((NZ, seqs, wg.shape[1]), BF), V((NZ, seqs, wg.shape[1]), BF),
             V((EP, ow.shape[1], ow.shape[0]), BF), V((EP, sg.shape[0], 3 * hs), BF),
-            V((seqs, width), BF), V((nx, seqs, width), BF),
-            V((khs, dk, seqs), F32), V((khs, dk, seqs), F32), V((heads, seqs, dv), F32),
+            V((MIX_CHUNKS, seqs, width // MIX_CHUNKS), BF), V((nx, MIX_CHUNKS, seqs, width // MIX_CHUNKS), BF),
+            V((2 * khs * dk, 3 * seqs), BF), V((heads, seqs, dv), F32),
             V((seqs, LANES), F32), V((heads, seqs, dv), F32), V((heads, seqs, dv), F32),
             V((width, 2 * he), BF), V((nx, he, qc), BF), V((nx, he, qc), BF),
             V((nx * ch, seqs, LANES), BF), V((nx * ch, seqs, LANES), BF),
@@ -477,14 +529,8 @@
             V((nx, EP * SLOTS, he), BF), V((EP * msg, LANES), F32),
             V((EP, msg, LANES), BF), V((EP, msg, LANES), BF),
             V((nx, wide, LANES), BF), V((nx, wide, LANES), BF), V((nx, wide, LANES), BF),
-            dma((32,)),
-            dma((NY,)), dma((NY,)), dma((NY,)), dma((NY,)),
-            dma((NZ,)), dma((NZ,)), dma((NZ,)), dma((NZ,)), dma((NZ,)), dma((NZ,)),
-            dma((NZ,)), dma((NZ,)), dma((NY, NZ)), dma((NY, NZ)), dma((NY, NZ)), dma((NY, NZ)),
-            dma((NZ,)), dma((NZ,)), dma((NY, NZ)), dma((NY, NZ)), dma((NY, NZ)), dma((NY, NZ)),
-            dma((nx,)), dma((nx,)), dma((nx,)), dma((nx,)),
-            dma, dma((NZ,)), dma((nx, NZ)), dma((nx, NZ)), dma((nx,)), dma((nx,)), dma, dma((NZ,)),
-            dma((nx,)), dma((nx,)), dma((nx,)), dma((nx,)),
+            dma((26,)), dma((NY,)), dma((NY,)), dma((4,)), dma((4,)), dma((4,)), dma((4,)), dma((NZ,)),
+            *[dma] * 29,
         ],
         compiler_params=pltpu.CompilerParams(
             collective_id=1, has_side_effects=True, vmem_limit_bytes=LAYER_VMEM
@@ -499,11 +545,6 @@
             )
         )
     )
-
-
-def column(ref, i, s):
-    t = ref[i]
-    return jnp.sum(jnp.where(iota(t.shape, 1) == s, t, 0.0), axis=1, keepdims=True)
 
 
 def store_kernel(layer_in, state, layer_out, new, sems):

time: 75.1 us -> 65.6 us (0.87)
  Pallas kernels: 74.3 us -> 64.9 us
    pallas_call x1, Pallas kernels: 72.3 us -> 62.8 us  [layer(): pl.pallas_call(layer_kernel, out_shape=(jax.ShapeDtypeStruct((seqs, width...]
where the time goes in v4:
time: 65.6 us; the launch traced here: 65.5 us
  Pallas kernels  64.9 us (99%)
    pallas_call x1, Pallas kernels, layer(): pl.pallas_call(layer_kernel, out_shape=(jax.ShapeDtypeStruct((seqs, width...  62.8 us
    pallas_call x1, Pallas kernels, per_device(): pl.pallas_call(store_kernel, out_shape=(jax.ShapeDtypeStruct(layer_out.sh...  2.06 us

profile of v4, /device:TPU:1, one launch (start us, length us, event | category | flops | bytes accessed | tf_op | source)
XLA Modules:
  0.0 65.5 jit_solution(18076600233226520825)
XLA Ops:
  0.6 62.8 %layer.1 = (bf16[16,2048]{1,0:T(8,128)(2,1)S(1)}, f32[16,4,128,128]{3,2,1,0:T(8,128)S(1)}) custom-call(bf16[16,2048]{1,0:T(8,128)(2,1)} %tokens_h.1, bf16[2048]{0:T(1024)(128)(2,1)} %norm_gain_h.1, bf16[32,256]{1,0:T(8,128)(2,1)} %wq.1, bf16[32,256]{1,0:T(8,128)(2,1)} %wk.1, bf16[32,512]{1,0:T(8,128)(2,1)} %wv.1, bf16[32,512]{1,0:T(8,128)(2,1)} %wg.1, ...), custom_call_target="tpu_custom_call" | custom-call | tf_op jit(solution)/shard_map/layer/pallas_call | solution.py:507
  63.5 2.1 %store.1 = (bf16[16,2048]{1,0:T(8,128)(2,1)}, f32[16,4,128,128]{3,2,1,0:T(8,128)}) custom-call(bf16[16,2048]{1,0:T(8,128)(2,1)S(1)} %get-tuple-element.4.layer_in, f32[16,4,128,128]{3,2,1,0:T(8,128)S(1)} %get-tuple-element.5.state), custom_call_target="tpu_custom_call" | custom-call | tf_op jit(solution)/shard_map/store/pallas_call | solution.py:569

commit v5 on v4

--- a/solution.py
+++ b/solution.py
@@ -13,10 +13,11 @@
 SLOTS = 2
 UNROLL = 2
 STATE_COPIES = 4
-MIX_CHUNKS = 4
 FAR = (4, 3, 5, 2, 6, 1, 7)
 NEAR = (1, 7, 2, 6, 3, 5, 4)
 GROUPS = ((0,), (1, 7), (2, 6), (3, 5, 4))
+SEND_ORDER = (0, 7, 1, 6, 2, 5, 3, 4)
+ARRIVAL = (0, 7, 1, 6, 2, 5, 3, 4)
 GROUP = {d: i for i, g in enumerate(GROUPS) for d in g}
 LAYER_VMEM = 40 * 1024 * 1024
 LANES = 128
@@ -57,10 +58,10 @@
     tokens, norm_gain, bw, dw, rate, bias, head_gain, ffn_gain, routes, rweight, branch_gate,
     wbuf, gbuf, tok_src, tokbuf, psend, prec, gsend, grec, obuf, sbuf, mix_send, mix_rec,
     kqt, vals, rs_ref, ro, corr,
-    egu, dsrc, dbuf, chunks, res_chunks, dsend, xrows, rowsf, act_all, outf, rsend, rrecv, sh_send, sh_rec, fin,
+    egu, dsrc, dbuf, tok_chunks, res_all, dsend, xrows, rowsf, act_all, outf, rsend, rrecv, sh_send, sh_rec, fin,
     load_sem, w_r, gw_r, o1_r, o2_r, s1_r, s2_r, d_r,
-    t_r, wf_r, gf_r, p_r, g_r, o3_r, s3_r, m_r, ed_r, x_r, a_r, r_r, h_r, f_r,
-    t_s, w_s, gw_s, p_s, g_s, o_s, s_s, m_s, ed_s, d_s, x_s, a_s, r_s, h_s, f_s,
+    x_r, a_r, t_r, wf_r, gf_r, p_r, g_r, o3_r, s3_r, m_r, ed_r, r_r, h_r, f_r, n_r,
+    t_s, w_s, gw_s, p_s, g_s, o_s, s_s, m_s, ed_s, d_s, x_s, a_s, r_s, h_s, f_s, n_s,
 ):
     e = lax.axis_index("ep")
     x = lax.axis_index("tp")
@@ -71,6 +72,8 @@
     zdev = lambda d: lax.rem(z + d, NZ) * YC + yc
     ydev = lambda d: z * YC + lax.rem(y + d, NY) * NC + c
     xdev = lambda d: lax.rem(x + d, nx)
+    peers = sorted(range(1, nx), key=lambda d: -min(d, nx - d))
+    ypeers = sorted(range(1, NY), key=lambda d: -min(d, NY - d))
     seqs, width = tokens.shape
     heads, dk, dv = rec.shape[1:]
 
@@ -86,43 +89,40 @@
 
     count = [0]
 
-    def load(src, dst):
-        cp = pltpu.make_async_copy(src, dst, load_sem.at[count[0]])
+    def load(*pairs):
+        sem = load_sem.at[count[0]]
         count[0] += 1
-        cp.start()
-        return cp
-
-    first = [load(tokens_h, tokens), load(norm_gain_h, norm_gain)]
-    wloads = []
-    at = 0
+        for src, dst in pairs:
+            pltpu.make_async_copy(src, dst, sem).start()
+        return sem
+
+    cuts = [0]
     for w in (wq, wk, wv):
-        n = w.shape[1]
-        wloads.append(load(w, wbuf.at[yc, :, at : at + n]))
-        at += n
-    wloads.append(load(wg, gbuf.at[yc]))
-    oload = load(ow_h, obuf.at[e])
+        cuts.append(cuts[-1] + w.shape[1])
+    w_load = load(*((w, wbuf.at[yc, :, cuts[i] : cuts[i + 1]]) for i, w in enumerate((wq, wk, wv))))
+    first = [(a, load((b, a))) for a, b in ((tokens, tokens_h), (norm_gain, norm_gain_h))]
+    g_load = load((wg, gbuf.at[yc]))
+    o_load = load((ow_h, obuf.at[e]))
     qc = width // nx
-    edloads = [load(ed_h.at[0, :, q * qc : (q + 1) * qc], dsrc.at[q]) for q in range(nx)]
+    ed_load = load(*((ed_h.at[0, :, q * qc : (q + 1) * qc], dsrc.at[q]) for q in range(nx)))
     small = [
-        load(a, b)
+        (b, load((a, b)))
         for a, b in (
             (bw_h, bw), (dw_h, dw), (rate_h, rate), (bias_h, bias), (head_gain_h, head_gain),
             (ffn_gain_h, ffn_gain), (routes_h, routes), (rweight_h, rweight), (branch_h, branch_gate),
         )
     ]
     hs = sg_h.shape[1]
-    sloads = [
-        load(a, sbuf.at[e, :, i * hs : (i + 1) * hs]) for i, a in enumerate((sg_h, su_h, sd_h))
-    ]
-    load_state = load(rec, state)
+    s_load = load(
+        *((a, sbuf.at[e, :, i * hs : (i + 1) * hs]) for i, a in enumerate((sg_h, su_h, sd_h)))
+    )
+    state_load = load((rec, state))
     he = eg_h.shape[2]
-    eloads = [load(eg_h.at[0], egu.at[:, 0:he]), load(eu_h.at[0], egu.at[:, he : 2 * he])]
+    e_load = load((eg_h.at[0], egu.at[:, 0:he]), (eu_h.at[0], egu.at[:, he : 2 * he]))
 
     barrier = pltpu.get_barrier_semaphore()
     zbase = [lax.rem(z + d, NZ) * YC for d in range(NZ)]
     ypart = [lax.rem(yc + d, YC) for d in range(YC)]
-    far_first = [(dz, d) for dz in (4, 3, 5, 2, 6, 1, 7, 0) for d in range(YC) if dz or d]
-    near_first = far_first[::-1]
     for dz in (4, 3, 5, 2, 6, 1, 7):
         pl.semaphore_signal(barrier, inc=1, device_id=(zbase[dz] + yc, x), device_id_type=MESH)
     for d in range(1, YC):
@@ -130,32 +130,32 @@
     for d in range(1, nx):
         pl.semaphore_signal(barrier, inc=1, device_id=(e, xdev(d)), device_id_type=MESH)
 
-    for l in first:
-        l.wait()
+    def rows_y(buf, ss, rs, fr):
+        rcopies = [rcopy(buf.at[yc], buf.at[yc], ss, rs.at[d], ydev(d), x) for d in ypeers]
+        rcopy(buf.at[yc], buf.at[yc], ss, fr, partner, x)
+        return dict(zip(ypeers, rcopies))
+
+    def rows_c(buf, over_y, ss, fr, which):
+        for d in which:
+            over_y[d].wait_recv()
+            j = lax.rem(y + NY - d, NY) * NC + c
+            rcopy(buf.at[j], buf.at[j], ss, fr, partner, x)
+
+    wait_all(wbuf.at[yc], w_load)
+    pl.semaphore_wait(barrier, (NZ - 1) + (YC - 1) + (nx - 1))
+    ws = rows_y(wbuf, w_s, w_r, wf_r)
+    for ref, sem in first:
+        wait_all(ref, sem)
     normed = rms(tokens[...].astype(F32), norm_gain[...].reshape(1, width).astype(F32)).astype(BF)
     kz = tokbuf.shape[2]
     for i in range(NZ):
         tok_src[i] = normed[:, i * kz : (i + 1) * kz]
-    for l in wloads + [oload] + edloads:
-        l.wait()
-    pl.semaphore_wait(barrier, (NZ - 1) + (YC - 1) + (nx - 1))
-
     for d in FAR:
         rcopy(tok_src.at[lax.rem(z + d, NZ)], tokbuf.at[d], t_s, t_r, zdev(d), x)
-
-    def rows_y(buf, ss, rs, fr):
-        rcopies = [rcopy(buf.at[yc], buf.at[yc], ss, rs.at[d], ydev(d), x) for d in range(1, NY)]
-        rcopy(buf.at[yc], buf.at[yc], ss, fr, partner, x)
-        return rcopies
-
-    def rows_c(buf, over_y, ss, fr, which):
-        for d in which:
-            over_y[d - 1].wait_recv()
-            j = lax.rem(y + NY - d, NY) * NC + c
-            rcopy(buf.at[j], buf.at[j], ss, fr, partner, x)
-
-    ws = rows_y(wbuf, w_s, w_r, wf_r)
+    wait_all(gbuf.at[yc], g_load)
     gws = rows_y(gbuf, gw_s, gw_r, gf_r)
+    wait_all(obuf.at[e], o_load)
+    wait_all(dsrc, ed_load)
 
     def spread_z(buf, ss, rs):
         for d in NEAR:
@@ -167,7 +167,7 @@
     def spread_y(buf, group, ss, rs, fr):
         for zb in z_blocks(GROUPS[group]):
             j = zb + yc
-            for dy in range(1, NY):
+            for dy in ypeers:
                 rcopy(buf.at[j], buf.at[j], ss, rs.at[group], ydev(dy), x)
             rcopy(buf.at[j], buf.at[j], ss, fr, partner, x)
 
@@ -180,12 +180,12 @@
 
     spread_z(obuf, o_s, o1_r)
     spread_y(obuf, 0, o_s, o2_r, o3_r)
-    for d in range(1, nx):
+    for d in peers:
         rcopy(dsrc.at[xdev(d)], dbuf.at[d], ed_s, ed_r, e, xdev(d))
     tokbuf[0] = tok_src[z]
 
-    for l in small:
-        l.wait()
+    for ref, sem in small:
+        wait_all(ref, sem)
     bl = nt_dot(normed, bw[...])
     dl = nt_dot(normed, dw[...])
     lanes = iota(bl.shape, 1)
@@ -236,10 +236,18 @@
     project(gbuf, gsend, grec, g_s, g_r)
     wait_all(obuf.at[pl.ds(0, len(GROUPS[3]))], o1_r.at[3])
     spread_y(obuf, 3, o_s, o2_r, o3_r)
-    for l in sloads:
-        l.wait()
+    wait_all(sbuf.at[e], s_load)
     spread_z(sbuf, s_s, s1_r)
 
+    def s_relay(group):
+        if group:
+            wait_all(sbuf.at[pl.ds(0, len(GROUPS[group]))], s1_r.at[group])
+        spread_y(sbuf, group, s_s, s2_r, s3_r)
+
+
+    ch = qc // LANES
+    for i in range(nx * ch):
+        tok_chunks[i] = tokens[:, i * LANES : (i + 1) * LANES]
     topk = routes.shape[0]
     rrow = [routes[k : k + 1, :] for k in range(topk)]
     square = (seqs, seqs)
@@ -260,7 +268,6 @@
             hits_r += jnp.where(before_r & (rrow[k] == rcol[k2]), 1.0, 0.0)
         tcol.append(rcol[k] * SLOTS + jnp.sum(hits_c, axis=1, keepdims=True))
         trow.append(rrow[k] * SLOTS + jnp.sum(hits_r, axis=0, keepdims=True))
-    ch = qc // LANES
     wide = ch * seqs
     spreadm = (iota((seqs, wide), 1) % seqs == iota((seqs, wide), 0)).astype(BF)
     rows_all = EP * SLOTS * ch
@@ -311,7 +318,7 @@
     vbase = 2 * khs * dk
     for h in range(heads):
         vals[h] = silu(proj[:, vbase + h * dv : vbase + (h + 1) * dv])
-    load_state.wait()
+    wait_all(state, state_load)
 
     span = 2 * dv
 
@@ -348,14 +355,11 @@
     parts = [rms(ro[h], hg) * silu(gate[:, h * dv : (h + 1) * dv]) for h in range(heads)]
     heads_out = jnp.concatenate(parts, axis=1).astype(BF)
     wait_all(obuf.at[pl.ds(0, EP // NC)], o3_r)
-    per_chunk = EP // MIX_CHUNKS
-    for i in range(MIX_CHUNKS):
-        n = width // MIX_CHUNKS
-        mix_send[i] = nt_dot(
-            heads_out, obuf[i * per_chunk : (i + 1) * per_chunk].reshape(n, heads * dv)
-        ).astype(BF)
-        for d in range(1, nx):
-            rcopy(mix_send.at[i], mix_rec.at[d, i], m_s, m_r, e, xdev(d))
+    mix = nt_dot(heads_out, obuf[...].reshape(width, heads * dv)).astype(BF)
+    for q in range(nx):
+        mix_send[q] = mix[:, q * qc : (q + 1) * qc]
+    for d in peers:
+        rcopy(mix_send.at[xdev(d)], mix_rec.at[d], m_s, m_r, e, xdev(d))
     def write_pair(p, carry):
         both = spread_columns(2 * p, khs * dk)
         for j in range(2):
@@ -368,105 +372,122 @@
         return carry
 
     lax.fori_loop(0, seqs // 2, write_pair, 0, unroll=UNROLL)
+    s_relay(0)
+    s_relay(1)
     wait_all(mix_rec.at[pl.ds(1, nx - 1)], m_r)
-    mixed = []
-    for i in range(MIX_CHUNKS):
-        part = mix_send[i].astype(F32)
-        for d in range(1, nx):
-            part = part + mix_rec[d, i].astype(F32)
-        mixed.append(part)
-    mixed = jnp.concatenate(mixed, axis=1)
-    residual = (tokens[...].astype(F32) + mixed).astype(BF)
-    ffn_in = rms(residual.astype(F32), ffn_gain[...].reshape(1, width).astype(F32)).astype(BF)
-    for i in range(nx * ch):
-        chunks[i] = ffn_in[:, i * LANES : (i + 1) * LANES]
-        res_chunks[i] = residual[:, i * LANES : (i + 1) * LANES]
-
-    mine = chunks[pl.ds(x * ch, ch)].reshape(wide, LANES)
+    mixed = mix_send[x].astype(F32)
+    for d in range(1, nx):
+        mixed = mixed + mix_rec[d].astype(F32)
+    own = tok_chunks[pl.ds(x * ch, ch)].astype(F32)
+    mine = jnp.concatenate(
+        [own[cc] + mixed[:, cc * LANES : (cc + 1) * LANES] for cc in range(ch)], axis=0
+    ).astype(BF)
+    res_all[x] = mine
     msg = SLOTS * ch
     dsend[...] = (
         jnp.dot(place, mine, preferred_element_type=F32).astype(BF).reshape(EP, msg, LANES)
     )
 
-    def exchange(src, dst, ss, rs, order):
-        for dz, d in order:
-            to = zbase[dz] + ypart[d]
-            pltpu.make_async_remote_copy(
-                src_ref=src.at[to], dst_ref=dst.at[e], send_sem=ss, recv_sem=rs(dz),
-                device_id=(to, x), device_id_type=MESH,
-            ).start()
-
-    def group_wait(dst, dz, rs):
-        zs = lax.rem(z + NZ - dz, NZ)
-        n = YC - 1 if dz == 0 else YC
-        ref = dst.at[pl.ds(0, n)]
-        pltpu.make_async_copy(ref, ref, rs.at[dz]).wait()
-        return zs
-
-    exchange(dsend, xrows.at[x], d_s, lambda dz: d_r.at[dz], near_first)
-    xrows[x, e] = dsend[e]
-    for dz in (0, 7, 1, 6, 2, 5, 3, 4):
-        zs = group_wait(xrows.at[x], dz, d_r)
+    zback = [lax.rem(z + NZ - d, NZ) * YC for d in range(NZ)]
+    yback = [lax.rem(yc + YC - d, YC) for d in range(YC)]
+    place_of = {dz: i * YC for i, dz in enumerate(ARRIVAL)}
+    half = EP // 2
+    part_of = lambda dz: place_of[dz] // half
+    for dz in SEND_ORDER:
+        for d in range(YC):
+            if dz or d:
+                to = zbase[dz] + ypart[d]
+                rcopy(dsend.at[to], xrows.at[x, place_of[dz] + d], d_s, d_r.at[dz], to, x)
+    xrows[x, 0] = dsend[e]
+    for d in peers:
+        rcopy(res_all.at[x], res_all.at[x], n_s, n_r, e, xdev(d))
+    for dz in ARRIVAL:
+        n = YC if dz else YC - 1
+        wait_all(xrows.at[x, pl.ds(place_of[dz], n)], d_r.at[dz])
+        block = xrows.at[x, pl.ds(place_of[dz], YC)]
+        for d in peers:
+            rcopy(block, block, x_s, x_r.at[part_of(dz)], e, xdev(d))
+    s_relay(2)
+    s_relay(3)
+    wait_all(egu, e_load)
+    fgain = ffn_gain[...].reshape(1, width).astype(F32)
+    nrows = half * SLOTS
+
+    def dense_branch():
+        for group in range(4):
+            spread_c(sbuf, group, s_s, s2_r, s3_r)
+        wait_all(sbuf.at[pl.ds(0, EP // NC)], s3_r)
+        wait_all(res_all.at[pl.ds(0, nx - 1)], n_r)
+        residual = jnp.concatenate(
+            [res_all[i // ch, (i % ch) * seqs : (i % ch + 1) * seqs, :] for i in range(nx * ch)], axis=1
+        ).astype(F32)
+        ffn_in = rms(residual, fgain).astype(BF)
+        sgu = jnp.dot(ffn_in, sbuf[:, :, 0 : 2 * hs].reshape(width, 2 * hs), preferred_element_type=F32)
+        sact = (silu(sgu[:, 0:hs]) * sgu[:, hs:]).astype(BF)
+        spart = nt_dot(sact, sbuf[:, :, 2 * hs :].reshape(width, hs)).astype(BF)
+        for i in range(nx * ch):
+            sh_send[i // ch, (i % ch) * seqs : (i % ch + 1) * seqs, :] = spart[:, i * LANES : (i + 1) * LANES]
+        for d in peers:
+            rcopy(sh_send.at[xdev(d)], sh_rec.at[d], h_s, h_r, e, xdev(d))
+        branch = sigmoid(
+            jnp.sum(
+                ffn_in.astype(F32) * branch_gate[...].reshape(1, width).astype(F32), axis=1, keepdims=True
+            )
+        )
+        return branch
+
+    for p in range(2):
+        wait_all(xrows.at[pl.ds(1, nx - 1), pl.ds(p * half, half)], x_r.at[p])
+        for q in range(nx):
+            rowsf[q] = xrows[q, p * half : (p + 1) * half].reshape(half * msg, LANES).astype(F32)
+        piece = lambda q, cc: rowsf[q, pl.ds(cc, nrows, stride=ch), :]
+        squares = jnp.zeros((nrows, LANES), F32)
+        for q in range(nx):
+            for cc in range(ch):
+                v = piece(q, cc)
+                squares = squares + v * v
+        inv = lax.rsqrt(jnp.sum(squares, axis=1, keepdims=True) / width + EPS)
+        gu = jnp.zeros((nrows, 2 * he), F32)
+        for q in range(nx):
+            left = jnp.concatenate(
+                [
+                    piece(q, cc) * inv * fgain[:, q * qc + cc * LANES : q * qc + (cc + 1) * LANES]
+                    for cc in range(ch)
+                ],
+                axis=1,
+            ).astype(BF)
+            gu = gu + jnp.dot(left, egu[q * qc : (q + 1) * qc, :], preferred_element_type=F32)
+        act_all[p, 0] = (silu(gu[:, 0:he]) * gu[:, he:]).astype(BF)
+        for d in peers:
+            rcopy(act_all.at[p, 0], act_all.at[p, d], a_s, a_r.at[p], e, xdev(d))
+
+    wait_all(dbuf.at[pl.ds(1, nx - 1)], ed_r)
+    for p in range(2):
+        eout = jnp.dot(act_all[p, 0], dsrc[x], preferred_element_type=F32)
+        wait_all(act_all.at[p, pl.ds(1, nx - 1)], a_r.at[p])
         for d in range(1, nx):
-            block = xrows.at[x, pl.ds(zs * YC, YC)]
-            rcopy(block, block, x_s, x_r, e, xdev(d))
-    for l in eloads:
-        l.wait()
-    for group in range(4):
-        if group:
-            wait_all(sbuf.at[pl.ds(0, len(GROUPS[group]))], s1_r.at[group])
-        spread_y(sbuf, group, s_s, s2_r, s3_r)
-    wait_all(xrows.at[pl.ds(1, nx - 1)], x_r)
-    gu = jnp.zeros((EP * SLOTS, 2 * he), F32)
-    for q in range(nx):
-        rowsf[q] = xrows[q].reshape(rows_all, LANES).astype(F32)
-    for q in range(nx):
-        left = jnp.concatenate(
-            [rowsf[q, pl.ds(cc, EP * SLOTS, stride=ch), :] for cc in range(ch)], axis=1
-        ).astype(BF)
-        gu = gu + jnp.dot(left, egu[q * qc : (q + 1) * qc, :], preferred_element_type=F32)
-    act_all[0] = (silu(gu[:, 0:he]) * gu[:, he:]).astype(BF)
-    for d in range(1, nx):
-        rcopy(act_all.at[0], act_all.at[d], a_s, a_r, e, xdev(d))
-    wait_all(dbuf.at[pl.ds(1, nx - 1)], ed_r)
-    eout = jnp.dot(act_all[0], dsrc[x], preferred_element_type=F32)
-    wait_all(act_all.at[pl.ds(1, nx - 1)], a_r)
-    for d in range(1, nx):
-        eout = eout + jnp.dot(act_all[d], dbuf[d], preferred_element_type=F32)
-    for cc in range(ch):
-        outf[pl.ds(cc, EP * SLOTS, stride=ch), :] = eout[:, cc * LANES : (cc + 1) * LANES]
-    rsend[...] = outf[...].astype(BF).reshape(EP, msg, LANES)
-    exchange(rsend, rrecv, r_s, lambda dz: r_r, far_first)
-    rrecv[e] = rsend[e]
-    for group in range(4):
-        spread_c(sbuf, group, s_s, s2_r, s3_r)
-    wait_all(sbuf.at[pl.ds(0, EP // NC)], s3_r)
-    sgu = jnp.dot(ffn_in, sbuf[:, :, 0 : 2 * hs].reshape(width, 2 * hs), preferred_element_type=F32)
-    sact = (silu(sgu[:, 0:hs]) * sgu[:, hs:]).astype(BF)
-    spart = nt_dot(sact, sbuf[:, :, 2 * hs :].reshape(width, hs)).astype(BF)
-    for i in range(nx * ch):
-        sh_send[i // ch, (i % ch) * seqs : (i % ch + 1) * seqs, :] = spart[:, i * LANES : (i + 1) * LANES]
-    for d in range(1, nx):
-        rcopy(sh_send.at[xdev(d)], sh_rec.at[d], h_s, h_r, e, xdev(d))
-    branch = sigmoid(
-        jnp.sum(
-            ffn_in.astype(F32) * branch_gate[...].reshape(1, width).astype(F32), axis=1, keepdims=True
-        )
-    )
-
-
+            eout = eout + jnp.dot(act_all[p, d], dbuf[d], preferred_element_type=F32)
+        for cc in range(ch):
+            outf[pl.ds(cc, nrows, stride=ch), :] = eout[:, cc * LANES : (cc + 1) * LANES]
+        rsend[p * half : (p + 1) * half] = outf[...].astype(BF).reshape(half, msg, LANES)
+        for dz in ARRIVAL[::-1]:
+            for d in range(YC):
+                if part_of(dz) == p and (dz or d):
+                    rcopy(rsend.at[place_of[dz] + d], rrecv.at[e], r_s, r_r, zback[dz] + yback[d], x)
+    rrecv[e] = rsend[0]
+    branch = dense_branch()
     shared = sh_send[x].astype(F32)
     wait_all(sh_rec.at[pl.ds(1, nx - 1)], h_r)
     for d in range(1, nx):
         shared = shared + sh_rec[d].astype(F32)
-    base = res_chunks[pl.ds(x * ch, ch)].reshape(wide, LANES).astype(F32)
+    base = mine.astype(F32)
     base = base + jnp.concatenate([branch] * ch, axis=0) * shared
     wait_all(rrecv.at[pl.ds(0, EP - 1)], r_r)
     got = jnp.dot(pick, rrecv[...].reshape(rows_all, LANES), preferred_element_type=F32) * scale_col
     for k in range(topk):
         base = base + got[k * wide : (k + 1) * wide]
     fin[x] = base.astype(BF)
-    for d in range(1, nx):
+    for d in peers:
         rcopy(fin.at[x], fin.at[x], f_s, f_r, e, xdev(d))
     wait_all(fin.at[pl.ds(0, nx - 1)], f_r)
     for i in range(nx * ch):
@@ -477,8 +498,8 @@
         (some(tokbuf, NZ - 1), t_s), (some(wbuf, 2 * NY - 1), w_s), (some(gbuf, 2 * NY - 1), gw_s),
         (some(psend, NZ - 1), p_s), (some(gsend, NZ - 1), g_s), (some(obuf, EP - 1), o_s),
         (some(sbuf, EP - 1), s_s), (some(mix_rec, nx - 1), m_s), (some(dsrc, nx - 1), ed_s),
-        (some(dsend, EP - 1), d_s), (some(xrows, nx - 1), x_s), (some(act_all, nx - 1), a_s),
-        (some(rsend, EP - 1), r_s), (some(sh_send, nx - 1), h_s), (some(fin, nx - 1), f_s),
+        (some(dsend, EP - 1), d_s), (some(xrows, nx - 1), x_s), (act_all.at[:, pl.ds(1, nx - 1)], a_s),
+        (some(rsend, EP - 1), r_s), (some(sh_send, nx - 1), h_s), (some(fin, nx - 1), f_s), (some(res_all, nx - 1), n_s),
     ):
         wait_all(ref, sem)
 
@@ -520,17 +541,17 @@
             V((NZ, seqs, cols - wg.shape[1]), BF), V((NZ, seqs, cols - wg.shape[1]), BF),
             V((NZ, seqs, wg.shape[1]), BF), V((NZ, seqs, wg.shape[1]), BF),
             V((EP, ow.shape[1], ow.shape[0]), BF), V((EP, sg.shape[0], 3 * hs), BF),
-            V((MIX_CHUNKS, seqs, width // MIX_CHUNKS), BF), V((nx, MIX_CHUNKS, seqs, width // MIX_CHUNKS), BF),
+            V((nx, seqs, qc), BF), V((nx, seqs, qc), BF),
             V((2 * khs * dk, 3 * seqs), BF), V((heads, seqs, dv), F32),
             V((seqs, LANES), F32), V((heads, seqs, dv), F32), V((heads, seqs, dv), F32),
             V((width, 2 * he), BF), V((nx, he, qc), BF), V((nx, he, qc), BF),
-            V((nx * ch, seqs, LANES), BF), V((nx * ch, seqs, LANES), BF),
-            V((EP, msg, LANES), BF), V((nx, EP, msg, LANES), BF), V((nx, EP * msg, LANES), F32),
-            V((nx, EP * SLOTS, he), BF), V((EP * msg, LANES), F32),
+            V((nx * ch, seqs, LANES), BF), V((nx, wide, LANES), BF),
+            V((EP, msg, LANES), BF), V((nx, EP, msg, LANES), BF), V((nx, EP * msg // 2, LANES), F32),
+            V((2, nx, EP * SLOTS // 2, he), BF), V((EP * msg // 2, LANES), F32),
             V((EP, msg, LANES), BF), V((EP, msg, LANES), BF),
             V((nx, wide, LANES), BF), V((nx, wide, LANES), BF), V((nx, wide, LANES), BF),
-            dma((26,)), dma((NY,)), dma((NY,)), dma((4,)), dma((4,)), dma((4,)), dma((4,)), dma((NZ,)),
-            *[dma] * 29,
+            dma((18,)), dma((NY,)), dma((NY,)), dma((4,)), dma((4,)), dma((4,)), dma((4,)), dma((NZ,)),
+            dma((2,)), dma((2,)), *[dma] * 29,
         ],
         compiler_params=pltpu.CompilerParams(
             collective_id=1, has_side_effects=True, vmem_limit_bytes=LAYER_VMEM

time: 65.6 us -> 63.1 us (0.962)
  Pallas kernels: 64.9 us -> 62.4 us
    pallas_call x1, Pallas kernels: 62.8 us -> 60.3 us  [layer(): pl.pallas_call(layer_kernel, out_shape=(jax.ShapeDtypeStruct((seqs, width...]
where the time goes in v5:
time: 63.1 us; the launch traced here: 63 us
  Pallas kernels  62.4 us (99%)
  between operations  0.65 us (1%)
    pallas_call x1, Pallas kernels, layer(): pl.pallas_call(layer_kernel, out_shape=(jax.ShapeDtypeStruct((seqs, width...  60.3 us
    pallas_call x1, Pallas kernels, per_device(): pl.pallas_call(store_kernel, out_shape=(jax.ShapeDtypeStruct(layer_out.sh...  2.06 us

profile of v5, /device:TPU:1, one launch (start us, length us, event | category | flops | bytes accessed | tf_op | source)
XLA Modules:
  0.0 63.0 jit_solution(5529382281173983310)
XLA Ops:
  0.6 60.3 %layer.1 = (bf16[16,2048]{1,0:T(8,128)(2,1)S(1)}, f32[16,4,128,128]{3,2,1,0:T(8,128)S(1)}) custom-call(bf16[16,2048]{1,0:T(8,128)(2,1)} %tokens_h.1, bf16[2048]{0:T(1024)(128)(2,1)} %norm_gain_h.1, bf16[32,256]{1,0:T(8,128)(2,1)} %wq.1, bf16[32,256]{1,0:T(8,128)(2,1)} %wk.1, bf16[32,512]{1,0:T(8,128)(2,1)} %wv.1, bf16[32,512]{1,0:T(8,128)(2,1)} %wg.1, ...), custom_call_target="tpu_custom_call" | custom-call | tf_op jit(solution)/shard_map/layer/pallas_call | solution.py:528
  61.0 2.1 %store.1 = (bf16[16,2048]{1,0:T(8,128)(2,1)}, f32[16,4,128,128]{3,2,1,0:T(8,128)}) custom-call(bf16[16,2048]{1,0:T(8,128)(2,1)S(1)} %get-tuple-element.4.layer_in, f32[16,4,128,128]{3,2,1,0:T(8,128)S(1)} %get-tuple-element.5.state), custom_call_target="tpu_custom_call" | custom-call | tf_op jit(solution)/shard_map/store/pallas_call | solution.py:590

commit v6 on v5

--- a/solution.py
+++ b/solution.py
@@ -12,12 +12,14 @@
 EP = NZ * YC
 SLOTS = 2
 UNROLL = 2
-STATE_COPIES = 4
+STATE_COPIES = 8
 FAR = (4, 3, 5, 2, 6, 1, 7)
 NEAR = (1, 7, 2, 6, 3, 5, 4)
 GROUPS = ((0,), (1, 7), (2, 6), (3, 5, 4))
-SEND_ORDER = (0, 7, 1, 6, 2, 5, 3, 4)
-ARRIVAL = (0, 7, 1, 6, 2, 5, 3, 4)
+PAIRS = ((0,), (7, 1), (6,), (2, 5), (3, 4))
+ARRIVAL = tuple(d for g in PAIRS for d in g)
+PAIR = {d: i for i, g in enumerate(PAIRS) for d in g}
+NEAR_Z = 5
 GROUP = {d: i for i, g in enumerate(GROUPS) for d in g}
 LAYER_VMEM = 40 * 1024 * 1024
 LANES = 128
@@ -59,8 +61,8 @@
     wbuf, gbuf, tok_src, tokbuf, psend, prec, gsend, grec, obuf, sbuf, mix_send, mix_rec,
     kqt, vals, rs_ref, ro, corr,
     egu, dsrc, dbuf, tok_chunks, res_all, dsend, xrows, rowsf, act_all, outf, rsend, rrecv, sh_send, sh_rec, fin,
-    load_sem, w_r, gw_r, o1_r, o2_r, s1_r, s2_r, d_r,
-    x_r, a_r, t_r, wf_r, gf_r, p_r, g_r, o3_r, s3_r, m_r, ed_r, r_r, h_r, f_r, n_r,
+    load_sem, o1_r, o2_r, s1_r, s2_r, o3_r, d_r,
+    x_r, a_r, t_r, wf_r, gf_r, p_r, g_r, w_r, gw_r, s3_r, m_r, ed_r, r_r, h_r, f_r, n_r,
     t_s, w_s, gw_s, p_s, g_s, o_s, s_s, m_s, ed_s, d_s, x_s, a_s, r_s, h_s, f_s, n_s,
 ):
     e = lax.axis_index("ep")
@@ -131,19 +133,19 @@
         pl.semaphore_signal(barrier, inc=1, device_id=(e, xdev(d)), device_id_type=MESH)
 
     def rows_y(buf, ss, rs, fr):
-        rcopies = [rcopy(buf.at[yc], buf.at[yc], ss, rs.at[d], ydev(d), x) for d in ypeers]
+        for d in ypeers:
+            rcopy(buf.at[yc], buf.at[yc], ss, rs, ydev(d), x)
         rcopy(buf.at[yc], buf.at[yc], ss, fr, partner, x)
-        return dict(zip(ypeers, rcopies))
-
-    def rows_c(buf, over_y, ss, fr, which):
-        for d in which:
-            over_y[d].wait_recv()
+
+    def rows_c(buf, ss, rs, fr):
+        wait_all(buf.at[pl.ds(0, NY - 1)], rs)
+        for d in range(1, NY):
             j = lax.rem(y + NY - d, NY) * NC + c
             rcopy(buf.at[j], buf.at[j], ss, fr, partner, x)
 
     wait_all(wbuf.at[yc], w_load)
     pl.semaphore_wait(barrier, (NZ - 1) + (YC - 1) + (nx - 1))
-    ws = rows_y(wbuf, w_s, w_r, wf_r)
+    rows_y(wbuf, w_s, w_r, wf_r)
     for ref, sem in first:
         wait_all(ref, sem)
     normed = rms(tokens[...].astype(F32), norm_gain[...].reshape(1, width).astype(F32)).astype(BF)
@@ -153,7 +155,7 @@
     for d in FAR:
         rcopy(tok_src.at[lax.rem(z + d, NZ)], tokbuf.at[d], t_s, t_r, zdev(d), x)
     wait_all(gbuf.at[yc], g_load)
-    gws = rows_y(gbuf, gw_s, gw_r, gf_r)
+    rows_y(gbuf, gw_s, gw_r, gf_r)
     wait_all(obuf.at[e], o_load)
     wait_all(dsrc, ed_load)
 
@@ -169,17 +171,19 @@
             j = zb + yc
             for dy in ypeers:
                 rcopy(buf.at[j], buf.at[j], ss, rs.at[group], ydev(dy), x)
-            rcopy(buf.at[j], buf.at[j], ss, fr, partner, x)
+            rcopy(buf.at[j], buf.at[j], ss, fr(group), partner, x)
 
     def spread_c(buf, group, ss, rs, fr):
         wait_all(buf.at[pl.ds(0, len(GROUPS[group]) * (NY - 1))], rs.at[group])
         for zb in z_blocks(GROUPS[group]):
             for dy in range(1, NY):
                 j = zb + lax.rem(y + NY - dy, NY) * NC + c
-                rcopy(buf.at[j], buf.at[j], ss, fr, partner, x)
-
+                rcopy(buf.at[j], buf.at[j], ss, fr(group), partner, x)
+
+    last_o = lambda group: o3_r.at[1 if group == 3 else 0]
+    last_s = lambda group: s3_r
     spread_z(obuf, o_s, o1_r)
-    spread_y(obuf, 0, o_s, o2_r, o3_r)
+    spread_y(obuf, 0, o_s, o2_r, last_o)
     for d in peers:
         rcopy(dsrc.at[xdev(d)], dbuf.at[d], ed_s, ed_r, e, xdev(d))
     tokbuf[0] = tok_src[z]
@@ -203,10 +207,9 @@
         packed = jnp.where(lane == h, retain[h], packed)
         packed = jnp.where(lane == heads + h, strength[h], packed)
 
-    rows_c(wbuf, ws, w_s, wf_r, (1, 3))
+    rows_c(wbuf, w_s, w_r, wf_r)
     wait_all(obuf.at[pl.ds(0, len(GROUPS[1]))], o1_r.at[1])
-    spread_y(obuf, 1, o_s, o2_r, o3_r)
-    rows_c(wbuf, ws, w_s, wf_r, (2,))
+    spread_y(obuf, 1, o_s, o2_r, last_o)
     wait_all(tokbuf.at[pl.ds(1, NZ - 1)], t_r)
     wait_all(wbuf.at[pl.ds(0, NY)], wf_r)
     toks_all = tokbuf[...].reshape(NZ * seqs, kz)
@@ -229,20 +232,20 @@
         return total.astype(BF).astype(F32)
 
     project(wbuf, psend, prec, p_s, p_r)
-    rows_c(gbuf, gws, gw_s, gf_r, (1, 3, 2))
+    rows_c(gbuf, gw_s, gw_r, gf_r)
     wait_all(obuf.at[pl.ds(0, len(GROUPS[2]))], o1_r.at[2])
-    spread_y(obuf, 2, o_s, o2_r, o3_r)
+    spread_y(obuf, 2, o_s, o2_r, last_o)
     wait_all(gbuf.at[pl.ds(0, NY)], gf_r)
     project(gbuf, gsend, grec, g_s, g_r)
     wait_all(obuf.at[pl.ds(0, len(GROUPS[3]))], o1_r.at[3])
-    spread_y(obuf, 3, o_s, o2_r, o3_r)
+    spread_y(obuf, 3, o_s, o2_r, last_o)
     wait_all(sbuf.at[e], s_load)
     spread_z(sbuf, s_s, s1_r)
 
     def s_relay(group):
         if group:
             wait_all(sbuf.at[pl.ds(0, len(GROUPS[group]))], s1_r.at[group])
-        spread_y(sbuf, group, s_s, s2_r, s3_r)
+        spread_y(sbuf, group, s_s, s2_r, last_s)
 
 
     ch = qc // LANES
@@ -295,7 +298,7 @@
 
     proj = collected(psend, prec, p_r)
     for group in range(3):
-        spread_c(obuf, group, o_s, o2_r, o3_r)
+        spread_c(obuf, group, o_s, o2_r, last_o)
     khs = wq.shape[1] // dk
     per = heads // khs
     kq = []
@@ -349,17 +352,26 @@
 
     lax.fori_loop(0, seqs // 2, read_pair, 0, unroll=UNROLL)
 
-    spread_c(obuf, 3, o_s, o2_r, o3_r)
+    spread_c(obuf, 3, o_s, o2_r, last_o)
     gate = collected(gsend, grec, g_r)
     hg = head_gain[...].reshape(1, dv).astype(F32)
     parts = [rms(ro[h], hg) * silu(gate[:, h * dv : (h + 1) * dv]) for h in range(heads)]
     heads_out = jnp.concatenate(parts, axis=1).astype(BF)
-    wait_all(obuf.at[pl.ds(0, EP // NC)], o3_r)
-    mix = nt_dot(heads_out, obuf[...].reshape(width, heads * dv)).astype(BF)
-    for q in range(nx):
-        mix_send[q] = mix[:, q * qc : (q + 1) * qc]
+    def project_out(which):
+        for zb in z_blocks(which):
+            zi = lax.div(zb, YC)
+            mix_send[zi] = nt_dot(
+                heads_out, obuf[pl.ds(zb, YC)].reshape(YC * obuf.shape[1], heads * dv)
+            ).astype(BF)
+
+    wait_all(obuf.at[pl.ds(0, NEAR_Z * NY)], o3_r.at[0])
+    project_out([d for g in GROUPS[:3] for d in g])
+    wait_all(obuf.at[pl.ds(0, (NZ - NEAR_Z) * NY)], o3_r.at[1])
+    project_out(GROUPS[3])
+    zq = NZ // nx
     for d in peers:
-        rcopy(mix_send.at[xdev(d)], mix_rec.at[d], m_s, m_r, e, xdev(d))
+        q = xdev(d)
+        rcopy(mix_send.at[pl.ds(q * zq, zq)], mix_rec.at[d], m_s, m_r, e, q)
     def write_pair(p, carry):
         both = spread_columns(2 * p, khs * dk)
         for j in range(2):
@@ -375,9 +387,10 @@
     s_relay(0)
     s_relay(1)
     wait_all(mix_rec.at[pl.ds(1, nx - 1)], m_r)
-    mixed = mix_send[x].astype(F32)
+    mixed = mix_send[pl.ds(x * zq, zq)].astype(F32)
     for d in range(1, nx):
         mixed = mixed + mix_rec[d].astype(F32)
+    mixed = jnp.concatenate([mixed[i] for i in range(zq)], axis=1)
     own = tok_chunks[pl.ds(x * ch, ch)].astype(F32)
     mine = jnp.concatenate(
         [own[cc] + mixed[:, cc * LANES : (cc + 1) * LANES] for cc in range(ch)], axis=0
@@ -393,48 +406,41 @@
     place_of = {dz: i * YC for i, dz in enumerate(ARRIVAL)}
     half = EP // 2
     part_of = lambda dz: place_of[dz] // half
-    for dz in SEND_ORDER:
+    for dz in ARRIVAL:
         for d in range(YC):
             if dz or d:
                 to = zbase[dz] + ypart[d]
-                rcopy(dsend.at[to], xrows.at[x, place_of[dz] + d], d_s, d_r.at[dz], to, x)
+                rcopy(dsend.at[to], xrows.at[x, place_of[dz] + d], d_s, d_r.at[PAIR[dz]], to, x)
     xrows[x, 0] = dsend[e]
     for d in peers:
         rcopy(res_all.at[x], res_all.at[x], n_s, n_r, e, xdev(d))
-    for dz in ARRIVAL:
-        n = YC if dz else YC - 1
-        wait_all(xrows.at[x, pl.ds(place_of[dz], n)], d_r.at[dz])
-        block = xrows.at[x, pl.ds(place_of[dz], YC)]
+    for i, group in enumerate(PAIRS):
+        n = len(group) * YC - (0 in group)
+        at = pl.ds(place_of[group[0]], len(group) * YC)
+        wait_all(xrows.at[x, pl.ds(place_of[group[0]], n)], d_r.at[i])
         for d in peers:
-            rcopy(block, block, x_s, x_r.at[part_of(dz)], e, xdev(d))
+            block = xrows.at[x, at]
+            rcopy(block, block, x_s, x_r.at[part_of(group[0])], e, xdev(d))
     s_relay(2)
     s_relay(3)
+    for group in (0, 1):
+        spread_c(sbuf, group, s_s, s2_r, last_s)
     wait_all(egu, e_load)
     fgain = ffn_gain[...].reshape(1, width).astype(F32)
     nrows = half * SLOTS
 
-    def dense_branch():
-        for group in range(4):
-            spread_c(sbuf, group, s_s, s2_r, s3_r)
-        wait_all(sbuf.at[pl.ds(0, EP // NC)], s3_r)
+    def full_rows():
         wait_all(res_all.at[pl.ds(0, nx - 1)], n_r)
         residual = jnp.concatenate(
             [res_all[i // ch, (i % ch) * seqs : (i % ch + 1) * seqs, :] for i in range(nx * ch)], axis=1
         ).astype(F32)
         ffn_in = rms(residual, fgain).astype(BF)
-        sgu = jnp.dot(ffn_in, sbuf[:, :, 0 : 2 * hs].reshape(width, 2 * hs), preferred_element_type=F32)
-        sact = (silu(sgu[:, 0:hs]) * sgu[:, hs:]).astype(BF)
-        spart = nt_dot(sact, sbuf[:, :, 2 * hs :].reshape(width, hs)).astype(BF)
-        for i in range(nx * ch):
-            sh_send[i // ch, (i % ch) * seqs : (i % ch + 1) * seqs, :] = spart[:, i * LANES : (i + 1) * LANES]
-        for d in peers:
-            rcopy(sh_send.at[xdev(d)], sh_rec.at[d], h_s, h_r, e, xdev(d))
         branch = sigmoid(
             jnp.sum(
                 ffn_in.astype(F32) * branch_gate[...].reshape(1, width).astype(F32), axis=1, keepdims=True
             )
         )
-        return branch
+        return ffn_in, branch
 
     for p in range(2):
         wait_all(xrows.at[pl.ds(1, nx - 1), pl.ds(p * half, half)], x_r.at[p])
@@ -463,6 +469,9 @@
 
     wait_all(dbuf.at[pl.ds(1, nx - 1)], ed_r)
     for p in range(2):
+        if p == 1:
+            spread_c(sbuf, 2, s_s, s2_r, last_s)
+            ffn_in, branch = full_rows()
         eout = jnp.dot(act_all[p, 0], dsrc[x], preferred_element_type=F32)
         wait_all(act_all.at[p, pl.ds(1, nx - 1)], a_r.at[p])
         for d in range(1, nx):
@@ -475,7 +484,15 @@
                 if part_of(dz) == p and (dz or d):
                     rcopy(rsend.at[place_of[dz] + d], rrecv.at[e], r_s, r_r, zback[dz] + yback[d], x)
     rrecv[e] = rsend[0]
-    branch = dense_branch()
+    spread_c(sbuf, 3, s_s, s2_r, last_s)
+    wait_all(sbuf.at[pl.ds(0, EP // NC)], s3_r)
+    sgu = jnp.dot(ffn_in, sbuf[:, :, 0 : 2 * hs].reshape(width, 2 * hs), preferred_element_type=F32)
+    sact = (silu(sgu[:, 0:hs]) * sgu[:, hs:]).astype(BF)
+    spart = nt_dot(sact, sbuf[:, :, 2 * hs :].reshape(width, hs)).astype(BF)
+    for i in range(nx * ch):
+        sh_send[i // ch, (i % ch) * seqs : (i % ch + 1) * seqs, :] = spart[:, i * LANES : (i + 1) * LANES]
+    for d in peers:
+        rcopy(sh_send.at[xdev(d)], sh_rec.at[d], h_s, h_r, e, xdev(d))
     shared = sh_send[x].astype(F32)
     wait_all(sh_rec.at[pl.ds(1, nx - 1)], h_r)
     for d in range(1, nx):
@@ -541,7 +558,7 @@
             V((NZ, seqs, cols - wg.shape[1]), BF), V((NZ, seqs, cols - wg.shape[1]), BF),
             V((NZ, seqs, wg.shape[1]), BF), V((NZ, seqs, wg.shape[1]), BF),
             V((EP, ow.shape[1], ow.shape[0]), BF), V((EP, sg.shape[0], 3 * hs), BF),
-            V((nx, seqs, qc), BF), V((nx, seqs, qc), BF),
+            V((NZ, seqs, width // NZ), BF), V((nx, NZ // nx, seqs, width // NZ), BF),
             V((2 * khs * dk, 3 * seqs), BF), V((heads, seqs, dv), F32),
             V((seqs, LANES), F32), V((heads, seqs, dv), F32), V((heads, seqs, dv), F32),
             V((width, 2 * he), BF), V((nx, he, qc), BF), V((nx, he, qc), BF),
@@ -550,8 +567,8 @@
             V((2, nx, EP * SLOTS // 2, he), BF), V((EP * msg // 2, LANES), F32),
             V((EP, msg, LANES), BF), V((EP, msg, LANES), BF),
             V((nx, wide, LANES), BF), V((nx, wide, LANES), BF), V((nx, wide, LANES), BF),
-            dma((18,)), dma((NY,)), dma((NY,)), dma((4,)), dma((4,)), dma((4,)), dma((4,)), dma((NZ,)),
-            dma((2,)), dma((2,)), *[dma] * 29,
+            dma((18,)), dma((4,)), dma((4,)), dma((4,)), dma((4,)), dma((2,)), dma((5,)),
+            dma((2,)), dma((2,)), *[dma] * 30,
         ],
         compiler_params=pltpu.CompilerParams(
             collective_id=1, has_side_effects=True, vmem_limit_bytes=LAYER_VMEM

time: 63.1 us -> 62.8 us (level)
  no operation moved by 1% of the time
where the time goes in v6:
time: 62.8 us
  Pallas kernels  62.1 us (99%)
  between operations  0.65 us (1%)
    pallas_call x1, Pallas kernels, layer(): pl.pallas_call(layer_kernel, out_shape=(jax.ShapeDtypeStruct((seqs, width...  60 us
    pallas_call x1, Pallas kernels, per_device(): pl.pallas_call(store_kernel, out_shape=(jax.ShapeDtypeStruct(layer_out.sh...  2.09 us

profile of v6, /device:TPU:1, one launch (start us, length us, event | category | flops | bytes accessed | tf_op | source)
XLA Modules:
  0.0 62.8 jit_solution(6265386788221308678)
XLA Ops:
  0.6 60.0 %layer.1 = (bf16[16,2048]{1,0:T(8,128)(2,1)S(1)}, f32[16,4,128,128]{3,2,1,0:T(8,128)S(1)}) custom-call(bf16[16,2048]{1,0:T(8,128)(2,1)} %tokens_h.1, bf16[2048]{0:T(1024)(128)(2,1)} %norm_gain_h.1, bf16[32,256]{1,0:T(8,128)(2,1)} %wq.1, bf16[32,256]{1,0:T(8,128)(2,1)} %wk.1, bf16[32,512]{1,0:T(8,128)(2,1)} %wv.1, bf16[32,512]{1,0:T(8,128)(2,1)} %wg.1, ...), custom_call_target="tpu_custom_call" | custom-call | tf_op jit(solution)/shard_map/layer/pallas_call | solution.py:545
  60.7 2.1 %store.1 = (bf16[16,2048]{1,0:T(8,128)(2,1)}, f32[16,4,128,128]{3,2,1,0:T(8,128)}) custom-call(bf16[16,2048]{1,0:T(8,128)(2,1)S(1)} %get-tuple-element.4.layer_in, f32[16,4,128,128]{3,2,1,0:T(8,128)S(1)} %get-tuple-element.5.state), custom_call_target="tpu_custom_call" | custom-call | tf_op jit(solution)/shard_map/store/pallas_call | solution.py:607

commit v7 on v6

--- a/solution.py
+++ b/solution.py
@@ -57,7 +57,7 @@
     tokens_h, norm_gain_h, wq, wk, wv, wg, bw_h, dw_h, rate_h, bias_h, head_gain_h, rec, ow_h, ffn_gain_h,
     routes_h, rweight_h, eg_h, eu_h, ed_h, sg_h, su_h, sd_h, branch_h,
     out_ref, state,
-    tokens, norm_gain, bw, dw, rate, bias, head_gain, ffn_gain, routes, rweight, branch_gate,
+    tokens, norm_gain, bd, rate, bias, head_gain, ffn_gain, routes, rweight, branch_gate,
     wbuf, gbuf, tok_src, tokbuf, psend, prec, gsend, grec, obuf, sbuf, mix_send, mix_rec,
     kqt, vals, rs_ref, ro, corr,
     egu, dsrc, dbuf, tok_chunks, res_all, dsend, xrows, rowsf, act_all, outf, rsend, rrecv, sh_send, sh_rec, fin,
@@ -89,6 +89,16 @@
         cp.start()
         return cp
 
+    barrier = pltpu.get_barrier_semaphore()
+    zbase = [lax.rem(z + d, NZ) * YC for d in range(NZ)]
+    ypart = [lax.rem(yc + d, YC) for d in range(YC)]
+    for dz in (4, 3, 5, 2, 6, 1, 7):
+        pl.semaphore_signal(barrier, inc=1, device_id=(zbase[dz] + yc, x), device_id_type=MESH)
+    for d in range(1, YC):
+        pl.semaphore_signal(barrier, inc=1, device_id=(zbase[0] + ypart[d], x), device_id_type=MESH)
+    for d in range(1, nx):
+        pl.semaphore_signal(barrier, inc=1, device_id=(e, xdev(d)), device_id_type=MESH)
+
     count = [0]
 
     def load(*pairs):
@@ -110,10 +120,11 @@
     small = [
         (b, load((a, b)))
         for a, b in (
-            (bw_h, bw), (dw_h, dw), (rate_h, rate), (bias_h, bias), (head_gain_h, head_gain),
+            (rate_h, rate), (bias_h, bias), (head_gain_h, head_gain),
             (ffn_gain_h, ffn_gain), (routes_h, routes), (rweight_h, rweight), (branch_h, branch_gate),
         )
     ]
+    bd_load = load((bw_h, bd.at[0]), (dw_h, bd.at[1]))
     hs = sg_h.shape[1]
     s_load = load(
         *((a, sbuf.at[e, :, i * hs : (i + 1) * hs]) for i, a in enumerate((sg_h, su_h, sd_h)))
@@ -121,16 +132,6 @@
     state_load = load((rec, state))
     he = eg_h.shape[2]
     e_load = load((eg_h.at[0], egu.at[:, 0:he]), (eu_h.at[0], egu.at[:, he : 2 * he]))
-
-    barrier = pltpu.get_barrier_semaphore()
-    zbase = [lax.rem(z + d, NZ) * YC for d in range(NZ)]
-    ypart = [lax.rem(yc + d, YC) for d in range(YC)]
-    for dz in (4, 3, 5, 2, 6, 1, 7):
-        pl.semaphore_signal(barrier, inc=1, device_id=(zbase[dz] + yc, x), device_id_type=MESH)
-    for d in range(1, YC):
-        pl.semaphore_signal(barrier, inc=1, device_id=(zbase[0] + ypart[d], x), device_id_type=MESH)
-    for d in range(1, nx):
-        pl.semaphore_signal(barrier, inc=1, device_id=(e, xdev(d)), device_id_type=MESH)
 
     def rows_y(buf, ss, rs, fr):
         for d in ypeers:
@@ -190,8 +191,9 @@
 
     for ref, sem in small:
         wait_all(ref, sem)
-    bl = nt_dot(normed, bw[...])
-    dl = nt_dot(normed, dw[...])
+    wait_all(bd, bd_load)
+    bl = nt_dot(normed, bd[0])
+    dl = nt_dot(normed, bd[1])
     lanes = iota(bl.shape, 1)
     retain, strength = [], []
     for h in range(heads):
@@ -446,23 +448,15 @@
         wait_all(xrows.at[pl.ds(1, nx - 1), pl.ds(p * half, half)], x_r.at[p])
         for q in range(nx):
             rowsf[q] = xrows[q, p * half : (p + 1) * half].reshape(half * msg, LANES).astype(F32)
-        piece = lambda q, cc: rowsf[q, pl.ds(cc, nrows, stride=ch), :]
         squares = jnp.zeros((nrows, LANES), F32)
-        for q in range(nx):
-            for cc in range(ch):
-                v = piece(q, cc)
-                squares = squares + v * v
-        inv = lax.rsqrt(jnp.sum(squares, axis=1, keepdims=True) / width + EPS)
         gu = jnp.zeros((nrows, 2 * he), F32)
         for q in range(nx):
-            left = jnp.concatenate(
-                [
-                    piece(q, cc) * inv * fgain[:, q * qc + cc * LANES : q * qc + (cc + 1) * LANES]
-                    for cc in range(ch)
-                ],
-                axis=1,
-            ).astype(BF)
+            pieces = [rowsf[q, pl.ds(cc, nrows, stride=ch), :] for cc in range(ch)]
+            for v in pieces:
+                squares = squares + v * v
+            left = (jnp.concatenate(pieces, axis=1) * fgain[:, q * qc : (q + 1) * qc]).astype(BF)
             gu = gu + jnp.dot(left, egu[q * qc : (q + 1) * qc, :], preferred_element_type=F32)
+        gu = gu * lax.rsqrt(jnp.sum(squares, axis=1, keepdims=True) / width + EPS)
         act_all[p, 0] = (silu(gu[:, 0:he]) * gu[:, he:]).astype(BF)
         for d in peers:
             rcopy(act_all.at[p, 0], act_all.at[p, d], a_s, a_r.at[p], e, xdev(d))
@@ -551,7 +545,7 @@
         in_specs=[hbm] * 23,
         out_specs=(vmem,) * 2,
         scratch_shapes=[
-            V((seqs, width), BF), V((width,), BF), V(bw.shape[::-1], BF), V(dw.shape[::-1], BF),
+            V((seqs, width), BF), V((width,), BF), V((2, *bw.shape[::-1]), BF),
             pltpu.SMEM((heads,), F32), pltpu.SMEM((heads,), F32), V((dv,), BF), V((width,), BF),
             V((topk, seqs), I32), V((topk, seqs), F32), V((width,), BF),
             V((YC, rows, cols - wg.shape[1]), BF), V((YC, rows, wg.shape[1]), BF), V((NZ, seqs, kz), BF), V((NZ, seqs, kz), BF),
@@ -567,7 +561,7 @@
             V((2, nx, EP * SLOTS // 2, he), BF), V((EP * msg // 2, LANES), F32),
             V((EP, msg, LANES), BF), V((EP, msg, LANES), BF),
             V((nx, wide, LANES), BF), V((nx, wide, LANES), BF), V((nx, wide, LANES), BF),
-            dma((18,)), dma((4,)), dma((4,)), dma((4,)), dma((4,)), dma((2,)), dma((5,)),
+            dma((17,)), dma((4,)), dma((4,)), dma((4,)), dma((4,)), dma((2,)), dma((5,)),
             dma((2,)), dma((2,)), *[dma] * 30,
         ],
         compiler_params=pltpu.CompilerParams(

time: 62.8 us -> 62.8 us (level)
  no operation moved by 1% of the time
where the time goes in v7:
time: 62.8 us; the launch traced here: 62.7 us
  Pallas kernels  62 us (99%)
  between operations  0.65 us (1%)
    pallas_call x1, Pallas kernels, layer(): pl.pallas_call(layer_kernel, out_shape=(jax.ShapeDtypeStruct((seqs, width...  60 us
    pallas_call x1, Pallas kernels, per_device(): pl.pallas_call(store_kernel, out_shape=(jax.ShapeDtypeStruct(layer_out.sh...  2.09 us

profile of v7, /device:TPU:1, one launch (start us, length us, event | category | flops | bytes accessed | tf_op | source)
XLA Modules:
  0.0 62.7 jit_solution(14579102495976006521)
XLA Ops:
  0.6 60.0 %layer.1 = (bf16[16,2048]{1,0:T(8,128)(2,1)S(1)}, f32[16,4,128,128]{3,2,1,0:T(8,128)S(1)}) custom-call(bf16[16,2048]{1,0:T(8,128)(2,1)} %tokens_h.1, bf16[2048]{0:T(1024)(128)(2,1)} %norm_gain_h.1, bf16[32,256]{1,0:T(8,128)(2,1)} %wq.1, bf16[32,256]{1,0:T(8,128)(2,1)} %wk.1, bf16[32,512]{1,0:T(8,128)(2,1)} %wv.1, bf16[32,512]{1,0:T(8,128)(2,1)} %wg.1, ...), custom_call_target="tpu_custom_call" | custom-call | tf_op jit(solution)/shard_map/layer/pallas_call | solution.py:539
  60.6 2.1 %store.1 = (bf16[16,2048]{1,0:T(8,128)(2,1)}, f32[16,4,128,128]{3,2,1,0:T(8,128)}) custom-call(bf16[16,2048]{1,0:T(8,128)(2,1)S(1)} %get-tuple-element.4.layer_in, f32[16,4,128,128]{3,2,1,0:T(8,128)S(1)} %get-tuple-element.5.state), custom_call_target="tpu_custom_call" | custom-call | tf_op jit(solution)/shard_map/store/pallas_call | solution.py:601
